TPU v7x, 512 devices: a whole 4x4x16 slice. The times are simulated.
512 devices in a mesh: sp: 32 (over z, core), tp: 16 (over y, x).
Axes of the slice: x: 4, y: 4, z: 16, core: 2. Of those that a mesh axis runs over, the one named last changes fastest.
Arguments:
- residual: bfloat16 [4096, 2048], P('sp'), may hold values from -45 to 45
- query_a: bfloat16 [4096, 16, 128], P('sp', 'tp'), may hold values from -125 to 125
- keys_a: bfloat16 [4096, 16, 128], P('sp', 'tp'), may hold values from -8 to 8
- values_a: bfloat16 [4096, 16, 128], P('sp', 'tp'), may hold values from -6 to 6
- query_b: bfloat16 [4096, 16, 256], P('sp', 'tp'), may hold values from -125 to 125
- keys_b: bfloat16 [4096, 16, 256], P('sp', 'tp'), may hold values from -8 to 8
- values_b: bfloat16 [4096, 16, 256], P('sp', 'tp'), may hold values from -6 to 6
- lambda_a: float32 [16], P('tp'), may hold values from 0.3 to 0.8
- lambda_b: float32 [16], P('tp'), may hold values from 0.3 to 0.8
- gain_a: float32 [128], replicated, may hold values from 0.1 to 1.9
- gain_b: float32 [256], replicated, may hold values from 0.1 to 1.9
- proj_a: bfloat16 [2048, 2048], P('tp'), may hold values from -0.078125 to 0.078125
- proj_b: bfloat16 [4096, 2048], P('tp'), may hold values from -0.078125 to 0.078125
- norm_gain: float32 [2048], replicated, may hold values from 0.1 to 1.9
- routes: int32 [4096, 2], P('sp'), may hold values from 0 to 31, all different within a row; in each aligned block of 128 rows (0 to 127, 128 to 255, ...) at most 16 rows name the same one
- route_weight: float32 [4096, 2], P('sp'), may hold values from 0.2 to 2
- expert_gate: bfloat16 [32, 2048, 2048], P('sp', None, 'tp'), may hold values from -0.125 to 0.125
- expert_up: bfloat16 [32, 2048, 2048], P('sp', None, 'tp'), may hold values from -0.125 to 0.125
- expert_down: bfloat16 [32, 2048, 2048], P('sp', 'tp'), may hold values from -0.125 to 0.125
Outputs:
- layer_out: bfloat16 [4096, 2048], P('sp', 'tp')
Inputs may be any that keep to these rules, and one draw needn't show every extreme that they name: `routes`: each row names 2 different experts; in each aligned block of 128 rows no expert is named more than 16 times, a bound that some block reaches.
All inputs are finite; a program needn't handle non-finite values.
Results may differ from a plain program's by a relative error of at most 0.013.
Values may be sent and summed in bfloat16 or wider, within the bound.
No kernel may reach another device: no remote copies, remote signals or barrier semaphores. Data moves between devices by JAX's collectives and lax.ppermute only.
A program may use at most 64 MiB of HBM per device.

v0:
```python
import functools

import jax
import jax.numpy as jnp
from jax import lax
from jax.experimental import pallas as pl
from jax.experimental.pallas import tpu as pltpu
from jax.sharding import PartitionSpec as P


DK_A = 64
DK_B = 128
SEG = 64
TOP = 2
LINE = 4
EPS = 1e-06
LOW = -1e30


VMEM = pl.BlockSpec(memory_space=pltpu.VMEM)
SMEM = pl.BlockSpec(memory_space=pltpu.SMEM)
HBM = pl.BlockSpec(memory_space=pltpu.HBM)

MAPS = (
    (slice(0, 128), slice(0, 128), slice(128, 256), slice(0, 128), DK_A**-0.5),
    (slice(128, 256), slice(0, 128), slice(128, 256), slice(128, 256), DK_A**-0.5),
    (slice(256, 384), slice(256, 384), slice(512, 768), slice(256, 512), DK_B**-0.5),
    (slice(384, 512), slice(384, 512), slice(512, 768), slice(512, 768), DK_B**-0.5),
)
SUMS = 768
STATE = SUMS + 8


def absorb(first, blocks, flag_ref, own_q_ref, got_q_ref, *refs):
    kv_refs = refs[:blocks]
    olds = None if first else refs[blocks : blocks + 2]
    outs = refs[-2:]
    half = outs[0].shape[1]

    def both(refs, rows):
        return jnp.concatenate([r[rows, :] for r in refs], axis=1)

    def keep(rows, value):
        outs[0][rows, :] = value[:, :half]
        outs[1][rows, :] = value[:, half:]

    def work():
        for index, (q_cols, k_cols, v_cols, rows, factor) in enumerate(MAPS):
            keys = jnp.concatenate([r[:, k_cols] for r in kv_refs], axis=0)
            queries = jnp.concatenate([own_q_ref[:, q_cols], got_q_ref[:, q_cols]], axis=0)
            values = jnp.concatenate([r[:, v_cols] for r in kv_refs], axis=0)
            scores = (
                lax.dot_general(
                    keys,
                    queries,
                    (((1,), (1,)), ((), ())),
                    preferred_element_type=jnp.float32,
                )
                * factor
            )
            at_max = slice(SUMS + index, SUMS + index + 1)
            at_sum = slice(SUMS + 4 + index, SUMS + 5 + index)
            if first:
                key_seg = lax.broadcasted_iota(jnp.int32, scores.shape, 0) // SEG
                column = lax.broadcasted_iota(jnp.int32, scores.shape, 1)
                query_seg = jnp.where(
                    column < half, column // SEG, (column - half) // SEG + flag_ref[0]
                )
                visible = key_seg <= query_seg
                scores = jnp.where(visible, scores, LOW)
                new_max = jnp.max(scores, axis=0, keepdims=True)
                expo = jnp.where(visible, jnp.exp(scores - new_max), 0.0)
            else:
                old_max = both(olds, at_max)
                new_max = jnp.maximum(old_max, jnp.max(scores, axis=0, keepdims=True))
                expo = jnp.exp(scores - new_max)
            total = jnp.sum(expo, axis=0, keepdims=True)
            summed = lax.dot_general(
                values,
                expo.astype(jnp.bfloat16),
                (((0,), (0,)), ((), ())),
                preferred_element_type=jnp.float32,
            )
            if not first:
                shrink = jnp.exp(old_max - new_max)
                total = total + both(olds, at_sum) * shrink
                summed = summed + both(olds, rows) * shrink
            keep(rows, summed)
            keep(at_max, new_max)
            keep(at_sum, total)

    if first:
        work()
    else:
        pl.when(flag_ref[0] > 0)(work)

        @pl.when(flag_ref[0] <= 0)
        def _():
            outs[0][...] = olds[0][...]
            outs[1][...] = olds[1][...]


def absorbed(flag, queries, kvs, olds):
    half = queries[0].shape[0]
    shape = jax.ShapeDtypeStruct((STATE, half), jnp.float32)
    keys = len(kvs) * kvs[0].shape[0]
    return pl.pallas_call(
        functools.partial(absorb, olds is None, len(kvs)),
        out_shape=(shape, shape),
        in_specs=[SMEM] + [VMEM] * (2 + len(kvs) + (0 if olds is None else 2)),
        out_specs=(VMEM, VMEM),
        cost_estimate=pl.CostEstimate(
            flops=2 * 2 * half * keys * (512 + SUMS), bytes_accessed=0, transcendentals=0
        ),
        compiler_params=pltpu.CompilerParams(vmem_limit_bytes=12 << 20),
        name="absorb",
    )(flag, *queries, *kvs, *(olds or ()))


def pack(qa_ref, qb_ref, ka_ref, va_ref, kb_ref, vb_ref, q_ref, kv_ref, qa_buf, sems):
    width = qa_buf.shape[1]
    places = (
        (qa_ref, qa_buf),
        (ka_ref, kv_ref.at[:, :width]),
        (va_ref, kv_ref.at[:, width : 2 * width]),
        (kb_ref, kv_ref.at[:, 2 * width : 4 * width]),
        (vb_ref, kv_ref.at[:, 4 * width :]),
        (qb_ref, q_ref.at[:, 2 * width :]),
    )
    copies = [pltpu.make_async_copy(a, b, sems.at[i]) for i, (a, b) in enumerate(places)]
    for copy in copies:
        copy.start()
    for copy in copies:
        copy.wait()
    both = qa_buf[...]
    first = lax.broadcasted_iota(jnp.int32, both.shape, 1) < DK_A
    q_ref[:, :width] = jnp.where(first, both, 0)
    q_ref[:, width : 2 * width] = jnp.where(first, 0, both)


def pack_weights(gate_ref, up_ref, down_ref, out_ref, sems):
    deep, width = gate_ref.shape
    places = [(gate_ref, out_ref.at[:deep, :width]), (up_ref, out_ref.at[:deep, width:])]
    for j in range(deep // (2 * width)):
        start = deep + j * width
        places.append(
            (
                down_ref.at[:, 2 * j * width : 2 * (j + 1) * width],
                out_ref.at[start : start + width, :],
            )
        )
    copies = [pltpu.make_async_copy(a, b, sems.at[i]) for i, (a, b) in enumerate(places)]
    for copy in copies:
        copy.start()
    for copy in copies:
        copy.wait()


def finish(mix_ref, own_ref, got_ref, gain_a_ref, gain_b_ref, from_a_ref, from_b_ref, out_ref, *bufs):
    proj_a_ref, proj_b_ref, sems = bufs
    copy_a = pltpu.make_async_copy(from_a_ref, proj_a_ref, sems.at[0])
    copy_b = pltpu.make_async_copy(from_b_ref, proj_b_ref, sems.at[1])
    copy_a.start()
    copy_b.start()

    def merged(index):
        at_max = slice(SUMS + index, SUMS + index + 1)
        at_sum = slice(SUMS + 4 + index, SUMS + 5 + index)
        rows = MAPS[index][3]
        own_max, got_max = own_ref[at_max, :], got_ref[at_max, :]
        new_max = jnp.maximum(own_max, got_max)
        own_w, got_w = jnp.exp(own_max - new_max), jnp.exp(got_max - new_max)
        total = own_ref[at_sum, :] * own_w + got_ref[at_sum, :] * got_w
        return own_ref[rows, :] * (own_w / total) + got_ref[rows, :] * (got_w / total)

    def head(index, mixing, gain_ref):
        mixed = merged(index) - mixing * merged(index + 1)
        mean_sq = jnp.mean(mixed * mixed, axis=0, keepdims=True)
        gain = jnp.broadcast_to(gain_ref[...], mixed.shape[::-1]).T
        return (mixed * lax.rsqrt(mean_sq + EPS) * gain).astype(jnp.bfloat16)

    heads_a = head(0, mix_ref[0], gain_a_ref)
    heads_b = head(2, mix_ref[1], gain_b_ref)
    copy_a.wait()
    copy_b.wait()
    width = out_ref.shape[2]
    across = (((0,), (0,)), ((), ()))
    step = 4
    for piece in range(0, out_ref.shape[0], step):
        cols = slice(piece * width, (piece + step) * width)
        branch = lax.dot_general(
            heads_a, proj_a_ref[:, cols], across, preferred_element_type=jnp.float32
        ) + lax.dot_general(
            heads_b, proj_b_ref[:, cols], across, preferred_element_type=jnp.float32
        )
        for i in range(step):
            out_ref[piece + i] = branch[:, i * width : (i + 1) * width].astype(jnp.bfloat16)


def experts(rows_ref, gain_ref, *refs):
    froms, out_ref, bufs, sems = refs[:LINE], refs[LINE], refs[LINE + 1 : -1], refs[-1]
    copies = [pltpu.make_async_copy(a, b, sems.at[i]) for i, (a, b) in enumerate(zip(froms, bufs))]
    for copy in copies:
        copy.start()
    parts, _, width = rows_ref.shape
    model_width = parts * width
    rows = jnp.concatenate([rows_ref[i] for i in range(parts)], axis=1).astype(jnp.float32)
    mean_sq = jnp.sum(rows * rows, axis=1, keepdims=True) / model_width
    normed = (rows * lax.rsqrt(mean_sq + EPS) * gain_ref[...]).astype(jnp.bfloat16)

    def dot(a, b):
        return jnp.dot(a, b, preferred_element_type=jnp.float32)

    hidden = []
    for copy, ref in zip(copies, bufs):
        copy.wait()
        both = dot(normed, ref[:model_width, :])
        gate, up = both[:, :width], both[:, width:]
        hidden.append((gate / (1.0 + jnp.exp(-gate)) * up).astype(jnp.bfloat16))
    for j in range(parts // 2):
        start = model_width + j * width
        down = dot(hidden[0], bufs[0][start : start + width, :])
        for i in range(1, LINE):
            down = down + dot(hidden[i], bufs[i][start : start + width, :])
        out_ref[2 * j] = down[:, :width].astype(jnp.bfloat16)
        out_ref[2 * j + 1] = down[:, width:].astype(jnp.bfloat16)


def held(value):
    return pltpu.with_memory_space_constraint(value, pltpu.HBM)


def summed_on_arrival(pieces, axis):
    arrived = lax.all_to_all(pieces, axis, split_axis=0, concat_axis=0, tiled=True)
    return arrived.astype(jnp.float32)


def local(
    residual,
    query_a,
    keys_a,
    values_a,
    query_b,
    keys_b,
    values_b,
    lambda_a,
    lambda_b,
    gain_a,
    gain_b,
    proj_a,
    proj_b,
    norm_gain,
    routes,
    route_weight,
    expert_gate,
    expert_up,
    expert_down,
):
    tok_rows = residual.shape[0]
    model_width = residual.shape[1]
    seq_devices = lax.axis_size("sp")
    head_devices = lax.axis_size("tp")
    head_index = lax.axis_index("tp")
    seq_index = lax.axis_index("sp")
    columns = model_width // head_devices

    chips = seq_devices // 2
    chip, core = seq_index // 2, seq_index % 2
    partner = [(i, i ^ 1) for i in range(seq_devices)]
    half_way = chips // 2

    def onward(step, down_blocks):
        up = [(2 * i, 2 * (i + 1)) for i in range(step - 1, chips - 1)]
        places = [(block - step) % chips for block in range(down_blocks)]
        return up + [(2 * ((i + 1) % chips) + 1, 2 * i + 1) for i in places]

    fields = [a[:, 0] for a in (query_a, query_b, keys_a, values_a, keys_b, values_b)]
    own_q, own_kv = pl.pallas_call(
        pack,
        out_shape=(
            jax.ShapeDtypeStruct((tok_rows, 4 * DK_B), jnp.bfloat16),
            jax.ShapeDtypeStruct((tok_rows, SUMS), jnp.bfloat16),
        ),
        in_specs=[HBM] * 6,
        out_specs=(VMEM, VMEM),
        scratch_shapes=[pltpu.VMEM(fields[0].shape, jnp.bfloat16), pltpu.SemaphoreType.DMA((6,))],
        compiler_params=pltpu.CompilerParams(vmem_limit_bytes=8 << 20),
        name="pack",
    )(*[held(a) for a in fields])
    got_kv = lax.ppermute(own_kv, "sp", partner)
    got_q = lax.ppermute(own_q, "sp", partner)
    queries = (own_q, got_q)

    lines = head_devices // LINE
    width = expert_gate.shape[2]
    deep = expert_gate.shape[1]
    packed = pl.pallas_call(
        pack_weights,
        out_shape=pltpu.HBM((deep + deep // 2, 2 * width), jnp.bfloat16),
        in_specs=[HBM] * 3,
        out_specs=VMEM,
        scratch_shapes=[pltpu.SemaphoreType.DMA((2 + deep // (2 * width),))],
        compiler_params=pltpu.CompilerParams(vmem_limit_bytes=8 << 20),
        name="w_pack",
    )(*[held(a[0]) for a in (expert_gate, expert_up, expert_down)])
    packed = [packed]
    along = [
        (s * head_devices + t, s * head_devices + (t + (lines if s % 2 == 0 else -lines)) % head_devices)
        for s in range(seq_devices)
        for t in range(head_devices)
    ]
    for _ in range(1, LINE):
        packed.append(lax.ppermute(packed[-1], ("sp", "tp"), along))

    segments = tok_rows // SEG
    later = jnp.where(core == 0, segments, -segments).astype(jnp.int32).reshape(1)
    state = absorbed(later, queries, (own_kv,), None)
    mine, theirs = own_kv, got_kv
    for step in range(1, chips // 2 + 1):
        source = jnp.where(core == 0, chip - step, chip + step) % chips
        seen = (source < chip).astype(jnp.int32).reshape(1)
        mine = lax.ppermute(mine, "sp", onward(step, half_way))
        blocks = (mine,)
        if step < chips // 2:
            theirs = lax.ppermute(theirs, "sp", onward(step, half_way - 1))
            blocks = (mine, theirs)
        state = absorbed(seen, queries, blocks, state)
    got_state = lax.ppermute(state[1], "sp", partner)
    pieces = pl.pallas_call(
        finish,
        out_shape=jax.ShapeDtypeStruct((head_devices, tok_rows, columns), jnp.bfloat16),
        in_specs=[SMEM] + [VMEM] * 4 + [HBM] * 2,
        out_specs=VMEM,
        scratch_shapes=[
            pltpu.VMEM(proj_a.shape, jnp.bfloat16),
            pltpu.VMEM(proj_b.shape, jnp.bfloat16),
            pltpu.SemaphoreType.DMA((2,)),
        ],
        cost_estimate=pl.CostEstimate(
            flops=2 * tok_rows * model_width * 384, bytes_accessed=0, transcendentals=0
        ),
        compiler_params=pltpu.CompilerParams(vmem_limit_bytes=16 << 20),
        name="finish",
    )(
        jnp.concatenate([lambda_a, lambda_b]),
        state[0],
        got_state,
        gain_a[None, :],
        gain_b[None, :],
        held(proj_a),
        held(proj_b),
    )

    col_start = head_index * columns
    summed_cols = summed_on_arrival(pieces, "tp").sum(axis=0)
    residual_cols = lax.dynamic_slice_in_dim(residual, col_start, columns, 1)
    stream_cols = (residual_cols.astype(jnp.float32) + summed_cols).astype(jnp.bfloat16)
    slot_count = 2 * tok_rows * TOP // seq_devices
    assign = routes.reshape(-1)
    onehot = (assign[:, None] == jnp.arange(seq_devices, dtype=jnp.int32)[None, :]).astype(
        jnp.int32
    )
    earlier = jnp.cumsum(onehot, axis=0) - onehot
    slot_index = jnp.sum(earlier * onehot, axis=1)
    target = assign * slot_count + slot_index
    placed = (
        target[:, None] == jnp.arange(seq_devices * slot_count, dtype=jnp.int32)[None, :]
    ).reshape(tok_rows, TOP, -1)
    select = jnp.sum(placed.astype(jnp.bfloat16), axis=1)
    gates = route_weight / jnp.sum(route_weight, axis=1, keepdims=True)
    combine = jnp.sum(placed.astype(jnp.float32) * gates[:, :, None], axis=1)
    send_rows = jnp.einsum(
        "ts,td->sd", select, stream_cols, preferred_element_type=jnp.float32
    ).astype(jnp.bfloat16)
    send_rows = send_rows.reshape(seq_devices, slot_count, columns)
    routed = lax.all_to_all(send_rows, "sp", split_axis=0, concat_axis=0, tiled=True)
    group_rows = seq_devices * slot_count // LINE
    grouped = routed.reshape(LINE, 1, group_rows, columns)
    copies = jnp.broadcast_to(grouped, (LINE, lines, group_rows, columns))
    arrived = lax.all_to_all(
        copies.reshape(head_devices, group_rows, columns),
        "tp",
        split_axis=0,
        concat_axis=0,
        tiled=True,
    )
    parts = pl.pallas_call(
        experts,
        out_shape=jax.ShapeDtypeStruct((head_devices, group_rows, columns), jnp.bfloat16),
        in_specs=[VMEM] * 2 + [HBM] * LINE,
        out_specs=VMEM,
        scratch_shapes=[
            pltpu.VMEM(packed[0].shape, jnp.bfloat16) for _ in range(LINE)
        ]
        + [pltpu.SemaphoreType.DMA((LINE,))],
        cost_estimate=pl.CostEstimate(
            flops=6 * group_rows * model_width * LINE * width, bytes_accessed=0, transcendentals=0
        ),
        compiler_params=pltpu.CompilerParams(vmem_limit_bytes=24 << 20),
        name="experts",
    )(arrived, norm_gain[None, :], *[held(a) for a in packed])
    results = (
        summed_on_arrival(parts, "tp")
        .reshape(LINE, lines, group_rows, columns)
        .sum(axis=1)
        .astype(jnp.bfloat16)
        .reshape(seq_devices, slot_count, columns)
    )
    returned = lax.all_to_all(results, "sp", split_axis=0, concat_axis=0, tiled=True)
    returned_flat = returned.reshape(seq_devices * slot_count, columns).astype(jnp.float32)
    experts_sum = jnp.dot(combine, returned_flat, precision=lax.Precision.HIGHEST)
    return (stream_cols.astype(jnp.float32) + experts_sum).astype(jnp.bfloat16)


def solution(mesh):
    placed = (
        P("sp", None),
        P("sp", "tp", None),
        P("sp", "tp", None),
        P("sp", "tp", None),
        P("sp", "tp", None),
        P("sp", "tp", None),
        P("sp", "tp", None),
        P("tp"),
        P("tp"),
        P(),
        P(),
        P("tp", None),
        P("tp", None),
        P(),
        P("sp", None),
        P("sp", None),
        P("sp", None, "tp"),
        P("sp", None, "tp"),
        P("sp", "tp", None),
    )
    return jax.shard_map(
        local, mesh=mesh, in_specs=placed, out_specs=P("sp", "tp"), check_vma=False
    )
```

profile of v0, /device:TPU:1, one launch (start us, length us, event | category | flops | bytes accessed | tf_op | source)
XLA Modules:
  0.0 197.3 jit_solution(4261035768420894256)
XLA Ops:
  0.0 2.6 %w_pack.1.refs_0_ = bf16[3072,256]{1,0:T(8,128)(2,1)} custom-call(bf16[2048,128]{1,0:T(8,128)(2,1)} %bitcast.58, bf16[2048,128]{1,0:T(8,128)(2,1)} %bitcast.59, bf16[128,2048]{1,0:T(8,128)(2,1)} %bitcast.60), custom_call_target="tpu_custom_call" | custom-call | tf_op jit(solution)/shard_map/w_pack/pallas_call | solution.py:297
  2.6 5.5 %collective-permute-start.18 = (bf16[3072,256]{1,0:T(8,128)(2,1)}, bf16[3072,256]{1,0:T(8,128)(2,1)}, u32[]{:S(2)}, u32[]{:S(2)}) collective-permute-start(bf16[3072,256]{1,0:T(8,128)(2,1)} %w_pack.1.refs_0_), channel_id=1, source_target_pairs={{0,4},{1,5},{2,6},{3,7},{4,8},{5,9},{6,10},{7,11},{8,12},{9,13},{1... | collective-permute-start | bytes 4718600 | tf_op jit(solution)/shard_map/ppermute | solution.py:313
  8.0 1.0 pack.1
  9.1 5.2 %collective-permute-start.9 = (bf16[128,768]{1,0:T(8,128)(2,1)S(1)}, bf16[128,768]{1,0:T(8,128)(2,1)S(1)}, u32[]{:S(2)}, u32[]{:S(2)}) collective-permute-start(bf16[128,768]{1,0:T(8,128)(2,1)S(1)} %get-tuple-element.26.refs_0_), channel_id=1, source_target_pairs={{0,16},{16,0},{32,48},{48,32},{64,80},{80,64},{96,112},{112,96},{1... | collective-permute-start | bytes 589832 | tf_op jit(solution)/shard_map/ppermute | solution.py:290
  14.3 7.8 %collective-permute-start.1 = (bf16[128,768]{1,0:T(8,128)(2,1)S(1)}, bf16[128,768]{1,0:T(8,128)(2,1)S(1)}, u32[]{:S(2)}, u32[]{:S(2)}) collective-permute-start(bf16[128,768]{1,0:T(8,128)(2,1)S(1)} %get-tuple-element.26.refs_0_), channel_id=1, source_target_pairs={{0,32},{32,64},{64,96},{96,128},{128,160},{160,192},{192,224},{224... | collective-permute-start | bytes 589832 | tf_op jit(solution)/shard_map/ppermute | solution.py:322
  22.1 1.9 collective-permute-start.10
  24.1 0.7 collective-permute-done.1.refs_0_
  24.7 5.4 %collective-permute-start.2 = (bf16[128,768]{1,0:T(8,128)(2,1)S(1)}, bf16[128,768]{1,0:T(8,128)(2,1)S(1)}, u32[]{:S(2)}, u32[]{:S(2)}) collective-permute-start(bf16[128,768]{1,0:T(8,128)(2,1)S(1)} %collective-permute-done.1.refs_0_), channel_id=1, source_target_pairs={{32,64},{64,96},{96,128},{128,160},{160,192},{192,224},{224,256},{... | collective-permute-start | bytes 589832 | tf_op jit(solution)/shard_map/ppermute | solution.py:322
  30.2 2.1 %collective-permute-start.11 = (bf16[128,768]{1,0:T(8,128)(2,1)S(1)}, bf16[128,768]{1,0:T(8,128)(2,1)S(1)}, u32[]{:S(2)}, u32[]{:S(2)}) collective-permute-start(bf16[128,768]{1,0:T(8,128)(2,1)S(1)} %collective-permute-done.10.refs_1_), channel_id=1, source_target_pairs={{32,64},{64,96},{96,128},{128,160},{160,192},{192,224},{224,256},{... | collective-permute-start | bytes 589832 | tf_op jit(solution)/shard_map/ppermute | solution.py:325
  32.3 0.5 collective-permute-done.2.refs_0_
  32.7 5.4 %collective-permute-start.3 = (bf16[128,768]{1,0:T(8,128)(2,1)S(1)}, bf16[128,768]{1,0:T(8,128)(2,1)S(1)}, u32[]{:S(2)}, u32[]{:S(2)}) collective-permute-start(bf16[128,768]{1,0:T(8,128)(2,1)S(1)} %collective-permute-done.2.refs_0_), channel_id=1, source_target_pairs={{64,96},{96,128},{128,160},{160,192},{192,224},{224,256},{256,288}... | collective-permute-start | bytes 589832 | tf_op jit(solution)/shard_map/ppermute | solution.py:322
  38.2 1.9 collective-permute-start.12
  40.1 0.7 collective-permute-done.3.refs_0_
  40.8 5.0 %collective-permute-start.4 = (bf16[128,768]{1,0:T(8,128)(2,1)S(1)}, bf16[128,768]{1,0:T(8,128)(2,1)S(1)}, u32[]{:S(2)}, u32[]{:S(2)}) collective-permute-start(bf16[128,768]{1,0:T(8,128)(2,1)S(1)} %collective-permute-done.3.refs_0_), channel_id=1, source_target_pairs={{96,128},{128,160},{160,192},{192,224},{224,256},{256,288},{288,32... | collective-permute-start | bytes 589832 | tf_op jit(solution)/shard_map/ppermute | solution.py:322
  45.8 2.1 %collective-permute-start.13 = (bf16[128,768]{1,0:T(8,128)(2,1)S(1)}, bf16[128,768]{1,0:T(8,128)(2,1)S(1)}, u32[]{:S(2)}, u32[]{:S(2)}) collective-permute-start(bf16[128,768]{1,0:T(8,128)(2,1)S(1)} %collective-permute-done.12.refs_1_), channel_id=1, source_target_pairs={{96,128},{128,160},{160,192},{192,224},{224,256},{256,288},{288,32... | collective-permute-start | bytes 589832 | tf_op jit(solution)/shard_map/ppermute | solution.py:325
  47.9 0.5 collective-permute-done.4.refs_0_
  48.4 5.0 %collective-permute-start.5 = (bf16[128,768]{1,0:T(8,128)(2,1)S(1)}, bf16[128,768]{1,0:T(8,128)(2,1)S(1)}, u32[]{:S(2)}, u32[]{:S(2)}) collective-permute-start(bf16[128,768]{1,0:T(8,128)(2,1)S(1)} %collective-permute-done.4.refs_0_), channel_id=1, source_target_pairs={{128,160},{160,192},{192,224},{224,256},{256,288},{288,320},{320,3... | collective-permute-start | bytes 589832 | tf_op jit(solution)/shard_map/ppermute | solution.py:322
  53.4 2.1 %collective-permute-start.14 = (bf16[128,768]{1,0:T(8,128)(2,1)S(1)}, bf16[128,768]{1,0:T(8,128)(2,1)S(1)}, u32[]{:S(2)}, u32[]{:S(2)}) collective-permute-start(bf16[128,768]{1,0:T(8,128)(2,1)S(1)} %collective-permute-done.13.refs_1_), channel_id=1, source_target_pairs={{128,160},{160,192},{192,224},{224,256},{256,288},{288,320},{320,3... | collective-permute-start | bytes 589832 | tf_op jit(solution)/shard_map/ppermute | solution.py:325
  55.5 0.5 collective-permute-done.5.refs_0_
  56.0 5.0 %collective-permute-start.6 = (bf16[128,768]{1,0:T(8,128)(2,1)S(1)}, bf16[128,768]{1,0:T(8,128)(2,1)S(1)}, u32[]{:S(2)}, u32[]{:S(2)}) collective-permute-start(bf16[128,768]{1,0:T(8,128)(2,1)S(1)} %collective-permute-done.5.refs_0_), channel_id=1, source_target_pairs={{160,192},{192,224},{224,256},{256,288},{288,320},{320,352},{352,3... | collective-permute-start | bytes 589832 | tf_op jit(solution)/shard_map/ppermute | solution.py:322
  61.0 2.0 %collective-permute-start.19 = (bf16[3072,256]{1,0:T(8,128)(2,1)}, bf16[3072,256]{1,0:T(8,128)(2,1)}, u32[]{:S(2)}, u32[]{:S(2)}) collective-permute-start(bf16[3072,256]{1,0:T(8,128)(2,1)} %collective-permute-done.18.refs_1_), channel_id=1, source_target_pairs={{0,4},{1,5},{2,6},{3,7},{4,8},{5,9},{6,10},{7,11},{8,12},{9,13},{1... | collective-permute-start | bytes 4718600 | tf_op jit(solution)/shard_map/ppermute | solution.py:313
  63.0 1.9 collective-permute-start.15
  65.0 4.0 %collective-permute-start.7 = (bf16[128,768]{1,0:T(8,128)(2,1)S(1)}, bf16[128,768]{1,0:T(8,128)(2,1)S(1)}, u32[]{:S(2)}, u32[]{:S(2)}) collective-permute-start(bf16[128,768]{1,0:T(8,128)(2,1)S(1)} %collective-permute-done.6.refs_0_), channel_id=1, source_target_pairs={{192,224},{224,256},{256,288},{288,320},{320,352},{352,384},{384,4... | collective-permute-start | bytes 589832 | tf_op jit(solution)/shard_map/ppermute | solution.py:322
  69.0 1.9 collective-permute-start
  71.0 2.0 %collective-permute-start.16 = (bf16[128,768]{1,0:T(8,128)(2,1)S(1)}, bf16[128,768]{1,0:T(8,128)(2,1)S(1)}, u32[]{:S(2)}, u32[]{:S(2)}) collective-permute-start(bf16[128,768]{1,0:T(8,128)(2,1)S(1)} %collective-permute-done.15.refs_1_), channel_id=1, source_target_pairs={{192,224},{224,256},{256,288},{288,320},{320,352},{352,384},{384,4... | collective-permute-start | bytes 589832 | tf_op jit(solution)/shard_map/ppermute | solution.py:325
  73.0 4.3 %collective-permute-start.8 = (bf16[128,768]{1,0:T(8,128)(2,1)S(1)}, bf16[128,768]{1,0:T(8,128)(2,1)S(1)}, u32[]{:S(2)}, u32[]{:S(2)}) collective-permute-start(bf16[128,768]{1,0:T(8,128)(2,1)S(1)} %collective-permute-done.7.refs_0_), channel_id=1, source_target_pairs={{224,256},{256,288},{288,320},{320,352},{352,384},{384,416},{416,4... | collective-permute-start | bytes 589832 | tf_op jit(solution)/shard_map/ppermute | solution.py:322
  77.5 0.7 absorb.9
  78.2 0.1 absorb.10
  78.3 0.1 absorb.11
  78.4 0.1 absorb.12
  78.4 0.1 absorb.13
  78.5 0.1 absorb.14
  78.6 0.1 absorb.15
  78.7 0.1 absorb.16
  78.8 1.1 collective-permute-done.8.refs_0_
  79.9 1.9 collective-permute-start.17
  83.2 0.1 copy.34
  83.3 0.1 eq.65
  83.4 0.6 reduce-window.6
  84.0 0.1 pad_maximum_fusion.mix_ref
  84.1 3.2 %finish.1 = bf16[16,128,128]{2,1,0:T(8,128)(2,1)} custom-call(f32[2]{0:T(128)S(1)} %pad_maximum_fusion.mix_ref, f32[776,128]{1,0:T(8,128)S(1)} %get-tuple-element.43.own_ref, f32[776,128]{1,0:T(8,128)S(1)} %collective-permute-done.17.got_ref, f32[1,128]{1,0:T(1,128)S(1)} %bitcast.53, f32[1,256]{1,0:T(1,128)S(1)} %bitcast.52, bf16[128,2048]{1,0:T(8,128)(2,1)} %from_a_ref.1, ...), custom_call_target="tpu_custom_call" | custom-call | flops 201326592 | tf_op jit(solution)/shard_map/finish/pallas_call | solution.py:329
  87.4 5.5 %all-to-all-start = ((bf16[16,128,128]{2,1,0:T(8,128)(2,1)}), bf16[16,128,128]{2,1,0:T(8,128)(2,1)S(1)}, u32[]{:S(2)}, u32[]{:S(2)}) async-start(bf16[16,128,128]{2,1,0:T(8,128)(2,1)} %finish.1), calls=%async_computation | async-start | bytes 1048576 | tf_op jit(solution)/shard_map/all_to_all | solution.py:234
  92.9 0.2 slice_reduce_fusion
  93.0 0.1 eq.61
  93.2 0.1 fusion.5
  93.3 0.1 reduce_sum.61
  93.5 0.1 copy.37
  93.6 0.1 fusion.2
  93.7 4.5 %collective-permute-start.20 = (bf16[3072,256]{1,0:T(8,128)(2,1)}, bf16[3072,256]{1,0:T(8,128)(2,1)S(1)}, u32[]{:S(2)}, u32[]{:S(2)}) collective-permute-start(bf16[3072,256]{1,0:T(8,128)(2,1)} %collective-permute-done.19.refs_2_), channel_id=1, source_target_pairs={{0,4},{1,5},{2,6},{3,7},{4,8},{5,9},{6,10},{7,11},{8,12},{9,13},{1... | collective-permute-start | bytes 4718600 | tf_op jit(solution)/shard_map/ppermute | solution.py:313
  98.2 5.3 %all-to-all-done = bf16[16,128,128]{2,1,0:T(8,128)(2,1)S(1)} async-done(((bf16[16,128,128]{2,1,0:T(8,128)(2,1)}), bf16[16,128,128]{2,1,0:T(8,128)(2,1)S(1)}, u32[]{:S(2)}, u32[]{:S(2)}) %all-to-all-start) | async-done | bytes 524320 | tf_op jit(solution)/shard_map/all_to_all | solution.py:234
  103.5 0.1 convert_reduce_fusion
  103.6 0.8 add_convert_fusion
  104.3 0.2 convolution_convert_fusion
  104.5 37.4 %all_to_all.25 = bf16[32,16,128]{2,1,0:T(8,128)(2,1)S(1)} all-to-all(bf16[32,16,128]{2,1,0:T(8,128)(2,1)S(1)} %bitcast.57), channel_id=1, replica_groups=mesh['sp'=32,'tp'=16] {'sp'}, dimensions={0} | all-to-all | bytes 262144 | tf_op jit(solution)/shard_map/all_to_all | solution.py:376
  141.9 0.1 broadcast_in_dim.24
  142.0 12.6 %all_to_all.26.rows_ref = bf16[16,128,128]{2,1,0:T(8,128)(2,1)S(1)} all-to-all(bf16[16,128,128]{2,1,0:T(8,128)(2,1)S(1)} %bitcast.54), channel_id=1, replica_groups=mesh['sp'=32,'tp'=16] {'tp'}, dimensions={0} | all-to-all | bytes 1048576 | tf_op jit(solution)/shard_map/all_to_all | solution.py:380
  154.7 1.2 copy-done.3
  155.9 3.8 %experts.1 = bf16[16,128,128]{2,1,0:T(8,128)(2,1)S(1)} custom-call(bf16[16,128,128]{2,1,0:T(8,128)(2,1)S(1)} %all_to_all.26.rows_ref, f32[1,2048]{1,0:T(1,128)S(1)} %bitcast.51, bf16[3072,256]{1,0:T(8,128)(2,1)} %w_pack.1.refs_0_, bf16[3072,256]{1,0:T(8,128)(2,1)} %collective-permute-done.18.refs_1_, bf16[3072,256]{1,0:T(8,128)(2,1)} %collective-permute-done.19.refs_2_, ...), custom_call_target="tpu_custom_call" | custom-call | flops 805306368 | tf_op jit(solution)/shard_map/experts/pallas_call | solution.py:387
  159.7 12.0 %all_to_all.27 = bf16[16,128,128]{2,1,0:T(8,128)(2,1)S(1)} all-to-all(bf16[16,128,128]{2,1,0:T(8,128)(2,1)S(1)} %experts.1), channel_id=1, replica_groups=mesh['sp'=32,'tp'=16] {'tp'}, dimensions={0} | all-to-all | bytes 1048576 | tf_op jit(solution)/shard_map/all_to_all | solution.py:234
  171.8 0.7 bitcast_reduce_fusion
  172.5 8.1 %all-to-all-start.4 = ((bf16[32,16,128]{2,1,0:T(8,128)(2,1)}), bf16[32,16,128]{2,1,0:T(8,128)(2,1)S(1)}, u32[]{:S(2)}, u32[]{:S(2)}) async-start(bf16[32,16,128]{2,1,0:T(8,128)(2,1)} %bitcast.26), calls=%async_computation.4 | async-start | bytes 262144 | tf_op jit(solution)/shard_map/all_to_all | solution.py:409
  180.6 0.1 select_reduce_fusion
  180.8 15.7 %all-to-all-done.4 = bf16[32,16,128]{2,1,0:T(8,128)(2,1)S(1)} async-done(((bf16[32,16,128]{2,1,0:T(8,128)(2,1)}), bf16[32,16,128]{2,1,0:T(8,128)(2,1)S(1)}, u32[]{:S(2)}, u32[]{:S(2)}) %all-to-all-start.4) | async-done | bytes 131104 | tf_op jit(solution)/shard_map/all_to_all | solution.py:409
  196.4 0.9 fusion
  (33 shorter events, 0.2 us)
Async XLA Ops:
  2.6 58.4 %collective-permute-start.18 = (bf16[3072,256]{1,0:T(8,128)(2,1)}, bf16[3072,256]{1,0:T(8,128)(2,1)}, u32[]{:S(2)}, u32[]{:S(2)}) collective-permute-start(bf16[3072,256]{1,0:T(8,128)(2,1)} %w_pack.1.refs_0_), channel_id=1, source_target_pairs={{0,4},{1,5},{2,6},{3,7},{4,8},{5,9},{6,10},{7,11},{8,12},{9,13},{1... | collective-permute-start | bytes 4718600 | tf_op jit(solution)/shard_map/ppermute | solution.py:313
  9.1 13.1 %collective-permute-start.9 = (bf16[128,768]{1,0:T(8,128)(2,1)S(1)}, bf16[128,768]{1,0:T(8,128)(2,1)S(1)}, u32[]{:S(2)}, u32[]{:S(2)}) collective-permute-start(bf16[128,768]{1,0:T(8,128)(2,1)S(1)} %get-tuple-element.26.refs_0_), channel_id=1, source_target_pairs={{0,16},{16,0},{32,48},{48,32},{64,80},{80,64},{96,112},{112,96},{1... | collective-permute-start | bytes 589832 | tf_op jit(solution)/shard_map/ppermute | solution.py:290
  14.3 10.4 %collective-permute-start.1 = (bf16[128,768]{1,0:T(8,128)(2,1)S(1)}, bf16[128,768]{1,0:T(8,128)(2,1)S(1)}, u32[]{:S(2)}, u32[]{:S(2)}) collective-permute-start(bf16[128,768]{1,0:T(8,128)(2,1)S(1)} %get-tuple-element.26.refs_0_), channel_id=1, source_target_pairs={{0,32},{32,64},{64,96},{96,128},{128,160},{160,192},{192,224},{224... | collective-permute-start | bytes 589832 | tf_op jit(solution)/shard_map/ppermute | solution.py:322
  22.1 8.0 %collective-permute-start.10 = (bf16[128,768]{1,0:T(8,128)(2,1)S(1)}, bf16[128,768]{1,0:T(8,128)(2,1)S(1)}, u32[]{:S(2)}, u32[]{:S(2)}) collective-permute-start(bf16[128,768]{1,0:T(8,128)(2,1)S(1)} %collective-permute-done.9), channel_id=1, source_target_pairs={{0,32},{32,64},{64,96},{96,128},{128,160},{160,192},{192,224},{224... | collective-permute-start | bytes 589832 | tf_op jit(solution)/shard_map/ppermute | solution.py:325
  24.7 8.0 %collective-permute-start.2 = (bf16[128,768]{1,0:T(8,128)(2,1)S(1)}, bf16[128,768]{1,0:T(8,128)(2,1)S(1)}, u32[]{:S(2)}, u32[]{:S(2)}) collective-permute-start(bf16[128,768]{1,0:T(8,128)(2,1)S(1)} %collective-permute-done.1.refs_0_), channel_id=1, source_target_pairs={{32,64},{64,96},{96,128},{128,160},{160,192},{192,224},{224,256},{... | collective-permute-start | bytes 589832 | tf_op jit(solution)/shard_map/ppermute | solution.py:322
  30.2 8.0 %collective-permute-start.11 = (bf16[128,768]{1,0:T(8,128)(2,1)S(1)}, bf16[128,768]{1,0:T(8,128)(2,1)S(1)}, u32[]{:S(2)}, u32[]{:S(2)}) collective-permute-start(bf16[128,768]{1,0:T(8,128)(2,1)S(1)} %collective-permute-done.10.refs_1_), channel_id=1, source_target_pairs={{32,64},{64,96},{96,128},{128,160},{160,192},{192,224},{224,256},{... | collective-permute-start | bytes 589832 | tf_op jit(solution)/shard_map/ppermute | solution.py:325
  32.7 8.0 %collective-permute-start.3 = (bf16[128,768]{1,0:T(8,128)(2,1)S(1)}, bf16[128,768]{1,0:T(8,128)(2,1)S(1)}, u32[]{:S(2)}, u32[]{:S(2)}) collective-permute-start(bf16[128,768]{1,0:T(8,128)(2,1)S(1)} %collective-permute-done.2.refs_0_), channel_id=1, source_target_pairs={{64,96},{96,128},{128,160},{160,192},{192,224},{224,256},{256,288}... | collective-permute-start | bytes 589832 | tf_op jit(solution)/shard_map/ppermute | solution.py:322
  38.2 7.6 %collective-permute-start.12 = (bf16[128,768]{1,0:T(8,128)(2,1)S(1)}, bf16[128,768]{1,0:T(8,128)(2,1)S(1)}, u32[]{:S(2)}, u32[]{:S(2)}) collective-permute-start(bf16[128,768]{1,0:T(8,128)(2,1)S(1)} %collective-permute-done.11.refs_1_), channel_id=1, source_target_pairs={{64,96},{96,128},{128,160},{160,192},{192,224},{224,256},{256,288}... | collective-permute-start | bytes 589832 | tf_op jit(solution)/shard_map/ppermute | solution.py:325
  40.8 7.6 %collective-permute-start.4 = (bf16[128,768]{1,0:T(8,128)(2,1)S(1)}, bf16[128,768]{1,0:T(8,128)(2,1)S(1)}, u32[]{:S(2)}, u32[]{:S(2)}) collective-permute-start(bf16[128,768]{1,0:T(8,128)(2,1)S(1)} %collective-permute-done.3.refs_0_), channel_id=1, source_target_pairs={{96,128},{128,160},{160,192},{192,224},{224,256},{256,288},{288,32... | collective-permute-start | bytes 589832 | tf_op jit(solution)/shard_map/ppermute | solution.py:322
  45.8 7.6 %collective-permute-start.13 = (bf16[128,768]{1,0:T(8,128)(2,1)S(1)}, bf16[128,768]{1,0:T(8,128)(2,1)S(1)}, u32[]{:S(2)}, u32[]{:S(2)}) collective-permute-start(bf16[128,768]{1,0:T(8,128)(2,1)S(1)} %collective-permute-done.12.refs_1_), channel_id=1, source_target_pairs={{96,128},{128,160},{160,192},{192,224},{224,256},{256,288},{288,32... | collective-permute-start | bytes 589832 | tf_op jit(solution)/shard_map/ppermute | solution.py:325
  48.4 7.6 %collective-permute-start.5 = (bf16[128,768]{1,0:T(8,128)(2,1)S(1)}, bf16[128,768]{1,0:T(8,128)(2,1)S(1)}, u32[]{:S(2)}, u32[]{:S(2)}) collective-permute-start(bf16[128,768]{1,0:T(8,128)(2,1)S(1)} %collective-permute-done.4.refs_0_), channel_id=1, source_target_pairs={{128,160},{160,192},{192,224},{224,256},{256,288},{288,320},{320,3... | collective-permute-start | bytes 589832 | tf_op jit(solution)/shard_map/ppermute | solution.py:322
  53.4 9.6 %collective-permute-start.14 = (bf16[128,768]{1,0:T(8,128)(2,1)S(1)}, bf16[128,768]{1,0:T(8,128)(2,1)S(1)}, u32[]{:S(2)}, u32[]{:S(2)}) collective-permute-start(bf16[128,768]{1,0:T(8,128)(2,1)S(1)} %collective-permute-done.13.refs_1_), channel_id=1, source_target_pairs={{128,160},{160,192},{192,224},{224,256},{256,288},{288,320},{320,3... | collective-permute-start | bytes 589832 | tf_op jit(solution)/shard_map/ppermute | solution.py:325
  56.0 9.0 %collective-permute-start.6 = (bf16[128,768]{1,0:T(8,128)(2,1)S(1)}, bf16[128,768]{1,0:T(8,128)(2,1)S(1)}, u32[]{:S(2)}, u32[]{:S(2)}) collective-permute-start(bf16[128,768]{1,0:T(8,128)(2,1)S(1)} %collective-permute-done.5.refs_0_), channel_id=1, source_target_pairs={{160,192},{192,224},{224,256},{256,288},{288,320},{320,352},{352,3... | collective-permute-start | bytes 589832 | tf_op jit(solution)/shard_map/ppermute | solution.py:322
  61.0 32.7 %collective-permute-start.19 = (bf16[3072,256]{1,0:T(8,128)(2,1)}, bf16[3072,256]{1,0:T(8,128)(2,1)}, u32[]{:S(2)}, u32[]{:S(2)}) collective-permute-start(bf16[3072,256]{1,0:T(8,128)(2,1)} %collective-permute-done.18.refs_1_), channel_id=1, source_target_pairs={{0,4},{1,5},{2,6},{3,7},{4,8},{5,9},{6,10},{7,11},{8,12},{9,13},{1... | collective-permute-start | bytes 4718600 | tf_op jit(solution)/shard_map/ppermute | solution.py:313
  63.0 7.9 %collective-permute-start.15 = (bf16[128,768]{1,0:T(8,128)(2,1)S(1)}, bf16[128,768]{1,0:T(8,128)(2,1)S(1)}, u32[]{:S(2)}, u32[]{:S(2)}) collective-permute-start(bf16[128,768]{1,0:T(8,128)(2,1)S(1)} %collective-permute-done.14.refs_1_), channel_id=1, source_target_pairs={{160,192},{192,224},{224,256},{256,288},{288,320},{320,352},{352,3... | collective-permute-start | bytes 589832 | tf_op jit(solution)/shard_map/ppermute | solution.py:325
  65.0 8.0 %collective-permute-start.7 = (bf16[128,768]{1,0:T(8,128)(2,1)S(1)}, bf16[128,768]{1,0:T(8,128)(2,1)S(1)}, u32[]{:S(2)}, u32[]{:S(2)}) collective-permute-start(bf16[128,768]{1,0:T(8,128)(2,1)S(1)} %collective-permute-done.6.refs_0_), channel_id=1, source_target_pairs={{192,224},{224,256},{256,288},{288,320},{320,352},{352,384},{384,4... | collective-permute-start | bytes 589832 | tf_op jit(solution)/shard_map/ppermute | solution.py:322
  69.0 8.5 %collective-permute-start = (bf16[128,512]{1,0:T(8,128)(2,1)S(1)}, bf16[128,512]{1,0:T(8,128)(2,1)S(1)}, u32[]{:S(2)}, u32[]{:S(2)}) collective-permute-start(bf16[128,512]{1,0:T(8,128)(2,1)S(1)} %get-tuple-element.25.own_q_ref), channel_id=1, source_target_pairs={{0,16},{16,0},{32,48},{48,32},{64,80},{80,64},{96,112},{112,96},{1... | collective-permute-start | bytes 393224 | tf_op jit(solution)/shard_map/ppermute | solution.py:291
  71.0 7.7 %collective-permute-start.16 = (bf16[128,768]{1,0:T(8,128)(2,1)S(1)}, bf16[128,768]{1,0:T(8,128)(2,1)S(1)}, u32[]{:S(2)}, u32[]{:S(2)}) collective-permute-start(bf16[128,768]{1,0:T(8,128)(2,1)S(1)} %collective-permute-done.15.refs_1_), channel_id=1, source_target_pairs={{192,224},{224,256},{256,288},{288,320},{320,352},{352,384},{384,4... | collective-permute-start | bytes 589832 | tf_op jit(solution)/shard_map/ppermute | solution.py:325
  73.0 6.9 %collective-permute-start.8 = (bf16[128,768]{1,0:T(8,128)(2,1)S(1)}, bf16[128,768]{1,0:T(8,128)(2,1)S(1)}, u32[]{:S(2)}, u32[]{:S(2)}) collective-permute-start(bf16[128,768]{1,0:T(8,128)(2,1)S(1)} %collective-permute-done.7.refs_0_), channel_id=1, source_target_pairs={{224,256},{256,288},{288,320},{320,352},{352,384},{384,416},{416,4... | collective-permute-start | bytes 589832 | tf_op jit(solution)/shard_map/ppermute | solution.py:322
  78.7 4.5 %copy-start.4 = (s32[128,2]{0,1:T(2,128)S(1)}, s32[128,2]{0,1:T(2,128)}, u32[]{:S(2)}) copy-start(s32[128,2]{0,1:T(2,128)} %param.33) | copy-start | bytes 3076
  78.7 5.4 %copy-start.1 = (f32[256]{0:T(256)S(1)}, f32[256]{0:T(256)}, u32[]{:S(2)}) copy-start(f32[256]{0:T(256)} %param.29) | copy-start | bytes 3076
  78.7 5.4 %copy-start.2 = (f32[128]{0:T(128)S(1)}, f32[128]{0:T(128)}, u32[]{:S(2)}) copy-start(f32[128]{0:T(128)} %param.28) | copy-start | bytes 1540
  79.9 4.2 %collective-permute-start.17 = (f32[776,128]{1,0:T(8,128)S(1)}, f32[776,128]{1,0:T(8,128)S(1)}, u32[]{:S(2)}, u32[]{:S(2)}) collective-permute-start(f32[776,128]{1,0:T(8,128)S(1)} %get-tuple-element.44), channel_id=1, source_target_pairs={{0,16},{16,0},{32,48},{48,32},{64,80},{80,64},{96,112},{112,96},{1... | collective-permute-start | bytes 1191944 | tf_op jit(solution)/shard_map/ppermute | solution.py:328
  87.4 16.1 %all-to-all-start = ((bf16[16,128,128]{2,1,0:T(8,128)(2,1)}), bf16[16,128,128]{2,1,0:T(8,128)(2,1)S(1)}, u32[]{:S(2)}, u32[]{:S(2)}) async-start(bf16[16,128,128]{2,1,0:T(8,128)(2,1)} %finish.1), calls=%async_computation | async-start | bytes 1048576 | tf_op jit(solution)/shard_map/all_to_all | solution.py:234
  93.5 62.3 %copy-start = (f32[2048]{0:T(1024)S(1)}, f32[2048]{0:T(1024)}, u32[]{:S(2)}) copy-start(f32[2048]{0:T(1024)} %param.32) | copy-start | bytes 24580
  93.7 61.0 %collective-permute-start.20 = (bf16[3072,256]{1,0:T(8,128)(2,1)}, bf16[3072,256]{1,0:T(8,128)(2,1)S(1)}, u32[]{:S(2)}, u32[]{:S(2)}) collective-permute-start(bf16[3072,256]{1,0:T(8,128)(2,1)} %collective-permute-done.19.refs_2_), channel_id=1, source_target_pairs={{0,4},{1,5},{2,6},{3,7},{4,8},{5,9},{6,10},{7,11},{8,12},{9,13},{1... | collective-permute-start | bytes 4718600 | tf_op jit(solution)/shard_map/ppermute | solution.py:313
  154.7 1.2 copy-start.3
  159.7 20.9 %copy-start.5 = (f32[128,2]{0,1:T(2,128)S(1)}, f32[128,2]{0,1:T(2,128)}, u32[]{:S(2)}) copy-start(f32[128,2]{0,1:T(2,128)} %param.34) | copy-start | bytes 3076
  172.5 24.0 %all-to-all-start.4 = ((bf16[32,16,128]{2,1,0:T(8,128)(2,1)}), bf16[32,16,128]{2,1,0:T(8,128)(2,1)S(1)}, u32[]{:S(2)}, u32[]{:S(2)}) async-start(bf16[32,16,128]{2,1,0:T(8,128)(2,1)} %bitcast.26), calls=%async_computation.4 | async-start | bytes 262144 | tf_op jit(solution)/shard_map/all_to_all | solution.py:409
where the time goes:
time: 198 us; the launch traced here: 197 us
  starting transfers between devices  90.7 us (46%)
  blocking collectives  62.1 us (31%)
  waiting for transfers between devices  24.8 us (13%)
  Pallas kernels  11.9 us (6%)
  other arithmetic  2.69 us (1%)
  local copies, waits for them, and re-layouts  2.08 us (1%)
  between operations  1.99 us (1%)
    ppermute x8, starting transfers between devices, local(): mine = lax.ppermute(mine, 'sp', onward(step, half_way))  42 us
    all_to_all x1, blocking collectives, local(): lax.all_to_all(send_rows, 'sp', split_axis=0, concat_axis=0, tiled=True)  37.4 us
    all_to_all x1, waiting for transfers between devices, local(): lax.all_to_all(results, 'sp', split_axis=0, concat_axis=0, tiled=True)  15.7 us
    ppermute x7, starting transfers between devices, local(): theirs = lax.ppermute(theirs, 'sp', onward(step, half_way - 1))  14 us
    all_to_all x1, blocking collectives, local(): lax.all_to_all(copies.reshape(head_devices, group_rows, columns), 'tp', s...  12.6 us
    all_to_all x1, blocking collectives, summed_on_arrival(): lax.all_to_all(pieces, axis, split_axis=0, concat_axis=0, tiled=True)  12 us
    ppermute x3, starting transfers between devices, local(): packed.append(lax.ppermute(packed[-1], ('sp', 'tp'), along))  11.9 us
    all_to_all x1, starting transfers between devices, local(): lax.all_to_all(results, 'sp', split_axis=0, concat_axis=0, tiled=True)  8.11 us
  transfers between devices with their start and end apart: 23, of which 8 were waited for; matrix products, arithmetic and copies ran while one was open for 2% of the time, Pallas kernels for 3%

commit v1 on v0

--- a/solution.py
+++ b/solution.py
@@ -119,13 +119,14 @@
 
 def pack(qa_ref, qb_ref, ka_ref, va_ref, kb_ref, vb_ref, q_ref, kv_ref, qa_buf, sems):
     width = qa_buf.shape[1]
+    q_cols = q_ref.shape[1] - kv_ref.shape[1]
     places = (
         (qa_ref, qa_buf),
         (ka_ref, kv_ref.at[:, :width]),
         (va_ref, kv_ref.at[:, width : 2 * width]),
         (kb_ref, kv_ref.at[:, 2 * width : 4 * width]),
         (vb_ref, kv_ref.at[:, 4 * width :]),
-        (qb_ref, q_ref.at[:, 2 * width :]),
+        (qb_ref, q_ref.at[:, 2 * width : q_cols]),
     )
     copies = [pltpu.make_async_copy(a, b, sems.at[i]) for i, (a, b) in enumerate(places)]
     for copy in copies:
@@ -136,23 +137,46 @@
     first = lax.broadcasted_iota(jnp.int32, both.shape, 1) < DK_A
     q_ref[:, :width] = jnp.where(first, both, 0)
     q_ref[:, width : 2 * width] = jnp.where(first, 0, both)
-
-
-def pack_weights(gate_ref, up_ref, down_ref, out_ref, sems):
+    q_ref[:, q_cols:] = kv_ref[...]
+
+
+def pack_weights(gate_ref, up_ref, down_ref, out_ref, buf, sems):
     deep, width = gate_ref.shape
-    places = [(gate_ref, out_ref.at[:deep, :width]), (up_ref, out_ref.at[:deep, width:])]
+    chunk = deep // 2
+    pieces = []
+    for start in range(0, deep, chunk):
+        rows = slice(start, start + chunk)
+        ins = [(ref.at[rows, :], buf.at[rows, cols]) for ref, cols in (
+            (gate_ref, slice(0, width)),
+            (up_ref, slice(width, 2 * width)),
+        )]
+        pieces.append((rows, ins))
+    ins = []
     for j in range(deep // (2 * width)):
         start = deep + j * width
-        places.append(
+        ins.append(
             (
                 down_ref.at[:, 2 * j * width : 2 * (j + 1) * width],
-                out_ref.at[start : start + width, :],
+                buf.at[start : start + width, :],
             )
         )
-    copies = [pltpu.make_async_copy(a, b, sems.at[i]) for i, (a, b) in enumerate(places)]
-    for copy in copies:
-        copy.start()
-    for copy in copies:
+    pieces.append((slice(deep, deep + deep // 2), ins))
+    count, started = 0, []
+    for rows, ins in pieces:
+        copies = []
+        for a, b in ins:
+            copies.append(pltpu.make_async_copy(a, b, sems.at[count]))
+            copies[-1].start()
+            count += 1
+        started.append((rows, copies))
+    outs = []
+    for rows, copies in started:
+        for copy in copies:
+            copy.wait()
+        outs.append(pltpu.make_async_copy(buf.at[rows, :], out_ref.at[rows, :], sems.at[count]))
+        outs[-1].start()
+        count += 1
+    for copy in outs:
         copy.wait()
 
 
@@ -198,7 +222,7 @@
 
 
 def experts(rows_ref, gain_ref, *refs):
-    froms, out_ref, bufs, sems = refs[:LINE], refs[LINE], refs[LINE + 1 : -1], refs[-1]
+    here, froms, out_ref, bufs, sems = refs[0], refs[1:LINE], refs[LINE], refs[LINE + 1 : -1], refs[-1]
     copies = [pltpu.make_async_copy(a, b, sems.at[i]) for i, (a, b) in enumerate(zip(froms, bufs))]
     for copy in copies:
         copy.start()
@@ -212,8 +236,10 @@
         return jnp.dot(a, b, preferred_element_type=jnp.float32)
 
     hidden = []
-    for copy, ref in zip(copies, bufs):
-        copy.wait()
+    bufs = (here, *bufs)
+    for index, ref in enumerate(bufs):
+        if index > 0:
+            copies[index - 1].wait()
         both = dot(normed, ref[:model_width, :])
         gate, up = both[:, :width], both[:, width:]
         hidden.append((gate / (1.0 + jnp.exp(-gate)) * up).astype(jnp.bfloat16))
@@ -269,16 +295,16 @@
     partner = [(i, i ^ 1) for i in range(seq_devices)]
     half_way = chips // 2
 
-    def onward(step, down_blocks):
-        up = [(2 * i, 2 * (i + 1)) for i in range(step - 1, chips - 1)]
-        places = [(block - step) % chips for block in range(down_blocks)]
-        return up + [(2 * ((i + 1) % chips) + 1, 2 * i + 1) for i in places]
+    def onward(step):
+        up = [(2 * i + 1, 2 * (i + 1) + 1) for i in range(step - 1, chips - 1)]
+        places = [(block - step) % chips for block in range(half_way - 1)] if step < half_way else []
+        return up + [(2 * ((i + 1) % chips), 2 * i) for i in places]
 
     fields = [a[:, 0] for a in (query_a, query_b, keys_a, values_a, keys_b, values_b)]
-    own_q, own_kv = pl.pallas_call(
+    own_all, own_kv = pl.pallas_call(
         pack,
         out_shape=(
-            jax.ShapeDtypeStruct((tok_rows, 4 * DK_B), jnp.bfloat16),
+            jax.ShapeDtypeStruct((tok_rows, 4 * DK_B + SUMS), jnp.bfloat16),
             jax.ShapeDtypeStruct((tok_rows, SUMS), jnp.bfloat16),
         ),
         in_specs=[HBM] * 6,
@@ -287,9 +313,9 @@
         compiler_params=pltpu.CompilerParams(vmem_limit_bytes=8 << 20),
         name="pack",
     )(*[held(a) for a in fields])
-    got_kv = lax.ppermute(own_kv, "sp", partner)
-    got_q = lax.ppermute(own_q, "sp", partner)
-    queries = (own_q, got_q)
+    got_all = lax.ppermute(own_all, "sp", partner)
+    got_kv = got_all[:, 4 * DK_B :]
+    queries = (own_all, got_all)
 
     lines = head_devices // LINE
     width = expert_gate.shape[2]
@@ -298,8 +324,11 @@
         pack_weights,
         out_shape=pltpu.HBM((deep + deep // 2, 2 * width), jnp.bfloat16),
         in_specs=[HBM] * 3,
-        out_specs=VMEM,
-        scratch_shapes=[pltpu.SemaphoreType.DMA((2 + deep // (2 * width),))],
+        out_specs=HBM,
+        scratch_shapes=[
+            pltpu.VMEM((deep + deep // 2, 2 * width), jnp.bfloat16),
+            pltpu.SemaphoreType.DMA((4 + deep // (2 * width) + 3,)),
+        ],
         compiler_params=pltpu.CompilerParams(vmem_limit_bytes=8 << 20),
         name="w_pack",
     )(*[held(a[0]) for a in (expert_gate, expert_up, expert_down)])
@@ -316,19 +345,16 @@
     later = jnp.where(core == 0, segments, -segments).astype(jnp.int32).reshape(1)
     state = absorbed(later, queries, (own_kv,), None)
     mine, theirs = own_kv, got_kv
-    for step in range(1, chips // 2 + 1):
-        source = jnp.where(core == 0, chip - step, chip + step) % chips
-        seen = (source < chip).astype(jnp.int32).reshape(1)
-        mine = lax.ppermute(mine, "sp", onward(step, half_way))
-        blocks = (mine,)
-        if step < chips // 2:
-            theirs = lax.ppermute(theirs, "sp", onward(step, half_way - 1))
-            blocks = (mine, theirs)
-        state = absorbed(seen, queries, blocks, state)
+    for step in range(1, half_way + 1):
+        source = jnp.where(core == 1, chip - step, chip + step) % chips
+        seen = ((source < chip) & ((core == 1) | (step < half_way))).astype(jnp.int32).reshape(1)
+        mine = lax.ppermute(mine, "sp", onward(step))
+        theirs = lax.ppermute(theirs, "sp", onward(step))
+        state = absorbed(seen, queries, (mine, theirs), state)
     got_state = lax.ppermute(state[1], "sp", partner)
     pieces = pl.pallas_call(
         finish,
-        out_shape=jax.ShapeDtypeStruct((head_devices, tok_rows, columns), jnp.bfloat16),
+        out_shape=pltpu.VMEM((head_devices, tok_rows, columns), jnp.bfloat16),
         in_specs=[SMEM] + [VMEM] * 4 + [HBM] * 2,
         out_specs=VMEM,
         scratch_shapes=[
@@ -352,7 +378,8 @@
     )
 
     col_start = head_index * columns
-    summed_cols = summed_on_arrival(pieces, "tp").sum(axis=0)
+    arrived = lax.all_to_all(pieces, "tp", split_axis=0, concat_axis=0, tiled=True)
+    summed_cols = arrived.astype(jnp.float32).sum(axis=0)
     residual_cols = lax.dynamic_slice_in_dim(residual, col_start, columns, 1)
     stream_cols = (residual_cols.astype(jnp.float32) + summed_cols).astype(jnp.bfloat16)
     slot_count = 2 * tok_rows * TOP // seq_devices
@@ -387,18 +414,18 @@
     parts = pl.pallas_call(
         experts,
         out_shape=jax.ShapeDtypeStruct((head_devices, group_rows, columns), jnp.bfloat16),
-        in_specs=[VMEM] * 2 + [HBM] * LINE,
+        in_specs=[VMEM] * 3 + [HBM] * (LINE - 1),
         out_specs=VMEM,
         scratch_shapes=[
-            pltpu.VMEM(packed[0].shape, jnp.bfloat16) for _ in range(LINE)
+            pltpu.VMEM(packed[0].shape, jnp.bfloat16) for _ in range(LINE - 1)
         ]
-        + [pltpu.SemaphoreType.DMA((LINE,))],
+        + [pltpu.SemaphoreType.DMA((LINE - 1,))],
         cost_estimate=pl.CostEstimate(
             flops=6 * group_rows * model_width * LINE * width, bytes_accessed=0, transcendentals=0
         ),
         compiler_params=pltpu.CompilerParams(vmem_limit_bytes=24 << 20),
         name="experts",
-    )(arrived, norm_gain[None, :], *[held(a) for a in packed])
+    )(arrived, norm_gain[None, :], packed[-1], *[held(a) for a in packed[:-1]])
     results = (
         summed_on_arrival(parts, "tp")
         .reshape(LINE, lines, group_rows, columns)

time: 198 us -> 196 us (0.990)
  blocking collectives: 62.1 us -> 54.7 us
  starting transfers between devices: 90.7 us -> 96.4 us
    ppermute x1, starting transfers between devices: 1.92 us -> 47.9 us  [local(): got_state = lax.ppermute(state[1], 'sp', partner)]
    ppermute x17, starting transfers between devices: 63.2 us -> 20.4 us  [the longest x8 8.56 us: local(): theirs = lax.ppermute(theirs, 'sp', onward(step))]
    all_to_all x1, blocking collectives: 37.4 us -> 29.9 us  [local(): lax.all_to_all(send_rows, 'sp', split_axis=0, concat_axis=0, tiled=True)]
    ppermute x3, starting transfers between devices: 11.9 us -> 14.4 us  [local(): packed.append(lax.ppermute(packed[-1], ('sp', 'tp'), along))]
  transfers between devices with their start and end apart: 23 -> 23, of which waited for: 8 -> 3; matrix products, arithmetic and copies ran while one was open for 2% -> 2% of each run, Pallas kernels for 3% -> 4%
where the time goes in v1:
time: 196 us; the launch traced here: 194 us
  starting transfers between devices  96.4 us (49%)
  blocking collectives  54.7 us (28%)
  waiting for transfers between devices  23.3 us (12%)
  Pallas kernels  13.5 us (7%)
  other arithmetic  2.69 us (1%)
    ppermute x1, starting transfers between devices, local(): got_state = lax.ppermute(state[1], 'sp', partner)  47.9 us
    all_to_all x1, blocking collectives, local(): lax.all_to_all(send_rows, 'sp', split_axis=0, concat_axis=0, tiled=True)  29.9 us
    all_to_all x1, waiting for transfers between devices, local(): lax.all_to_all(results, 'sp', split_axis=0, concat_axis=0, tiled=True)  15.7 us
    ppermute x3, starting transfers between devices, local(): packed.append(lax.ppermute(packed[-1], ('sp', 'tp'), along))  14.4 us
    all_to_all x1, blocking collectives, local(): lax.all_to_all(copies.reshape(head_devices, group_rows, columns), 'tp', s...  12.8 us
    all_to_all x1, blocking collectives, summed_on_arrival(): lax.all_to_all(pieces, axis, split_axis=0, concat_axis=0, tiled=True)  12 us
    ppermute x8, starting transfers between devices, local(): theirs = lax.ppermute(theirs, 'sp', onward(step))  8.56 us
    all_to_all x1, starting transfers between devices, local(): lax.all_to_all(results, 'sp', split_axis=0, concat_axis=0, tiled=True)  8.22 us
  transfers between devices with their start and end apart: 23, of which 3 were waited for; matrix products, arithmetic and copies ran while one was open for 2% of the time, Pallas kernels for 4%

profile of v1, /device:TPU:1, one launch (start us, length us, event | category | flops | bytes accessed | tf_op | source)
XLA Modules:
  0.0 194.4 jit_solution(6727084322833297236)
XLA Ops:
  0.0 2.3 %w_pack.1.refs_1_ = bf16[3072,256]{1,0:T(8,128)(2,1)} custom-call(bf16[2048,128]{1,0:T(8,128)(2,1)} %bitcast.58, bf16[2048,128]{1,0:T(8,128)(2,1)} %bitcast.59, bf16[128,2048]{1,0:T(8,128)(2,1)} %bitcast.60), custom_call_target="tpu_custom_call" | custom-call | tf_op jit(solution)/shard_map/w_pack/pallas_call | solution.py:323
  2.3 5.5 %collective-permute-start.18 = (bf16[3072,256]{1,0:T(8,128)(2,1)}, bf16[3072,256]{1,0:T(8,128)(2,1)}, u32[]{:S(2)}, u32[]{:S(2)}) collective-permute-start(bf16[3072,256]{1,0:T(8,128)(2,1)} %w_pack.1.refs_1_), channel_id=1, source_target_pairs={{0,4},{1,5},{2,6},{3,7},{4,8},{5,9},{6,10},{7,11},{8,12},{9,13},{1... | collective-permute-start | bytes 4718600 | tf_op jit(solution)/shard_map/ppermute | solution.py:342
  7.8 1.0 pack.1
  8.8 5.2 %collective-permute-start = (bf16[128,1280]{1,0:T(8,128)(2,1)S(1)}, bf16[128,1280]{1,0:T(8,128)(2,1)S(1)}, u32[]{:S(2)}, u32[]{:S(2)}) collective-permute-start(bf16[128,1280]{1,0:T(8,128)(2,1)S(1)} %get-tuple-element.25.own_q_ref), channel_id=1, source_target_pairs={{0,16},{16,0},{32,48},{48,32},{64,80},{80,64},{96,112},{112,96},{1... | collective-permute-start | bytes 983048 | tf_op jit(solution)/shard_map/ppermute | solution.py:316
  14.1 1.3 collective-permute-start.1
  15.4 2.5 %collective-permute-start.9 = (bf16[128,768]{1,0:T(8,128)(2,1)S(1)}, bf16[128,768]{1,0:T(8,128)(2,1)S(1)}, u32[]{:S(2)}, u32[]{:S(2)}) collective-permute-start(bf16[128,768]{1,0:T(8,128)(2,1)S(1)} %slice.12), channel_id=1, source_target_pairs={{16,48},{48,80},{80,112},{112,144},{144,176},{176,208},{208,240},{... | collective-permute-start | bytes 589832 | tf_op jit(solution)/shard_map/ppermute | solution.py:352
  17.9 0.0 collective-permute-done.1.refs_0_
  18.0 0.7 collective-permute-start.2
  18.6 1.9 collective-permute-done.9.refs_1_
  20.5 0.7 collective-permute-start.10
  21.2 0.7 collective-permute-start.3
  21.9 0.7 collective-permute-start.11
  22.6 0.7 collective-permute-start.4
  23.3 0.7 collective-permute-start.12
  24.0 0.7 collective-permute-start.5
  24.6 0.7 collective-permute-start.13
  25.3 0.7 collective-permute-start.6
  26.0 0.7 collective-permute-start.14
  26.7 4.4 %collective-permute-start.19 = (bf16[3072,256]{1,0:T(8,128)(2,1)}, bf16[3072,256]{1,0:T(8,128)(2,1)}, u32[]{:S(2)}, u32[]{:S(2)}) collective-permute-start(bf16[3072,256]{1,0:T(8,128)(2,1)} %collective-permute-done.18.refs_2_), channel_id=1, source_target_pairs={{0,4},{1,5},{2,6},{3,7},{4,8},{5,9},{6,10},{7,11},{8,12},{9,13},{1... | collective-permute-start | bytes 4718600 | tf_op jit(solution)/shard_map/ppermute | solution.py:342
  31.1 0.7 collective-permute-start.7
  31.8 1.4 collective-permute-start.15
  33.2 1.3 collective-permute-start.8
  34.5 1.3 collective-permute-start.16
  35.9 0.7 absorb.9
  36.6 0.1 absorb.10
  36.7 0.1 absorb.11
  36.8 0.1 absorb.12
  36.8 0.1 absorb.13
  36.9 0.1 absorb.14
  37.0 0.1 absorb.15
  37.1 0.0 copy-start.3
  37.1 0.0 copy-start.1
  37.1 0.0 copy-start.2
  37.1 1.0 absorb.16
  38.1 1.1 absorb.17
  39.2 47.9 %collective-permute-start.17 = (f32[776,128]{1,0:T(8,128)S(1)}, f32[776,128]{1,0:T(8,128)S(1)}, u32[]{:S(2)}, u32[]{:S(2)}) collective-permute-start(f32[776,128]{1,0:T(8,128)S(1)} %get-tuple-element.44), channel_id=1, source_target_pairs={{0,16},{16,0},{32,48},{48,32},{64,80},{80,64},{96,112},{112,96},{1... | collective-permute-start | bytes 1191944 | tf_op jit(solution)/shard_map/ppermute | solution.py:354
  88.4 0.1 copy.34
  88.5 0.1 eq.69
  88.7 0.6 reduce-window.6
  89.3 0.1 pad_maximum_fusion.mix_ref
  89.3 0.0 copy-done.2
  89.4 3.2 %finish.1 = bf16[16,128,128]{2,1,0:T(8,128)(2,1)} custom-call(f32[2]{0:T(128)S(1)} %pad_maximum_fusion.mix_ref, f32[776,128]{1,0:T(8,128)S(1)} %get-tuple-element.43.own_ref, f32[776,128]{1,0:T(8,128)S(1)} %collective-permute-done.17.got_ref, f32[1,128]{1,0:T(1,128)S(1)} %bitcast.53, f32[1,256]{1,0:T(1,128)S(1)} %bitcast.52, bf16[128,2048]{1,0:T(8,128)(2,1)} %from_a_ref.1, ...), custom_call_target="tpu_custom_call" | custom-call | flops 201326592 | tf_op jit(solution)/shard_map/finish/pallas_call | solution.py:355
  92.6 5.5 %all-to-all-start = ((bf16[16,128,128]{2,1,0:T(8,128)(2,1)}), bf16[16,128,128]{2,1,0:T(8,128)(2,1)S(1)}, u32[]{:S(2)}, u32[]{:S(2)}) async-start(bf16[16,128,128]{2,1,0:T(8,128)(2,1)} %finish.1), calls=%async_computation | async-start | bytes 1048576 | tf_op jit(solution)/shard_map/all_to_all | solution.py:381
  98.1 0.2 slice_reduce_fusion
  98.3 0.1 eq.65
  98.5 0.1 fusion.5
  98.6 0.1 reduce_sum.61
  98.7 0.1 copy.37
  98.8 0.1 fusion.2
  98.9 4.5 %collective-permute-start.20 = (bf16[3072,256]{1,0:T(8,128)(2,1)}, bf16[3072,256]{1,0:T(8,128)(2,1)S(1)}, u32[]{:S(2)}, u32[]{:S(2)}) collective-permute-start(bf16[3072,256]{1,0:T(8,128)(2,1)} %collective-permute-done.19.refs_3_), channel_id=1, source_target_pairs={{0,4},{1,5},{2,6},{3,7},{4,8},{5,9},{6,10},{7,11},{8,12},{9,13},{1... | collective-permute-start | bytes 4718600 | tf_op jit(solution)/shard_map/ppermute | solution.py:342
  103.4 5.7 %all-to-all-done = bf16[16,128,128]{2,1,0:T(8,128)(2,1)S(1)} async-done(((bf16[16,128,128]{2,1,0:T(8,128)(2,1)}), bf16[16,128,128]{2,1,0:T(8,128)(2,1)S(1)}, u32[]{:S(2)}, u32[]{:S(2)}) %all-to-all-start) | async-done | bytes 524320 | tf_op jit(solution)/shard_map/all_to_all | solution.py:381
  109.1 0.1 convert_reduce_fusion
  109.2 0.8 add_convert_fusion
  110.0 0.2 convolution_convert_fusion
  110.2 29.9 %all_to_all.25 = bf16[32,16,128]{2,1,0:T(8,128)(2,1)S(1)} all-to-all(bf16[32,16,128]{2,1,0:T(8,128)(2,1)S(1)} %bitcast.57), channel_id=1, replica_groups=mesh['sp'=32,'tp'=16] {'sp'}, dimensions={0} | all-to-all | bytes 262144 | tf_op jit(solution)/shard_map/all_to_all | solution.py:403
  140.1 0.1 broadcast_in_dim.24
  140.2 12.8 %all_to_all.26.rows_ref = bf16[16,128,128]{2,1,0:T(8,128)(2,1)S(1)} all-to-all(bf16[16,128,128]{2,1,0:T(8,128)(2,1)S(1)} %bitcast.54), channel_id=1, replica_groups=mesh['sp'=32,'tp'=16] {'tp'}, dimensions={0} | all-to-all | bytes 1048576 | tf_op jit(solution)/shard_map/all_to_all | solution.py:407
  153.0 3.7 %experts.1 = bf16[16,128,128]{2,1,0:T(8,128)(2,1)S(1)} custom-call(bf16[16,128,128]{2,1,0:T(8,128)(2,1)S(1)} %all_to_all.26.rows_ref, f32[1,2048]{1,0:T(1,128)S(1)} %bitcast.51, bf16[3072,256]{1,0:T(8,128)(2,1)S(1)} %collective-permute-done.20.refs_0_, bf16[3072,256]{1,0:T(8,128)(2,1)} %w_pack.1.refs_1_, bf16[3072,256]{1,0:T(8,128)(2,1)} %collective-permute-done.18.refs_2_, ...), custom_call_target="tpu_custom_call" | custom-call | flops 805306368 | tf_op jit(solution)/shard_map/experts/pallas_call | solution.py:414
  156.8 12.0 %all_to_all.27 = bf16[16,128,128]{2,1,0:T(8,128)(2,1)S(1)} all-to-all(bf16[16,128,128]{2,1,0:T(8,128)(2,1)S(1)} %experts.1), channel_id=1, replica_groups=mesh['sp'=32,'tp'=16] {'tp'}, dimensions={0} | all-to-all | bytes 1048576 | tf_op jit(solution)/shard_map/all_to_all | solution.py:260
  168.8 0.7 bitcast_reduce_fusion
  169.5 8.2 %all-to-all-start.4 = ((bf16[32,16,128]{2,1,0:T(8,128)(2,1)}), bf16[32,16,128]{2,1,0:T(8,128)(2,1)S(1)}, u32[]{:S(2)}, u32[]{:S(2)}) async-start(bf16[32,16,128]{2,1,0:T(8,128)(2,1)} %bitcast.26), calls=%async_computation.4 | async-start | bytes 262144 | tf_op jit(solution)/shard_map/all_to_all | solution.py:436
  177.8 0.1 select_reduce_fusion
  177.9 15.7 %all-to-all-done.4 = bf16[32,16,128]{2,1,0:T(8,128)(2,1)S(1)} async-done(((bf16[32,16,128]{2,1,0:T(8,128)(2,1)}), bf16[32,16,128]{2,1,0:T(8,128)(2,1)S(1)}, u32[]{:S(2)}, u32[]{:S(2)}) %all-to-all-start.4) | async-done | bytes 131104 | tf_op jit(solution)/shard_map/all_to_all | solution.py:436
  193.6 0.9 fusion
  (32 shorter events, 0.2 us)
Async XLA Ops:
  2.3 24.4 %collective-permute-start.18 = (bf16[3072,256]{1,0:T(8,128)(2,1)}, bf16[3072,256]{1,0:T(8,128)(2,1)}, u32[]{:S(2)}, u32[]{:S(2)}) collective-permute-start(bf16[3072,256]{1,0:T(8,128)(2,1)} %w_pack.1.refs_1_), channel_id=1, source_target_pairs={{0,4},{1,5},{2,6},{3,7},{4,8},{5,9},{6,10},{7,11},{8,12},{9,13},{1... | collective-permute-start | bytes 4718600 | tf_op jit(solution)/shard_map/ppermute | solution.py:342
  8.8 6.5 %collective-permute-start = (bf16[128,1280]{1,0:T(8,128)(2,1)S(1)}, bf16[128,1280]{1,0:T(8,128)(2,1)S(1)}, u32[]{:S(2)}, u32[]{:S(2)}) collective-permute-start(bf16[128,1280]{1,0:T(8,128)(2,1)S(1)} %get-tuple-element.25.own_q_ref), channel_id=1, source_target_pairs={{0,16},{16,0},{32,48},{48,32},{64,80},{80,64},{96,112},{112,96},{1... | collective-permute-start | bytes 983048 | tf_op jit(solution)/shard_map/ppermute | solution.py:316
  14.1 3.9 %collective-permute-start.1 = (bf16[128,768]{1,0:T(8,128)(2,1)S(1)}, bf16[128,768]{1,0:T(8,128)(2,1)S(1)}, u32[]{:S(2)}, u32[]{:S(2)}) collective-permute-start(bf16[128,768]{1,0:T(8,128)(2,1)S(1)} %get-tuple-element.26.refs_0_), channel_id=1, source_target_pairs={{16,48},{48,80},{80,112},{112,144},{144,176},{176,208},{208,240},{... | collective-permute-start | bytes 589832 | tf_op jit(solution)/shard_map/ppermute | solution.py:351
  15.4 5.1 %collective-permute-start.9 = (bf16[128,768]{1,0:T(8,128)(2,1)S(1)}, bf16[128,768]{1,0:T(8,128)(2,1)S(1)}, u32[]{:S(2)}, u32[]{:S(2)}) collective-permute-start(bf16[128,768]{1,0:T(8,128)(2,1)S(1)} %slice.12), channel_id=1, source_target_pairs={{16,48},{48,80},{80,112},{112,144},{144,176},{176,208},{208,240},{... | collective-permute-start | bytes 589832 | tf_op jit(solution)/shard_map/ppermute | solution.py:352
  18.0 3.2 %collective-permute-start.2 = (bf16[128,768]{1,0:T(8,128)(2,1)S(1)}, bf16[128,768]{1,0:T(8,128)(2,1)S(1)}, u32[]{:S(2)}, u32[]{:S(2)}) collective-permute-start(bf16[128,768]{1,0:T(8,128)(2,1)S(1)} %collective-permute-done.1.refs_0_), channel_id=1, source_target_pairs={{48,80},{80,112},{112,144},{144,176},{176,208},{208,240},{240,272}... | collective-permute-start | bytes 589832 | tf_op jit(solution)/shard_map/ppermute | solution.py:351
  20.5 1.4 collective-permute-start.10
  21.2 1.4 collective-permute-start.3
  21.9 1.4 collective-permute-start.11
  22.6 1.4 collective-permute-start.4
  23.3 1.4 collective-permute-start.12
  24.0 1.4 collective-permute-start.5
  24.6 1.4 collective-permute-start.13
  25.3 5.8 %collective-permute-start.6 = (bf16[128,768]{1,0:T(8,128)(2,1)S(1)}, bf16[128,768]{1,0:T(8,128)(2,1)S(1)}, u32[]{:S(2)}, u32[]{:S(2)}) collective-permute-start(bf16[128,768]{1,0:T(8,128)(2,1)S(1)} %collective-permute-done.5.refs_0_), channel_id=1, source_target_pairs={{176,208},{208,240},{240,272},{272,304},{304,336},{336,368},{368,4... | collective-permute-start | bytes 589832 | tf_op jit(solution)/shard_map/ppermute | solution.py:351
  26.0 5.8 %collective-permute-start.14 = (bf16[128,768]{1,0:T(8,128)(2,1)S(1)}, bf16[128,768]{1,0:T(8,128)(2,1)S(1)}, u32[]{:S(2)}, u32[]{:S(2)}) collective-permute-start(bf16[128,768]{1,0:T(8,128)(2,1)S(1)} %collective-permute-done.13.refs_1_), channel_id=1, source_target_pairs={{176,208},{208,240},{240,272},{272,304},{304,336},{336,368},{368,4... | collective-permute-start | bytes 589832 | tf_op jit(solution)/shard_map/ppermute | solution.py:352
  26.7 72.2 %collective-permute-start.19 = (bf16[3072,256]{1,0:T(8,128)(2,1)}, bf16[3072,256]{1,0:T(8,128)(2,1)}, u32[]{:S(2)}, u32[]{:S(2)}) collective-permute-start(bf16[3072,256]{1,0:T(8,128)(2,1)} %collective-permute-done.18.refs_2_), channel_id=1, source_target_pairs={{0,4},{1,5},{2,6},{3,7},{4,8},{5,9},{6,10},{7,11},{8,12},{9,13},{1... | collective-permute-start | bytes 4718600 | tf_op jit(solution)/shard_map/ppermute | solution.py:342
  31.1 2.1 %collective-permute-start.7 = (bf16[128,768]{1,0:T(8,128)(2,1)S(1)}, bf16[128,768]{1,0:T(8,128)(2,1)S(1)}, u32[]{:S(2)}, u32[]{:S(2)}) collective-permute-start(bf16[128,768]{1,0:T(8,128)(2,1)S(1)} %collective-permute-done.6.refs_0_), channel_id=1, source_target_pairs={{208,240},{240,272},{272,304},{304,336},{336,368},{368,400},{400,4... | collective-permute-start | bytes 589832 | tf_op jit(solution)/shard_map/ppermute | solution.py:351
  31.8 2.7 %collective-permute-start.15 = (bf16[128,768]{1,0:T(8,128)(2,1)S(1)}, bf16[128,768]{1,0:T(8,128)(2,1)}, u32[]{:S(2)}, u32[]{:S(2)}) collective-permute-start(bf16[128,768]{1,0:T(8,128)(2,1)S(1)} %collective-permute-done.14.refs_1_), channel_id=1, source_target_pairs={{208,240},{240,272},{272,304},{304,336},{336,368},{368,400},{400,4... | collective-permute-start | bytes 589832 | tf_op jit(solution)/shard_map/ppermute | solution.py:352
  33.2 4.9 %collective-permute-start.8 = (bf16[128,768]{1,0:T(8,128)(2,1)S(1)}, bf16[128,768]{1,0:T(8,128)(2,1)}, u32[]{:S(2)}, u32[]{:S(2)}) collective-permute-start(bf16[128,768]{1,0:T(8,128)(2,1)S(1)} %collective-permute-done.7.refs_0_), channel_id=1, source_target_pairs={{240,272},{272,304},{304,336},{336,368},{368,400},{400,432},{432,4... | collective-permute-start | bytes 589832 | tf_op jit(solution)/shard_map/ppermute | solution.py:351
  34.5 3.6 %collective-permute-start.16 = (bf16[128,768]{1,0:T(8,128)(2,1)}, bf16[128,768]{1,0:T(8,128)(2,1)}, u32[]{:S(2)}, u32[]{:S(2)}) collective-permute-start(bf16[128,768]{1,0:T(8,128)(2,1)} %collective-permute-done.15.refs_1_), channel_id=1, source_target_pairs={{240,272},{272,304},{304,336},{336,368},{368,400},{400,432},{432,4... | collective-permute-start | bytes 589832 | tf_op jit(solution)/shard_map/ppermute | solution.py:352
  37.1 51.3 %copy-start.3 = (s32[128,2]{0,1:T(2,128)S(1)}, s32[128,2]{0,1:T(2,128)}, u32[]{:S(2)}) copy-start(s32[128,2]{0,1:T(2,128)} %param.33) | copy-start | bytes 3076
  37.1 52.3 %copy-start.1 = (f32[256]{0:T(256)S(1)}, f32[256]{0:T(256)}, u32[]{:S(2)}) copy-start(f32[256]{0:T(256)} %param.29) | copy-start | bytes 3076
  37.1 52.3 %copy-start.2 = (f32[128]{0:T(128)S(1)}, f32[128]{0:T(128)}, u32[]{:S(2)}) copy-start(f32[128]{0:T(128)} %param.28) | copy-start | bytes 1540
  39.2 50.2 %collective-permute-start.17 = (f32[776,128]{1,0:T(8,128)S(1)}, f32[776,128]{1,0:T(8,128)S(1)}, u32[]{:S(2)}, u32[]{:S(2)}) collective-permute-start(f32[776,128]{1,0:T(8,128)S(1)} %get-tuple-element.44), channel_id=1, source_target_pairs={{0,16},{16,0},{32,48},{48,32},{64,80},{80,64},{96,112},{112,96},{1... | collective-permute-start | bytes 1191944 | tf_op jit(solution)/shard_map/ppermute | solution.py:354
  92.6 16.5 %all-to-all-start = ((bf16[16,128,128]{2,1,0:T(8,128)(2,1)}), bf16[16,128,128]{2,1,0:T(8,128)(2,1)S(1)}, u32[]{:S(2)}, u32[]{:S(2)}) async-start(bf16[16,128,128]{2,1,0:T(8,128)(2,1)} %finish.1), calls=%async_computation | async-start | bytes 1048576 | tf_op jit(solution)/shard_map/all_to_all | solution.py:381
  98.8 54.3 %copy-start = (f32[2048]{0:T(1024)S(1)}, f32[2048]{0:T(1024)}, u32[]{:S(2)}) copy-start(f32[2048]{0:T(1024)} %param.32) | copy-start | bytes 24580
  98.9 54.1 %collective-permute-start.20 = (bf16[3072,256]{1,0:T(8,128)(2,1)}, bf16[3072,256]{1,0:T(8,128)(2,1)S(1)}, u32[]{:S(2)}, u32[]{:S(2)}) collective-permute-start(bf16[3072,256]{1,0:T(8,128)(2,1)} %collective-permute-done.19.refs_3_), channel_id=1, source_target_pairs={{0,4},{1,5},{2,6},{3,7},{4,8},{5,9},{6,10},{7,11},{8,12},{9,13},{1... | collective-permute-start | bytes 4718600 | tf_op jit(solution)/shard_map/ppermute | solution.py:342
  156.8 21.0 %copy-start.4 = (f32[128,2]{0,1:T(2,128)S(1)}, f32[128,2]{0,1:T(2,128)}, u32[]{:S(2)}) copy-start(f32[128,2]{0,1:T(2,128)} %param.34) | copy-start | bytes 3076
  169.5 24.1 %all-to-all-start.4 = ((bf16[32,16,128]{2,1,0:T(8,128)(2,1)}), bf16[32,16,128]{2,1,0:T(8,128)(2,1)S(1)}, u32[]{:S(2)}, u32[]{:S(2)}) async-start(bf16[32,16,128]{2,1,0:T(8,128)(2,1)} %bitcast.26), calls=%async_computation.4 | async-start | bytes 262144 | tf_op jit(solution)/shard_map/all_to_all | solution.py:436

commit v2 on v1

--- a/solution.py
+++ b/solution.py
@@ -117,75 +117,77 @@
     )(flag, *queries, *kvs, *(olds or ()))
 
 
-def pack(qa_ref, qb_ref, ka_ref, va_ref, kb_ref, vb_ref, q_ref, kv_ref, qa_buf, sems):
+def pack(qa_ref, qb_ref, ka_ref, va_ref, kb_ref, vb_ref, gate_ref, up_ref, down_ref, *refs):
+    q_ref, kv_ref, out_ref, qa_buf, buf, sems = refs
     width = qa_buf.shape[1]
     q_cols = q_ref.shape[1] - kv_ref.shape[1]
-    places = (
-        (qa_ref, qa_buf),
-        (ka_ref, kv_ref.at[:, :width]),
-        (va_ref, kv_ref.at[:, width : 2 * width]),
-        (kb_ref, kv_ref.at[:, 2 * width : 4 * width]),
-        (vb_ref, kv_ref.at[:, 4 * width :]),
-        (qb_ref, q_ref.at[:, 2 * width : q_cols]),
-    )
-    copies = [pltpu.make_async_copy(a, b, sems.at[i]) for i, (a, b) in enumerate(places)]
+    deep, wide = gate_ref.shape
+    count = 0
+
+    def begin(places):
+        nonlocal count
+        copies = []
+        for a, b in places:
+            copies.append(pltpu.make_async_copy(a, b, sems.at[count]))
+            copies[-1].start()
+            count += 1
+        return copies
+
+    first = begin(
+        (
+            (qa_ref, qa_buf),
+            (ka_ref, kv_ref.at[:, :width]),
+            (va_ref, kv_ref.at[:, width : 2 * width]),
+            (kb_ref, kv_ref.at[:, 2 * width : 4 * width]),
+            (vb_ref, kv_ref.at[:, 4 * width :]),
+            (qb_ref, q_ref.at[:, 2 * width : q_cols]),
+        )
+    )
+    pieces = []
+    chunk = deep // 2
+    for start in range(0, deep, chunk):
+        rows = slice(start, start + chunk)
+        sides = ((gate_ref, slice(0, wide)), (up_ref, slice(wide, 2 * wide)))
+        pieces.append((rows, begin([(ref.at[rows, :], buf.at[rows, cols]) for ref, cols in sides])))
+    places = []
+    for j in range(deep // (2 * wide)):
+        start = deep + j * wide
+        cols = slice(2 * j * wide, 2 * (j + 1) * wide)
+        places.append((down_ref.at[:, cols], buf.at[start : start + wide, :]))
+    pieces.append((slice(deep, deep + deep // 2), begin(places)))
+    for copy in first:
+        copy.wait()
+    both = qa_buf[...]
+    first_map = lax.broadcasted_iota(jnp.int32, both.shape, 1) < DK_A
+    q_ref[:, :width] = jnp.where(first_map, both, 0)
+    q_ref[:, width : 2 * width] = jnp.where(first_map, 0, both)
+    q_ref[:, q_cols:] = kv_ref[...]
+    outs = []
+    for rows, copies in pieces:
+        for copy in copies:
+            copy.wait()
+        outs += begin([(buf.at[rows, :], out_ref.at[rows, :])])
+    for copy in outs:
+        copy.wait()
+
+
+def fetch(*refs):
+    count = (len(refs) - 1) // 2
+    sems = refs[-1]
+    copies = [pltpu.make_async_copy(refs[i], refs[count + i], sems.at[i]) for i in range(count)]
     for copy in copies:
         copy.start()
     for copy in copies:
         copy.wait()
-    both = qa_buf[...]
-    first = lax.broadcasted_iota(jnp.int32, both.shape, 1) < DK_A
-    q_ref[:, :width] = jnp.where(first, both, 0)
-    q_ref[:, width : 2 * width] = jnp.where(first, 0, both)
-    q_ref[:, q_cols:] = kv_ref[...]
-
-
-def pack_weights(gate_ref, up_ref, down_ref, out_ref, buf, sems):
-    deep, width = gate_ref.shape
-    chunk = deep // 2
-    pieces = []
-    for start in range(0, deep, chunk):
-        rows = slice(start, start + chunk)
-        ins = [(ref.at[rows, :], buf.at[rows, cols]) for ref, cols in (
-            (gate_ref, slice(0, width)),
-            (up_ref, slice(width, 2 * width)),
-        )]
-        pieces.append((rows, ins))
-    ins = []
-    for j in range(deep // (2 * width)):
-        start = deep + j * width
-        ins.append(
-            (
-                down_ref.at[:, 2 * j * width : 2 * (j + 1) * width],
-                buf.at[start : start + width, :],
-            )
-        )
-    pieces.append((slice(deep, deep + deep // 2), ins))
-    count, started = 0, []
-    for rows, ins in pieces:
-        copies = []
-        for a, b in ins:
-            copies.append(pltpu.make_async_copy(a, b, sems.at[count]))
-            copies[-1].start()
-            count += 1
-        started.append((rows, copies))
-    outs = []
-    for rows, copies in started:
-        for copy in copies:
-            copy.wait()
-        outs.append(pltpu.make_async_copy(buf.at[rows, :], out_ref.at[rows, :], sems.at[count]))
-        outs[-1].start()
-        count += 1
-    for copy in outs:
-        copy.wait()
-
-
-def finish(mix_ref, own_ref, got_ref, gain_a_ref, gain_b_ref, from_a_ref, from_b_ref, out_ref, *bufs):
-    proj_a_ref, proj_b_ref, sems = bufs
-    copy_a = pltpu.make_async_copy(from_a_ref, proj_a_ref, sems.at[0])
-    copy_b = pltpu.make_async_copy(from_b_ref, proj_b_ref, sems.at[1])
-    copy_a.start()
-    copy_b.start()
+
+
+def finish(mix_ref, at_ref, own_ref, got_ref, *refs):
+    gain_a_ref, gain_b_ref, proj_a_ref, proj_b_ref, residual_ref, out_ref, cols_ref, sem = refs
+    start = pl.multiple_of(at_ref[0] * cols_ref.shape[1], cols_ref.shape[1])
+    copy = pltpu.make_async_copy(
+        residual_ref.at[:, pl.ds(start, cols_ref.shape[1])], cols_ref, sem
+    )
+    copy.start()
 
     def merged(index):
         at_max = slice(SUMS + index, SUMS + index + 1)
@@ -205,8 +207,6 @@
 
     heads_a = head(0, mix_ref[0], gain_a_ref)
     heads_b = head(2, mix_ref[1], gain_b_ref)
-    copy_a.wait()
-    copy_b.wait()
     width = out_ref.shape[2]
     across = (((0,), (0,)), ((), ()))
     step = 4
@@ -219,6 +219,18 @@
         )
         for i in range(step):
             out_ref[piece + i] = branch[:, i * width : (i + 1) * width].astype(jnp.bfloat16)
+    copy.wait()
+
+
+def place(arrived_ref, residual_ref, select_ref, stream_ref, send_ref):
+    summed = arrived_ref[0].astype(jnp.float32)
+    for i in range(1, arrived_ref.shape[0]):
+        summed = summed + arrived_ref[i].astype(jnp.float32)
+    stream = (residual_ref[...].astype(jnp.float32) + summed).astype(jnp.bfloat16)
+    stream_ref[...] = stream
+    send_ref[...] = lax.dot_general(
+        select_ref[...], stream, (((0,), (0,)), ((), ())), preferred_element_type=jnp.float32
+    ).astype(jnp.bfloat16)
 
 
 def experts(rows_ref, gain_ref, *refs):
@@ -295,43 +307,38 @@
     partner = [(i, i ^ 1) for i in range(seq_devices)]
     half_way = chips // 2
 
-    def onward(step):
-        up = [(2 * i + 1, 2 * (i + 1) + 1) for i in range(step - 1, chips - 1)]
-        places = [(block - step) % chips for block in range(half_way - 1)] if step < half_way else []
-        return up + [(2 * ((i + 1) % chips), 2 * i) for i in places]
+    quarter = half_way // 2
+
+    def onward(step, up_blocks, down_blocks):
+        up = [block + step for block in up_blocks if block + step < chips]
+        down = [(block - step) % chips for block in down_blocks]
+        return [(2 * i - 1, 2 * i + 1) for i in up] + [(2 * ((i + 1) % chips), 2 * i) for i in down]
 
     fields = [a[:, 0] for a in (query_a, query_b, keys_a, values_a, keys_b, values_b)]
-    own_all, own_kv = pl.pallas_call(
+    deep, width = expert_gate.shape[1:]
+    weights = [a[0] for a in (expert_gate, expert_up, expert_down)]
+    own_all, own_kv, packed = pl.pallas_call(
         pack,
         out_shape=(
             jax.ShapeDtypeStruct((tok_rows, 4 * DK_B + SUMS), jnp.bfloat16),
             jax.ShapeDtypeStruct((tok_rows, SUMS), jnp.bfloat16),
-        ),
-        in_specs=[HBM] * 6,
-        out_specs=(VMEM, VMEM),
-        scratch_shapes=[pltpu.VMEM(fields[0].shape, jnp.bfloat16), pltpu.SemaphoreType.DMA((6,))],
+            pltpu.HBM((deep + deep // 2, 2 * width), jnp.bfloat16),
+        ),
+        in_specs=[HBM] * 9,
+        out_specs=(VMEM, VMEM, HBM),
+        scratch_shapes=[
+            pltpu.VMEM(fields[0].shape, jnp.bfloat16),
+            pltpu.VMEM((deep + deep // 2, 2 * width), jnp.bfloat16),
+            pltpu.SemaphoreType.DMA((6 + 4 + deep // (2 * width) + 3,)),
+        ],
         compiler_params=pltpu.CompilerParams(vmem_limit_bytes=8 << 20),
         name="pack",
-    )(*[held(a) for a in fields])
+    )(*[held(a) for a in fields + weights])
     got_all = lax.ppermute(own_all, "sp", partner)
     got_kv = got_all[:, 4 * DK_B :]
     queries = (own_all, got_all)
 
     lines = head_devices // LINE
-    width = expert_gate.shape[2]
-    deep = expert_gate.shape[1]
-    packed = pl.pallas_call(
-        pack_weights,
-        out_shape=pltpu.HBM((deep + deep // 2, 2 * width), jnp.bfloat16),
-        in_specs=[HBM] * 3,
-        out_specs=HBM,
-        scratch_shapes=[
-            pltpu.VMEM((deep + deep // 2, 2 * width), jnp.bfloat16),
-            pltpu.SemaphoreType.DMA((4 + deep // (2 * width) + 3,)),
-        ],
-        compiler_params=pltpu.CompilerParams(vmem_limit_bytes=8 << 20),
-        name="w_pack",
-    )(*[held(a[0]) for a in (expert_gate, expert_up, expert_down)])
     packed = [packed]
     along = [
         (s * head_devices + t, s * head_devices + (t + (lines if s % 2 == 0 else -lines)) % head_devices)
@@ -345,43 +352,57 @@
     later = jnp.where(core == 0, segments, -segments).astype(jnp.int32).reshape(1)
     state = absorbed(later, queries, (own_kv,), None)
     mine, theirs = own_kv, got_kv
-    for step in range(1, half_way + 1):
+    for step in range(1, half_way):
         source = jnp.where(core == 1, chip - step, chip + step) % chips
-        seen = ((source < chip) & ((core == 1) | (step < half_way))).astype(jnp.int32).reshape(1)
-        mine = lax.ppermute(mine, "sp", onward(step))
-        theirs = lax.ppermute(theirs, "sp", onward(step))
+        seen = (source < chip).astype(jnp.int32).reshape(1)
+        pairs = onward(step, range(chips), range(half_way - 1))
+        mine = lax.ppermute(mine, "sp", pairs)
+        theirs = lax.ppermute(theirs, "sp", pairs)
         state = absorbed(seen, queries, (mine, theirs), state)
+    near = (chip >= half_way) & (chip < half_way + quarter)
+    mine = lax.ppermute(mine, "sp", onward(half_way, range(half_way), range(quarter)))
+    theirs = lax.ppermute(theirs, "sp", onward(half_way, range(quarter, half_way), ()))
+    seen = jnp.where(core == 1, chip >= half_way, near).astype(jnp.int32).reshape(1)
+    state = absorbed(seen, queries, (mine,), state)
+    seen = ((core == 1) & (chip >= half_way + quarter)).astype(jnp.int32).reshape(1)
+    state = absorbed(seen, queries, (theirs,), state)
     got_state = lax.ppermute(state[1], "sp", partner)
-    pieces = pl.pallas_call(
+    projs = pl.pallas_call(
+        fetch,
+        out_shape=tuple(pltpu.VMEM(a.shape, jnp.bfloat16) for a in (proj_a, proj_b)),
+        in_specs=[HBM] * 2,
+        out_specs=(VMEM, VMEM),
+        scratch_shapes=[pltpu.SemaphoreType.DMA((2,))],
+        compiler_params=pltpu.CompilerParams(vmem_limit_bytes=4 << 20),
+        name="fetch",
+    )(held(proj_a), held(proj_b))
+    mix = jnp.concatenate([lambda_a, lambda_b])
+    pieces, residual_cols = pl.pallas_call(
         finish,
-        out_shape=pltpu.VMEM((head_devices, tok_rows, columns), jnp.bfloat16),
-        in_specs=[SMEM] + [VMEM] * 4 + [HBM] * 2,
-        out_specs=VMEM,
-        scratch_shapes=[
-            pltpu.VMEM(proj_a.shape, jnp.bfloat16),
-            pltpu.VMEM(proj_b.shape, jnp.bfloat16),
-            pltpu.SemaphoreType.DMA((2,)),
-        ],
+        out_shape=(
+            jax.ShapeDtypeStruct((head_devices, tok_rows, columns), jnp.bfloat16),
+            jax.ShapeDtypeStruct((tok_rows, columns), jnp.bfloat16),
+        ),
+        in_specs=[SMEM] * 2 + [VMEM] * 6 + [HBM],
+        out_specs=(VMEM, VMEM),
+        scratch_shapes=[pltpu.SemaphoreType.DMA],
         cost_estimate=pl.CostEstimate(
             flops=2 * tok_rows * model_width * 384, bytes_accessed=0, transcendentals=0
         ),
         compiler_params=pltpu.CompilerParams(vmem_limit_bytes=16 << 20),
         name="finish",
     )(
-        jnp.concatenate([lambda_a, lambda_b]),
+        mix,
+        head_index.astype(jnp.int32).reshape(1),
         state[0],
         got_state,
         gain_a[None, :],
         gain_b[None, :],
-        held(proj_a),
-        held(proj_b),
-    )
-
-    col_start = head_index * columns
+        *projs,
+        held(residual),
+    )
+
     arrived = lax.all_to_all(pieces, "tp", split_axis=0, concat_axis=0, tiled=True)
-    summed_cols = arrived.astype(jnp.float32).sum(axis=0)
-    residual_cols = lax.dynamic_slice_in_dim(residual, col_start, columns, 1)
-    stream_cols = (residual_cols.astype(jnp.float32) + summed_cols).astype(jnp.bfloat16)
     slot_count = 2 * tok_rows * TOP // seq_devices
     assign = routes.reshape(-1)
     onehot = (assign[:, None] == jnp.arange(seq_devices, dtype=jnp.int32)[None, :]).astype(
@@ -396,9 +417,17 @@
     select = jnp.sum(placed.astype(jnp.bfloat16), axis=1)
     gates = route_weight / jnp.sum(route_weight, axis=1, keepdims=True)
     combine = jnp.sum(placed.astype(jnp.float32) * gates[:, :, None], axis=1)
-    send_rows = jnp.einsum(
-        "ts,td->sd", select, stream_cols, preferred_element_type=jnp.float32
-    ).astype(jnp.bfloat16)
+    stream_cols, send_rows = pl.pallas_call(
+        place,
+        out_shape=(
+            jax.ShapeDtypeStruct((tok_rows, columns), jnp.bfloat16),
+            jax.ShapeDtypeStruct((seq_devices * slot_count, columns), jnp.bfloat16),
+        ),
+        in_specs=[VMEM] * 3,
+        out_specs=(VMEM, VMEM),
+        compiler_params=pltpu.CompilerParams(vmem_limit_bytes=4 << 20),
+        name="place",
+    )(arrived, residual_cols, select)
     send_rows = send_rows.reshape(seq_devices, slot_count, columns)
     routed = lax.all_to_all(send_rows, "sp", split_axis=0, concat_axis=0, tiled=True)
     group_rows = seq_devices * slot_count // LINE

time: 196 us -> 203 us (1.036)
  waiting for transfers between devices: 23.3 us -> 37.9 us
  starting transfers between devices: 96.4 us -> 88.4 us
  local copies, waits for them, and re-layouts: 0.92 us -> 3.11 us
    all_to_all x1, waiting for transfers between devices: 5.71 us -> 16.3 us  [local(): lax.all_to_all(pieces, 'tp', split_axis=0, concat_axis=0, tiled=True)]
    ppermute x1, starting transfers between devices: 47.9 us -> 42.7 us  [local(): got_state = lax.ppermute(state[1], 'sp', partner)]
    ppermute x3, waiting for transfers between devices: 0.01 us -> 3.95 us  [local(): packed.append(lax.ppermute(packed[-1], ('sp', 'tp'), along))]
    unnamed x11 -> x19, local copies, waits for them, and re-layouts: 0.14 us -> 2.33 us
    pallas_call x2 -> x3, Pallas kernels: 5.54 us -> 3.87 us  [the longest x1 2.22 us: local(): pl.pallas_call(finish, out_shape=(jax.ShapeDtypeStruct((head_devices, tok...]
  transfers between devices with their start and end apart: 23 -> 23, of which waited for: 3 -> 4; matrix products, arithmetic and copies ran while one was open for 2% -> 1% of each run, Pallas kernels for 4% -> 3%
where the time goes in v2:
time: 203 us; the launch traced here: 202 us
  starting transfers between devices  88.4 us (44%)
  blocking collectives  55.9 us (28%)
  waiting for transfers between devices  37.9 us (19%)
  Pallas kernels  12.3 us (6%)
  local copies, waits for them, and re-layouts  3.11 us (2%)
  other arithmetic  2.46 us (1%)
    ppermute x1, starting transfers between devices, local(): got_state = lax.ppermute(state[1], 'sp', partner)  42.7 us
    all_to_all x1, blocking collectives, local(): lax.all_to_all(send_rows, 'sp', split_axis=0, concat_axis=0, tiled=True)  29.7 us
    all_to_all x1, waiting for transfers between devices, local(): lax.all_to_all(pieces, 'tp', split_axis=0, concat_axis=0, tiled=True)  16.3 us
    all_to_all x1, waiting for transfers between devices, local(): lax.all_to_all(results, 'sp', split_axis=0, concat_axis=0, tiled=True)  15.7 us
    all_to_all x1, blocking collectives, local(): lax.all_to_all(copies.reshape(head_devices, group_rows, columns), 'tp', s...  14.2 us
    ppermute x3, starting transfers between devices, local(): packed.append(lax.ppermute(packed[-1], ('sp', 'tp'), along))  12.8 us
    all_to_all x1, blocking collectives, summed_on_arrival(): lax.all_to_all(pieces, axis, split_axis=0, concat_axis=0, tiled=True)  12 us
    all_to_all x1, starting transfers between devices, local(): lax.all_to_all(results, 'sp', split_axis=0, concat_axis=0, tiled=True)  8.29 us
  transfers between devices with their start and end apart: 23, of which 4 were waited for; matrix products, arithmetic and copies ran while one was open for 1% of the time, Pallas kernels for 3%

profile of v2, /device:TPU:1, one launch (start us, length us, event | category | flops | bytes accessed | tf_op | source)
XLA Modules:
  0.0 202.3 jit_solution(16767291614435887742)
XLA Ops:
  0.0 2.5 %pack.1 = (bf16[128,1280]{1,0:T(8,128)(2,1)S(1)}, bf16[128,768]{1,0:T(8,128)(2,1)S(1)}, bf16[3072,256]{1,0:T(8,128)(2,1)}) custom-call(bf16[128,128]{1,0:T(8,128)(2,1)} %bitcast.64, bf16[128,256]{1,0:T(8,128)(2,1)} %bitcast.61, bf16[128,128]{1,0:T(8,128)(2,1)} %bitcast.65, bf16[128,128]{1,0:T(8,128)(2,1)} %bitcast.66, bf16[128,256]{1,0:T(8,128)(2,1)} %bitcast.62, ...), custom_call_target="tpu_custom_call" | custom-call | tf_op jit(solution)/shard_map/pack/pallas_call | solution.py:320
  2.5 5.5 %collective-permute-start.18 = (bf16[3072,256]{1,0:T(8,128)(2,1)}, bf16[3072,256]{1,0:T(8,128)(2,1)}, u32[]{:S(2)}, u32[]{:S(2)}) collective-permute-start(bf16[3072,256]{1,0:T(8,128)(2,1)} %get-tuple-element.62.refs_1_), channel_id=1, source_target_pairs={{0,4},{1,5},{2,6},{3,7},{4,8},{5,9},{6,10},{7,11},{8,12},{9,13},{1... | collective-permute-start | bytes 4718600 | tf_op jit(solution)/shard_map/ppermute | solution.py:349
  8.0 5.2 %collective-permute-start = (bf16[128,1280]{1,0:T(8,128)(2,1)S(1)}, bf16[128,1280]{1,0:T(8,128)(2,1)S(1)}, u32[]{:S(2)}, u32[]{:S(2)}) collective-permute-start(bf16[128,1280]{1,0:T(8,128)(2,1)S(1)} %get-tuple-element.34.own_q_ref), channel_id=1, source_target_pairs={{0,16},{16,0},{32,48},{48,32},{64,80},{80,64},{96,112},{112,96},{1... | collective-permute-start | bytes 983048 | tf_op jit(solution)/shard_map/ppermute | solution.py:337
  13.2 1.3 collective-permute-start.9
  14.6 2.5 %collective-permute-start.1 = (bf16[128,768]{1,0:T(8,128)(2,1)S(1)}, bf16[128,768]{1,0:T(8,128)(2,1)S(1)}, u32[]{:S(2)}, u32[]{:S(2)}) collective-permute-start(bf16[128,768]{1,0:T(8,128)(2,1)S(1)} %slice.12), channel_id=1, source_target_pairs={{16,48},{48,80},{80,112},{112,144},{144,176},{176,208},{208,240},{... | collective-permute-start | bytes 589832 | tf_op jit(solution)/shard_map/ppermute | solution.py:360
  17.1 0.7 collective-permute-start.10
  17.8 1.9 collective-permute-done.1.refs_1_
  19.7 0.7 collective-permute-start.2
  20.3 0.7 collective-permute-start.11
  21.0 0.7 collective-permute-start.3
  21.7 3.9 %collective-permute-done.18.refs_2_ = bf16[3072,256]{1,0:T(8,128)(2,1)} collective-permute-done((bf16[3072,256]{1,0:T(8,128)(2,1)}, bf16[3072,256]{1,0:T(8,128)(2,1)}, u32[]{:S(2)}, u32[]{:S(2)}) %collective-permute-start.18) | collective-permute-done | bytes 1572896 | tf_op jit(solution)/shard_map/ppermute | solution.py:349
  25.7 5.0 %collective-permute-start.19 = (bf16[3072,256]{1,0:T(8,128)(2,1)}, bf16[3072,256]{1,0:T(8,128)(2,1)}, u32[]{:S(2)}, u32[]{:S(2)}) collective-permute-start(bf16[3072,256]{1,0:T(8,128)(2,1)} %collective-permute-done.18.refs_2_), channel_id=1, source_target_pairs={{0,4},{1,5},{2,6},{3,7},{4,8},{5,9},{6,10},{7,11},{8,12},{9,13},{1... | collective-permute-start | bytes 4718600 | tf_op jit(solution)/shard_map/ppermute | solution.py:349
  30.7 0.7 collective-permute-start.12
  31.4 0.7 collective-permute-start.4
  32.1 0.7 collective-permute-start.13
  32.8 0.7 collective-permute-start.5
  33.5 0.7 collective-permute-start.14
  34.2 0.7 collective-permute-start.6
  34.8 0.7 copy-done
  35.5 1.4 collective-permute-start.15
  36.9 0.7 collective-permute-start.7
  37.6 0.7 copy-done.2
  38.2 0.7 collective-permute-start.16
  38.9 0.7 collective-permute-start.8
  39.8 0.7 absorb.10
  40.5 0.1 absorb.11
  40.6 0.1 absorb.12
  40.7 0.1 absorb.13
  40.8 0.1 absorb.14
  40.8 0.8 copy-done.1
  41.6 0.1 absorb.15
  41.7 0.1 copy-done.3
  41.7 0.1 absorb.16
  41.8 1.0 absorb.17
  42.8 0.1 absorb.18
  42.9 0.1 absorb.19
  43.0 42.7 %collective-permute-start.17 = (f32[776,128]{1,0:T(8,128)S(1)}, f32[776,128]{1,0:T(8,128)S(1)}, u32[]{:S(2)}, u32[]{:S(2)}) collective-permute-start(f32[776,128]{1,0:T(8,128)S(1)} %get-tuple-element.55), channel_id=1, source_target_pairs={{0,16},{16,0},{32,48},{48,32},{64,80},{80,64},{96,112},{112,96},{1... | collective-permute-start | bytes 1191944 | tf_op jit(solution)/shard_map/ppermute | solution.py:369
  86.9 0.1 copy.34
  87.0 0.1 eq.68
  87.2 0.6 reduce-window.6
  87.8 1.4 fetch.1
  89.2 0.1 pad_maximum_fusion.mix_ref
  89.3 2.4 %collective-permute-start.20 = (bf16[3072,256]{1,0:T(8,128)(2,1)}, bf16[3072,256]{1,0:T(8,128)(2,1)S(1)}, u32[]{:S(2)}, u32[]{:S(2)}) collective-permute-start(bf16[3072,256]{1,0:T(8,128)(2,1)} %collective-permute-done.19.refs_3_), channel_id=1, source_target_pairs={{0,4},{1,5},{2,6},{3,7},{4,8},{5,9},{6,10},{7,11},{8,12},{9,13},{1... | collective-permute-start | bytes 4718600 | tf_op jit(solution)/shard_map/ppermute | solution.py:349
  91.7 2.2 %finish.1 = (bf16[16,128,128]{2,1,0:T(8,128)(2,1)}, bf16[128,128]{1,0:T(8,128)(2,1)S(1)}) custom-call(f32[2]{0:T(128)S(1)} %pad_maximum_fusion.mix_ref, s32[1]{0:T(128)} %bitcast.at_ref, f32[776,128]{1,0:T(8,128)S(1)} %get-tuple-element.54.own_ref, f32[776,128]{1,0:T(8,128)S(1)} %collective-permute-done.17.got_ref, f32[1,128]{1,0:T(1,128)S(1)} %bitcast.54, ...), custom_call_target="tpu_custom_call" | custom-call | flops 201326592 | tf_op jit(solution)/shard_map/finish/pallas_call | solution.py:380
  93.9 5.5 %all-to-all-start = ((bf16[16,128,128]{2,1,0:T(8,128)(2,1)}), bf16[16,128,128]{2,1,0:T(8,128)(2,1)S(1)}, u32[]{:S(2)}, u32[]{:S(2)}) async-start(bf16[16,128,128]{2,1,0:T(8,128)(2,1)} %get-tuple-element.58), calls=%async_computation | async-start | bytes 1048576 | tf_op jit(solution)/shard_map/all_to_all | solution.py:405
  99.4 0.2 slice_reduce_fusion
  99.6 0.1 eq.64
  99.8 0.1 fusion.4
  99.9 0.1 reduce_sum.51
  100.0 0.1 copy.37
  100.1 0.1 fusion.1.select_ref
  100.3 16.3 %all-to-all-done.arrived_ref = bf16[16,128,128]{2,1,0:T(8,128)(2,1)S(1)} async-done(((bf16[16,128,128]{2,1,0:T(8,128)(2,1)}), bf16[16,128,128]{2,1,0:T(8,128)(2,1)S(1)}, u32[]{:S(2)}, u32[]{:S(2)}) %all-to-all-start) | async-done | bytes 524320 | tf_op jit(solution)/shard_map/all_to_all | solution.py:405
  116.6 0.2 place.1
  116.8 29.7 %all_to_all.25 = bf16[32,16,128]{2,1,0:T(8,128)(2,1)S(1)} all-to-all(bf16[32,16,128]{2,1,0:T(8,128)(2,1)S(1)} %bitcast.51), channel_id=1, replica_groups=mesh['sp'=32,'tp'=16] {'sp'}, dimensions={0} | all-to-all | bytes 262144 | tf_op jit(solution)/shard_map/all_to_all | solution.py:432
  146.5 0.1 broadcast_in_dim.24
  146.6 14.2 %all_to_all.26.rows_ref = bf16[16,128,128]{2,1,0:T(8,128)(2,1)S(1)} all-to-all(bf16[16,128,128]{2,1,0:T(8,128)(2,1)S(1)} %bitcast.55), channel_id=1, replica_groups=mesh['sp'=32,'tp'=16] {'tp'}, dimensions={0} | all-to-all | bytes 1048576 | tf_op jit(solution)/shard_map/all_to_all | solution.py:436
  160.8 3.7 %experts.1 = bf16[16,128,128]{2,1,0:T(8,128)(2,1)S(1)} custom-call(bf16[16,128,128]{2,1,0:T(8,128)(2,1)S(1)} %all_to_all.26.rows_ref, f32[1,2048]{1,0:T(1,128)S(1)} %bitcast.52, bf16[3072,256]{1,0:T(8,128)(2,1)S(1)} %collective-permute-done.20.refs_0_, bf16[3072,256]{1,0:T(8,128)(2,1)} %get-tuple-element.62.refs_1_, ...), custom_call_target="tpu_custom_call" | custom-call | flops 805306368 | tf_op jit(solution)/shard_map/experts/pallas_call | solution.py:443
  164.6 12.0 %all_to_all.27 = bf16[16,128,128]{2,1,0:T(8,128)(2,1)S(1)} all-to-all(bf16[16,128,128]{2,1,0:T(8,128)(2,1)S(1)} %experts.1), channel_id=1, replica_groups=mesh['sp'=32,'tp'=16] {'tp'}, dimensions={0} | all-to-all | bytes 1048576 | tf_op jit(solution)/shard_map/all_to_all | solution.py:272
  176.6 0.7 bitcast_reduce_fusion
  177.3 8.3 %all-to-all-start.4 = ((bf16[32,16,128]{2,1,0:T(8,128)(2,1)}), bf16[32,16,128]{2,1,0:T(8,128)(2,1)S(1)}, u32[]{:S(2)}, u32[]{:S(2)}) async-start(bf16[32,16,128]{2,1,0:T(8,128)(2,1)} %bitcast.28), calls=%async_computation.4 | async-start | bytes 262144 | tf_op jit(solution)/shard_map/all_to_all | solution.py:465
  185.6 0.1 select_reduce_fusion
  185.8 15.7 %all-to-all-done.4 = bf16[32,16,128]{2,1,0:T(8,128)(2,1)S(1)} async-done(((bf16[32,16,128]{2,1,0:T(8,128)(2,1)}), bf16[32,16,128]{2,1,0:T(8,128)(2,1)S(1)}, u32[]{:S(2)}, u32[]{:S(2)}) %all-to-all-start.4) | async-done | bytes 131104 | tf_op jit(solution)/shard_map/all_to_all | solution.py:465
  201.4 0.3 fusion.6
  201.7 0.6 add_convert_fusion
  (40 shorter events, 0.2 us)
Async XLA Ops:
  2.5 23.1 %collective-permute-start.18 = (bf16[3072,256]{1,0:T(8,128)(2,1)}, bf16[3072,256]{1,0:T(8,128)(2,1)}, u32[]{:S(2)}, u32[]{:S(2)}) collective-permute-start(bf16[3072,256]{1,0:T(8,128)(2,1)} %get-tuple-element.62.refs_1_), channel_id=1, source_target_pairs={{0,4},{1,5},{2,6},{3,7},{4,8},{5,9},{6,10},{7,11},{8,12},{9,13},{1... | collective-permute-start | bytes 4718600 | tf_op jit(solution)/shard_map/ppermute | solution.py:349
  8.0 6.5 %collective-permute-start = (bf16[128,1280]{1,0:T(8,128)(2,1)S(1)}, bf16[128,1280]{1,0:T(8,128)(2,1)S(1)}, u32[]{:S(2)}, u32[]{:S(2)}) collective-permute-start(bf16[128,1280]{1,0:T(8,128)(2,1)S(1)} %get-tuple-element.34.own_q_ref), channel_id=1, source_target_pairs={{0,16},{16,0},{32,48},{48,32},{64,80},{80,64},{96,112},{112,96},{1... | collective-permute-start | bytes 983048 | tf_op jit(solution)/shard_map/ppermute | solution.py:337
  13.2 3.9 %collective-permute-start.9 = (bf16[128,768]{1,0:T(8,128)(2,1)S(1)}, bf16[128,768]{1,0:T(8,128)(2,1)S(1)}, u32[]{:S(2)}, u32[]{:S(2)}) collective-permute-start(bf16[128,768]{1,0:T(8,128)(2,1)S(1)} %get-tuple-element.35.refs_0_), channel_id=1, source_target_pairs={{16,48},{48,80},{80,112},{112,144},{144,176},{176,208},{208,240},{... | collective-permute-start | bytes 589832 | tf_op jit(solution)/shard_map/ppermute | solution.py:359
  14.6 5.1 %collective-permute-start.1 = (bf16[128,768]{1,0:T(8,128)(2,1)S(1)}, bf16[128,768]{1,0:T(8,128)(2,1)S(1)}, u32[]{:S(2)}, u32[]{:S(2)}) collective-permute-start(bf16[128,768]{1,0:T(8,128)(2,1)S(1)} %slice.12), channel_id=1, source_target_pairs={{16,48},{48,80},{80,112},{112,144},{144,176},{176,208},{208,240},{... | collective-permute-start | bytes 589832 | tf_op jit(solution)/shard_map/ppermute | solution.py:360
  17.1 3.2 %collective-permute-start.10 = (bf16[128,768]{1,0:T(8,128)(2,1)S(1)}, bf16[128,768]{1,0:T(8,128)(2,1)S(1)}, u32[]{:S(2)}, u32[]{:S(2)}) collective-permute-start(bf16[128,768]{1,0:T(8,128)(2,1)S(1)} %collective-permute-done.9.refs_0_), channel_id=1, source_target_pairs={{48,80},{80,112},{112,144},{144,176},{176,208},{208,240},{240,272}... | collective-permute-start | bytes 589832 | tf_op jit(solution)/shard_map/ppermute | solution.py:359
  19.7 1.4 collective-permute-start.2
  20.3 10.3 %collective-permute-start.11 = (bf16[128,768]{1,0:T(8,128)(2,1)S(1)}, bf16[128,768]{1,0:T(8,128)(2,1)S(1)}, u32[]{:S(2)}, u32[]{:S(2)}) collective-permute-start(bf16[128,768]{1,0:T(8,128)(2,1)S(1)} %collective-permute-done.10.refs_0_), channel_id=1, source_target_pairs={{80,112},{112,144},{144,176},{176,208},{208,240},{240,272},{272,30... | collective-permute-start | bytes 589832 | tf_op jit(solution)/shard_map/ppermute | solution.py:359
  21.0 10.3 %collective-permute-start.3 = (bf16[128,768]{1,0:T(8,128)(2,1)S(1)}, bf16[128,768]{1,0:T(8,128)(2,1)S(1)}, u32[]{:S(2)}, u32[]{:S(2)}) collective-permute-start(bf16[128,768]{1,0:T(8,128)(2,1)S(1)} %collective-permute-done.2.refs_1_), channel_id=1, source_target_pairs={{80,112},{112,144},{144,176},{176,208},{208,240},{240,272},{272,30... | collective-permute-start | bytes 589832 | tf_op jit(solution)/shard_map/ppermute | solution.py:360
  25.7 63.6 %collective-permute-start.19 = (bf16[3072,256]{1,0:T(8,128)(2,1)}, bf16[3072,256]{1,0:T(8,128)(2,1)}, u32[]{:S(2)}, u32[]{:S(2)}) collective-permute-start(bf16[3072,256]{1,0:T(8,128)(2,1)} %collective-permute-done.18.refs_2_), channel_id=1, source_target_pairs={{0,4},{1,5},{2,6},{3,7},{4,8},{5,9},{6,10},{7,11},{8,12},{9,13},{1... | collective-permute-start | bytes 4718600 | tf_op jit(solution)/shard_map/ppermute | solution.py:349
  30.7 1.4 collective-permute-start.12
  31.4 1.4 collective-permute-start.4
  32.1 1.4 collective-permute-start.13
  32.8 1.4 collective-permute-start.5
  33.5 2.1 %collective-permute-start.14 = (bf16[128,768]{1,0:T(8,128)(2,1)S(1)}, bf16[128,768]{1,0:T(8,128)(2,1)S(1)}, u32[]{:S(2)}, u32[]{:S(2)}) collective-permute-start(bf16[128,768]{1,0:T(8,128)(2,1)S(1)} %collective-permute-done.13.refs_0_), channel_id=1, source_target_pairs={{176,208},{208,240},{240,272},{272,304},{304,336},{336,368},{368,4... | collective-permute-start | bytes 589832 | tf_op jit(solution)/shard_map/ppermute | solution.py:359
  34.2 2.7 %collective-permute-start.6 = (bf16[128,768]{1,0:T(8,128)(2,1)S(1)}, bf16[128,768]{1,0:T(8,128)(2,1)S(1)}, u32[]{:S(2)}, u32[]{:S(2)}) collective-permute-start(bf16[128,768]{1,0:T(8,128)(2,1)S(1)} %collective-permute-done.5.refs_1_), channel_id=1, source_target_pairs={{176,208},{208,240},{240,272},{272,304},{304,336},{336,368},{368,4... | collective-permute-start | bytes 589832 | tf_op jit(solution)/shard_map/ppermute | solution.py:360
  34.8 0.7 copy-start
  35.5 2.7 %collective-permute-start.15 = (bf16[128,768]{1,0:T(8,128)(2,1)S(1)}, bf16[128,768]{1,0:T(8,128)(2,1)}, u32[]{:S(2)}, u32[]{:S(2)}) collective-permute-start(bf16[128,768]{1,0:T(8,128)(2,1)S(1)} %collective-permute-done.14.refs_0_), channel_id=1, source_target_pairs={{208,240},{240,272},{272,304},{304,336},{336,368},{368,400},{400,4... | collective-permute-start | bytes 589832 | tf_op jit(solution)/shard_map/ppermute | solution.py:359
  36.9 2.0 %collective-permute-start.7 = (bf16[128,768]{1,0:T(8,128)(2,1)S(1)}, bf16[128,768]{1,0:T(8,128)(2,1)S(1)}, u32[]{:S(2)}, u32[]{:S(2)}) collective-permute-start(bf16[128,768]{1,0:T(8,128)(2,1)S(1)} %collective-permute-done.6.refs_1_), channel_id=1, source_target_pairs={{208,240},{240,272},{272,304},{304,336},{336,368},{368,400},{400,4... | collective-permute-start | bytes 589832 | tf_op jit(solution)/shard_map/ppermute | solution.py:360
  37.6 0.7 copy-start.2
  38.2 4.5 %collective-permute-start.16 = (bf16[128,768]{1,0:T(8,128)(2,1)}, bf16[128,768]{1,0:T(8,128)(2,1)S(1)}, u32[]{:S(2)}, u32[]{:S(2)}) collective-permute-start(bf16[128,768]{1,0:T(8,128)(2,1)} %collective-permute-done.15.refs_0_), channel_id=1, source_target_pairs={{240,272},{272,304},{304,336},{336,368},{368,400},{400,432},{432,4... | collective-permute-start | bytes 589832 | tf_op jit(solution)/shard_map/ppermute | solution.py:363
  38.9 3.9 %collective-permute-start.8 = (bf16[128,768]{1,0:T(8,128)(2,1)S(1)}, bf16[128,768]{1,0:T(8,128)(2,1)S(1)}, u32[]{:S(2)}, u32[]{:S(2)}) collective-permute-start(bf16[128,768]{1,0:T(8,128)(2,1)S(1)} %collective-permute-done.7.refs_1_), channel_id=1, source_target_pairs={{368,400},{400,432},{432,464},{464,496},{369,401},{401,433},{433,4... | collective-permute-start | bytes 589832 | tf_op jit(solution)/shard_map/ppermute | solution.py:364
  40.7 0.9 copy-start.1
  40.8 1.0 copy-start.3
  42.8 44.2 %copy-start.7 = (s32[128,2]{0,1:T(2,128)S(1)}, s32[128,2]{0,1:T(2,128)}, u32[]{:S(2)}) copy-start(s32[128,2]{0,1:T(2,128)} %param.33) | copy-start | bytes 3076
  42.9 48.8 %copy-start.5 = (f32[256]{0:T(256)S(1)}, f32[256]{0:T(256)}, u32[]{:S(2)}) copy-start(f32[256]{0:T(256)} %param.29) | copy-start | bytes 3076
  42.9 48.8 %copy-start.6 = (f32[128]{0:T(128)S(1)}, f32[128]{0:T(128)}, u32[]{:S(2)}) copy-start(f32[128]{0:T(128)} %param.28) | copy-start | bytes 1540
  43.0 48.7 %collective-permute-start.17 = (f32[776,128]{1,0:T(8,128)S(1)}, f32[776,128]{1,0:T(8,128)S(1)}, u32[]{:S(2)}, u32[]{:S(2)}) collective-permute-start(f32[776,128]{1,0:T(8,128)S(1)} %get-tuple-element.55), channel_id=1, source_target_pairs={{0,16},{16,0},{32,48},{48,32},{64,80},{80,64},{96,112},{112,96},{1... | collective-permute-start | bytes 1191944 | tf_op jit(solution)/shard_map/ppermute | solution.py:369
  89.3 71.5 %collective-permute-start.20 = (bf16[3072,256]{1,0:T(8,128)(2,1)}, bf16[3072,256]{1,0:T(8,128)(2,1)S(1)}, u32[]{:S(2)}, u32[]{:S(2)}) collective-permute-start(bf16[3072,256]{1,0:T(8,128)(2,1)} %collective-permute-done.19.refs_3_), channel_id=1, source_target_pairs={{0,4},{1,5},{2,6},{3,7},{4,8},{5,9},{6,10},{7,11},{8,12},{9,13},{1... | collective-permute-start | bytes 4718600 | tf_op jit(solution)/shard_map/ppermute | solution.py:349
  93.9 22.6 %all-to-all-start = ((bf16[16,128,128]{2,1,0:T(8,128)(2,1)}), bf16[16,128,128]{2,1,0:T(8,128)(2,1)S(1)}, u32[]{:S(2)}, u32[]{:S(2)}) async-start(bf16[16,128,128]{2,1,0:T(8,128)(2,1)} %get-tuple-element.58), calls=%async_computation | async-start | bytes 1048576 | tf_op jit(solution)/shard_map/all_to_all | solution.py:405
  99.4 61.4 %copy-start.4 = (f32[2048]{0:T(1024)S(1)}, f32[2048]{0:T(1024)}, u32[]{:S(2)}) copy-start(f32[2048]{0:T(1024)} %param.32) | copy-start | bytes 24580
  164.6 21.0 %copy-start.8 = (f32[128,2]{0,1:T(2,128)S(1)}, f32[128,2]{0,1:T(2,128)}, u32[]{:S(2)}) copy-start(f32[128,2]{0,1:T(2,128)} %param.34) | copy-start | bytes 3076
  177.3 24.1 %all-to-all-start.4 = ((bf16[32,16,128]{2,1,0:T(8,128)(2,1)}), bf16[32,16,128]{2,1,0:T(8,128)(2,1)S(1)}, u32[]{:S(2)}, u32[]{:S(2)}) async-start(bf16[32,16,128]{2,1,0:T(8,128)(2,1)} %bitcast.28), calls=%async_computation.4 | async-start | bytes 262144 | tf_op jit(solution)/shard_map/all_to_all | solution.py:465

commit v3 on v2

--- a/solution.py
+++ b/solution.py
@@ -5,6 +5,7 @@
 from jax import lax
 from jax.experimental import pallas as pl
 from jax.experimental.pallas import tpu as pltpu
+from jax.sharding import Mesh
 from jax.sharding import PartitionSpec as P
 
 
@@ -28,6 +29,7 @@
     (slice(384, 512), slice(384, 512), slice(512, 768), slice(512, 768), DK_B**-0.5),
 )
 SUMS = 768
+SEQ = ("z", "core")
 STATE = SUMS + 8
 
 
@@ -238,9 +240,16 @@
     copies = [pltpu.make_async_copy(a, b, sems.at[i]) for i, (a, b) in enumerate(zip(froms, bufs))]
     for copy in copies:
         copy.start()
-    parts, _, width = rows_ref.shape
+    parts, group_rows, width = rows_ref.shape
+    parts = parts // 2
     model_width = parts * width
-    rows = jnp.concatenate([rows_ref[i] for i in range(parts)], axis=1).astype(jnp.float32)
+    rows = jnp.concatenate(
+        [
+            jnp.concatenate([rows_ref[core * parts + i] for i in range(parts)], axis=1)
+            for core in range(2)
+        ],
+        axis=0,
+    ).astype(jnp.float32)
     mean_sq = jnp.sum(rows * rows, axis=1, keepdims=True) / model_width
     normed = (rows * lax.rsqrt(mean_sq + EPS) * gain_ref[...]).astype(jnp.bfloat16)
 
@@ -260,8 +269,11 @@
         down = dot(hidden[0], bufs[0][start : start + width, :])
         for i in range(1, LINE):
             down = down + dot(hidden[i], bufs[i][start : start + width, :])
-        out_ref[2 * j] = down[:, :width].astype(jnp.bfloat16)
-        out_ref[2 * j + 1] = down[:, width:].astype(jnp.bfloat16)
+        down = down.astype(jnp.bfloat16)
+        for core in range(2):
+            half = down[core * group_rows : (core + 1) * group_rows]
+            out_ref[core * parts + 2 * j] = half[:, :width]
+            out_ref[core * parts + 2 * j + 1] = half[:, width:]
 
 
 def held(value):
@@ -296,10 +308,10 @@
 ):
     tok_rows = residual.shape[0]
     model_width = residual.shape[1]
-    seq_devices = lax.axis_size("sp")
+    seq_devices = lax.axis_size("z") * lax.axis_size("core")
     head_devices = lax.axis_size("tp")
     head_index = lax.axis_index("tp")
-    seq_index = lax.axis_index("sp")
+    seq_index = lax.axis_index(SEQ)
     columns = model_width // head_devices
 
     chips = seq_devices // 2
@@ -334,7 +346,7 @@
         compiler_params=pltpu.CompilerParams(vmem_limit_bytes=8 << 20),
         name="pack",
     )(*[held(a) for a in fields + weights])
-    got_all = lax.ppermute(own_all, "sp", partner)
+    got_all = lax.ppermute(own_all, SEQ, partner)
     got_kv = got_all[:, 4 * DK_B :]
     queries = (own_all, got_all)
 
@@ -346,7 +358,7 @@
         for t in range(head_devices)
     ]
     for _ in range(1, LINE):
-        packed.append(lax.ppermute(packed[-1], ("sp", "tp"), along))
+        packed.append(lax.ppermute(packed[-1], (*SEQ, "tp"), along))
 
     segments = tok_rows // SEG
     later = jnp.where(core == 0, segments, -segments).astype(jnp.int32).reshape(1)
@@ -356,17 +368,17 @@
         source = jnp.where(core == 1, chip - step, chip + step) % chips
         seen = (source < chip).astype(jnp.int32).reshape(1)
         pairs = onward(step, range(chips), range(half_way - 1))
-        mine = lax.ppermute(mine, "sp", pairs)
-        theirs = lax.ppermute(theirs, "sp", pairs)
+        mine = lax.ppermute(mine, SEQ, pairs)
+        theirs = lax.ppermute(theirs, SEQ, pairs)
         state = absorbed(seen, queries, (mine, theirs), state)
     near = (chip >= half_way) & (chip < half_way + quarter)
-    mine = lax.ppermute(mine, "sp", onward(half_way, range(half_way), range(quarter)))
-    theirs = lax.ppermute(theirs, "sp", onward(half_way, range(quarter, half_way), ()))
+    mine = lax.ppermute(mine, SEQ, onward(half_way, range(half_way), range(quarter)))
+    theirs = lax.ppermute(theirs, SEQ, onward(half_way, range(quarter, half_way), ()))
     seen = jnp.where(core == 1, chip >= half_way, near).astype(jnp.int32).reshape(1)
     state = absorbed(seen, queries, (mine,), state)
     seen = ((core == 1) & (chip >= half_way + quarter)).astype(jnp.int32).reshape(1)
     state = absorbed(seen, queries, (theirs,), state)
-    got_state = lax.ppermute(state[1], "sp", partner)
+    got_state = lax.ppermute(state[1], SEQ, partner)
     projs = pl.pallas_call(
         fetch,
         out_shape=tuple(pltpu.VMEM(a.shape, jnp.bfloat16) for a in (proj_a, proj_b)),
@@ -428,21 +440,29 @@
         compiler_params=pltpu.CompilerParams(vmem_limit_bytes=4 << 20),
         name="place",
     )(arrived, residual_cols, select)
-    send_rows = send_rows.reshape(seq_devices, slot_count, columns)
-    routed = lax.all_to_all(send_rows, "sp", split_axis=0, concat_axis=0, tiled=True)
-    group_rows = seq_devices * slot_count // LINE
-    grouped = routed.reshape(LINE, 1, group_rows, columns)
-    copies = jnp.broadcast_to(grouped, (LINE, lines, group_rows, columns))
-    arrived = lax.all_to_all(
-        copies.reshape(head_devices, group_rows, columns),
-        "tp",
+    routed = lax.all_to_all(
+        send_rows.reshape(chips, 2 * slot_count, columns),
+        "z",
         split_axis=0,
         concat_axis=0,
         tiled=True,
     )
+    share = chips // LINE
+    group_rows = share * slot_count
+    grouped = routed.reshape(LINE, share, 2, slot_count, columns).transpose(2, 0, 1, 3, 4)
+    copies = jnp.broadcast_to(
+        grouped.reshape(2, LINE, 1, group_rows, columns), (2, LINE, lines, group_rows, columns)
+    )
+    arrived = lax.all_to_all(
+        copies.reshape(2 * head_devices, group_rows, columns),
+        ("core", "tp"),
+        split_axis=0,
+        concat_axis=0,
+        tiled=True,
+    )
     parts = pl.pallas_call(
         experts,
-        out_shape=jax.ShapeDtypeStruct((head_devices, group_rows, columns), jnp.bfloat16),
+        out_shape=jax.ShapeDtypeStruct((2 * head_devices, group_rows, columns), jnp.bfloat16),
         in_specs=[VMEM] * 3 + [HBM] * (LINE - 1),
         out_specs=VMEM,
         scratch_shapes=[
@@ -450,19 +470,20 @@
         ]
         + [pltpu.SemaphoreType.DMA((LINE - 1,))],
         cost_estimate=pl.CostEstimate(
-            flops=6 * group_rows * model_width * LINE * width, bytes_accessed=0, transcendentals=0
+            flops=12 * group_rows * model_width * LINE * width, bytes_accessed=0, transcendentals=0
         ),
         compiler_params=pltpu.CompilerParams(vmem_limit_bytes=24 << 20),
         name="experts",
     )(arrived, norm_gain[None, :], packed[-1], *[held(a) for a in packed[:-1]])
     results = (
-        summed_on_arrival(parts, "tp")
-        .reshape(LINE, lines, group_rows, columns)
-        .sum(axis=1)
+        summed_on_arrival(parts, ("core", "tp"))
+        .reshape(2, LINE, lines, share, slot_count, columns)
+        .sum(axis=2)
         .astype(jnp.bfloat16)
-        .reshape(seq_devices, slot_count, columns)
-    )
-    returned = lax.all_to_all(results, "sp", split_axis=0, concat_axis=0, tiled=True)
+        .transpose(1, 2, 0, 3, 4)
+        .reshape(chips, 2 * slot_count, columns)
+    )
+    returned = lax.all_to_all(results, "z", split_axis=0, concat_axis=0, tiled=True)
     returned_flat = returned.reshape(seq_devices * slot_count, columns).astype(jnp.float32)
     experts_sum = jnp.dot(combine, returned_flat, precision=lax.Precision.HIGHEST)
     return (stream_cols.astype(jnp.float32) + experts_sum).astype(jnp.bfloat16)
@@ -470,13 +491,13 @@
 
 def solution(mesh):
     placed = (
-        P("sp", None),
-        P("sp", "tp", None),
-        P("sp", "tp", None),
-        P("sp", "tp", None),
-        P("sp", "tp", None),
-        P("sp", "tp", None),
-        P("sp", "tp", None),
+        P(SEQ, None),
+        P(SEQ, "tp", None),
+        P(SEQ, "tp", None),
+        P(SEQ, "tp", None),
+        P(SEQ, "tp", None),
+        P(SEQ, "tp", None),
+        P(SEQ, "tp", None),
         P("tp"),
         P("tp"),
         P(),
@@ -484,12 +505,13 @@
         P("tp", None),
         P("tp", None),
         P(),
-        P("sp", None),
-        P("sp", None),
-        P("sp", None, "tp"),
-        P("sp", None, "tp"),
-        P("sp", "tp", None),
-    )
+        P(SEQ, None),
+        P(SEQ, None),
+        P(SEQ, None, "tp"),
+        P(SEQ, None, "tp"),
+        P(SEQ, "tp", None),
+    )
+    split = Mesh(mesh.devices.reshape(-1, 2, mesh.shape["tp"]), (*SEQ, "tp"))
     return jax.shard_map(
-        local, mesh=mesh, in_specs=placed, out_specs=P("sp", "tp"), check_vma=False
-    )
+        local, mesh=split, in_specs=placed, out_specs=P(SEQ, "tp"), check_vma=False
+    )

time: 203 us -> 200 us (0.985); the launches traced: 202 us -> 197 us
  starting transfers between devices: 88.4 us -> 83.8 us
  waiting for transfers between devices: 37.9 us -> 34 us
  blocking collectives: 55.9 us -> 59.1 us
    all_to_all x1, starting transfers between devices: 8.29 us -> 3.68 us  [local(): lax.all_to_all(results, 'z', split_axis=0, concat_axis=0, tiled=True)]
    all_to_all x1, waiting for transfers between devices: 15.7 us -> 11.8 us  [local(): lax.all_to_all(results, 'z', split_axis=0, concat_axis=0, tiled=True)]
    all_to_all x1, blocking collectives: 12 us -> 15.1 us  [summed_on_arrival(): lax.all_to_all(pieces, axis, split_axis=0, concat_axis=0, tiled=True)]
where the time goes in v3:
time: 200 us; the launch traced here: 197 us
  starting transfers between devices  83.8 us (42%)
  blocking collectives  59.1 us (30%)
  waiting for transfers between devices  34 us (17%)
  Pallas kernels  12.3 us (6%)
  local copies, waits for them, and re-layouts  3.78 us (2%)
  between operations  2.04 us (1%)
    ppermute x1, starting transfers between devices, local(): got_state = lax.ppermute(state[1], SEQ, partner)  42.7 us
    all_to_all x1, blocking collectives, local(): lax.all_to_all(send_rows.reshape(chips, 2 * slot_count, columns), 'z', sp...  23.4 us
    all_to_all x1, blocking collectives, local(): lax.all_to_all(copies.reshape(2 * head_devices, group_rows, columns), ('c...  20.6 us
    all_to_all x1, waiting for transfers between devices, local(): lax.all_to_all(pieces, 'tp', split_axis=0, concat_axis=0, tiled=True)  16.3 us
    all_to_all x1, blocking collectives, summed_on_arrival(): lax.all_to_all(pieces, axis, split_axis=0, concat_axis=0, tiled=True)  15.1 us
    ppermute x3, starting transfers between devices, local(): packed.append(lax.ppermute(packed[-1], (*SEQ, 'tp'), along))  12.8 us
    all_to_all x1, waiting for transfers between devices, local(): lax.all_to_all(results, 'z', split_axis=0, concat_axis=0, tiled=True)  11.8 us
    ppermute x7, starting transfers between devices, local(): theirs = lax.ppermute(theirs, SEQ, pairs)  6.53 us
  transfers between devices with their start and end apart: 23, of which 4 were waited for; matrix products, arithmetic and copies ran while one was open for 1% of the time, Pallas kernels for 3%

profile of v3, /device:TPU:1, one launch (start us, length us, event | category | flops | bytes accessed | tf_op | source)
XLA Modules:
  0.0 197.0 jit_solution(11177930408192541292)
XLA Ops:
  0.0 2.5 %pack.1 = (bf16[128,1280]{1,0:T(8,128)(2,1)S(1)}, bf16[128,768]{1,0:T(8,128)(2,1)S(1)}, bf16[3072,256]{1,0:T(8,128)(2,1)}) custom-call(bf16[128,128]{1,0:T(8,128)(2,1)} %bitcast.70, bf16[128,256]{1,0:T(8,128)(2,1)} %bitcast.67, bf16[128,128]{1,0:T(8,128)(2,1)} %bitcast.71, bf16[128,128]{1,0:T(8,128)(2,1)} %bitcast.72, bf16[128,256]{1,0:T(8,128)(2,1)} %bitcast.68, ...), custom_call_target="tpu_custom_call" | custom-call | tf_op jit(solution)/shard_map/pack/pallas_call | solution.py:332
  2.5 5.5 %collective-permute-start.18 = (bf16[3072,256]{1,0:T(8,128)(2,1)}, bf16[3072,256]{1,0:T(8,128)(2,1)}, u32[]{:S(2)}, u32[]{:S(2)}) collective-permute-start(bf16[3072,256]{1,0:T(8,128)(2,1)} %get-tuple-element.62.refs_1_), channel_id=1, source_target_pairs={{0,4},{1,5},{2,6},{3,7},{4,8},{5,9},{6,10},{7,11},{8,12},{9,13},{1... | collective-permute-start | bytes 4718600 | tf_op jit(solution)/shard_map/ppermute | solution.py:361
  8.0 5.2 %collective-permute-start = (bf16[128,1280]{1,0:T(8,128)(2,1)S(1)}, bf16[128,1280]{1,0:T(8,128)(2,1)S(1)}, u32[]{:S(2)}, u32[]{:S(2)}) collective-permute-start(bf16[128,1280]{1,0:T(8,128)(2,1)S(1)} %get-tuple-element.34.own_q_ref), channel_id=1, source_target_pairs={{0,16},{16,0},{32,48},{48,32},{64,80},{80,64},{96,112},{112,96},{1... | collective-permute-start | bytes 983048 | tf_op jit(solution)/shard_map/ppermute | solution.py:349
  13.2 1.3 collective-permute-start.9
  14.6 2.5 %collective-permute-start.1 = (bf16[128,768]{1,0:T(8,128)(2,1)S(1)}, bf16[128,768]{1,0:T(8,128)(2,1)S(1)}, u32[]{:S(2)}, u32[]{:S(2)}) collective-permute-start(bf16[128,768]{1,0:T(8,128)(2,1)S(1)} %slice.12), channel_id=1, source_target_pairs={{16,48},{48,80},{80,112},{112,144},{144,176},{176,208},{208,240},{... | collective-permute-start | bytes 589832 | tf_op jit(solution)/shard_map/ppermute | solution.py:372
  17.1 0.7 collective-permute-start.10
  17.8 1.9 collective-permute-done.1.refs_1_
  19.7 0.7 collective-permute-start.2
  20.3 0.7 collective-permute-start.11
  21.0 0.7 collective-permute-start.3
  21.7 3.9 %collective-permute-done.18.refs_2_ = bf16[3072,256]{1,0:T(8,128)(2,1)} collective-permute-done((bf16[3072,256]{1,0:T(8,128)(2,1)}, bf16[3072,256]{1,0:T(8,128)(2,1)}, u32[]{:S(2)}, u32[]{:S(2)}) %collective-permute-start.18) | collective-permute-done | bytes 1572896 | tf_op jit(solution)/shard_map/ppermute | solution.py:361
  25.7 5.0 %collective-permute-start.19 = (bf16[3072,256]{1,0:T(8,128)(2,1)}, bf16[3072,256]{1,0:T(8,128)(2,1)}, u32[]{:S(2)}, u32[]{:S(2)}) collective-permute-start(bf16[3072,256]{1,0:T(8,128)(2,1)} %collective-permute-done.18.refs_2_), channel_id=1, source_target_pairs={{0,4},{1,5},{2,6},{3,7},{4,8},{5,9},{6,10},{7,11},{8,12},{9,13},{1... | collective-permute-start | bytes 4718600 | tf_op jit(solution)/shard_map/ppermute | solution.py:361
  30.7 0.7 collective-permute-start.12
  31.4 0.7 collective-permute-start.4
  32.1 0.7 collective-permute-start.13
  32.8 0.7 collective-permute-start.5
  33.5 0.7 collective-permute-start.14
  34.2 0.7 collective-permute-start.6
  34.8 0.7 copy-done
  35.5 1.4 collective-permute-start.15
  36.9 0.7 collective-permute-start.7
  37.6 0.7 copy-done.2
  38.2 0.7 collective-permute-start.16
  38.9 0.7 collective-permute-start.8
  39.8 0.7 absorb.10
  40.5 0.1 absorb.11
  40.6 0.1 absorb.12
  40.7 0.1 absorb.13
  40.8 0.1 absorb.14
  40.8 0.8 copy-done.1
  41.6 0.1 absorb.15
  41.7 0.1 copy-done.3
  41.8 1.0 absorb.17
  42.8 0.1 absorb.18
  42.9 0.1 absorb.19
  43.0 42.7 %collective-permute-start.17 = (f32[776,128]{1,0:T(8,128)S(1)}, f32[776,128]{1,0:T(8,128)S(1)}, u32[]{:S(2)}, u32[]{:S(2)}) collective-permute-start(f32[776,128]{1,0:T(8,128)S(1)} %get-tuple-element.55), channel_id=1, source_target_pairs={{0,16},{16,0},{32,48},{48,32},{64,80},{80,64},{96,112},{112,96},{1... | collective-permute-start | bytes 1191944 | tf_op jit(solution)/shard_map/ppermute | solution.py:381
  86.9 0.1 copy.46
  87.1 0.1 eq.68
  87.2 0.6 reduce-window.6
  87.8 1.4 fetch.1
  89.2 0.1 pad_maximum_fusion.mix_ref
  89.3 2.4 %collective-permute-start.20 = (bf16[3072,256]{1,0:T(8,128)(2,1)}, bf16[3072,256]{1,0:T(8,128)(2,1)S(1)}, u32[]{:S(2)}, u32[]{:S(2)}) collective-permute-start(bf16[3072,256]{1,0:T(8,128)(2,1)} %collective-permute-done.19.refs_3_), channel_id=1, source_target_pairs={{0,4},{1,5},{2,6},{3,7},{4,8},{5,9},{6,10},{7,11},{8,12},{9,13},{1... | collective-permute-start | bytes 4718600 | tf_op jit(solution)/shard_map/ppermute | solution.py:361
  91.7 2.2 %finish.1 = (bf16[16,128,128]{2,1,0:T(8,128)(2,1)}, bf16[128,128]{1,0:T(8,128)(2,1)S(1)}) custom-call(f32[2]{0:T(128)S(1)} %pad_maximum_fusion.mix_ref, s32[1]{0:T(128)} %bitcast.at_ref, f32[776,128]{1,0:T(8,128)S(1)} %get-tuple-element.54.own_ref, f32[776,128]{1,0:T(8,128)S(1)} %collective-permute-done.17.got_ref, f32[1,128]{1,0:T(1,128)S(1)} %bitcast.57, ...), custom_call_target="tpu_custom_call" | custom-call | flops 201326592 | tf_op jit(solution)/shard_map/finish/pallas_call | solution.py:392
  93.9 5.5 %all-to-all-start = ((bf16[16,128,128]{2,1,0:T(8,128)(2,1)}), bf16[16,128,128]{2,1,0:T(8,128)(2,1)S(1)}, u32[]{:S(2)}, u32[]{:S(2)}) async-start(bf16[16,128,128]{2,1,0:T(8,128)(2,1)} %get-tuple-element.58), calls=%async_computation | async-start | bytes 1048576 | tf_op jit(solution)/shard_map/all_to_all | solution.py:417
  99.4 0.2 slice_reduce_fusion
  99.6 0.1 eq.64
  99.8 0.1 fusion.4
  99.9 0.1 reduce_sum.51
  100.1 0.1 copy.49
  100.1 0.1 fusion.1.select_ref
  100.3 16.3 %all-to-all-done.arrived_ref = bf16[16,128,128]{2,1,0:T(8,128)(2,1)S(1)} async-done(((bf16[16,128,128]{2,1,0:T(8,128)(2,1)}), bf16[16,128,128]{2,1,0:T(8,128)(2,1)S(1)}, u32[]{:S(2)}, u32[]{:S(2)}) %all-to-all-start) | async-done | bytes 524320 | tf_op jit(solution)/shard_map/all_to_all | solution.py:417
  116.6 0.2 place.1
  116.8 23.4 %all_to_all.25 = bf16[16,32,128]{2,1,0:T(8,128)(2,1)S(1)} all-to-all(bf16[16,32,128]{2,1,0:T(8,128)(2,1)S(1)} %bitcast.54), channel_id=1, replica_groups=mesh['z'=16,'core'=2,'tp'=16] {'z'}, dimensions={0} | all-to-all | bytes 262144 | tf_op jit(solution)/shard_map/all_to_all | solution.py:443
  140.2 0.1 broadcast_in_dim.24
  140.3 20.6 %all_to_all.26.rows_ref = bf16[32,64,128]{2,1,0:T(8,128)(2,1)S(1)} all-to-all(bf16[32,64,128]{2,1,0:T(8,128)(2,1)S(1)} %bitcast.58), channel_id=1, replica_groups=mesh['z'=16,'core'=2,'tp'=16] {'core','tp'}, dimensions={0} | all-to-all | bytes 1048576 | tf_op jit(solution)/shard_map/all_to_all | solution.py:456
  161.0 3.7 %experts.1 = bf16[32,64,128]{2,1,0:T(8,128)(2,1)S(1)} custom-call(bf16[32,64,128]{2,1,0:T(8,128)(2,1)S(1)} %all_to_all.26.rows_ref, f32[1,2048]{1,0:T(1,128)S(1)} %bitcast.55, bf16[3072,256]{1,0:T(8,128)(2,1)S(1)} %collective-permute-done.20.refs_0_, bf16[3072,256]{1,0:T(8,128)(2,1)} %get-tuple-element.62.refs_1_, ...), custom_call_target="tpu_custom_call" | custom-call | flops 805306368 | tf_op jit(solution)/shard_map/experts/pallas_call | solution.py:463
  164.7 15.1 %all_to_all.27 = bf16[32,64,128]{2,1,0:T(8,128)(2,1)S(1)} all-to-all(bf16[32,64,128]{2,1,0:T(8,128)(2,1)S(1)} %experts.1), channel_id=1, replica_groups=mesh['z'=16,'core'=2,'tp'=16] {'core','tp'}, dimensions={0} | all-to-all | bytes 1048576 | tf_op jit(solution)/shard_map/all_to_all | solution.py:284
  179.8 0.1 reduce.1
  179.8 0.7 copy.51
  180.5 3.7 %all-to-all-start.4 = ((bf16[16,32,128]{2,1,0:T(8,128)(2,1)}), bf16[16,32,128]{2,1,0:T(8,128)(2,1)S(1)}, u32[]{:S(2)}, u32[]{:S(2)}) async-start(bf16[16,32,128]{2,1,0:T(8,128)(2,1)} %bitcast.31), calls=%async_computation.4 | async-start | bytes 262144 | tf_op jit(solution)/shard_map/all_to_all | solution.py:486
  184.2 0.1 select_reduce_fusion
  184.4 11.8 %all-to-all-done.4 = bf16[16,32,128]{2,1,0:T(8,128)(2,1)S(1)} async-done(((bf16[16,32,128]{2,1,0:T(8,128)(2,1)}), bf16[16,32,128]{2,1,0:T(8,128)(2,1)S(1)}, u32[]{:S(2)}, u32[]{:S(2)}) %all-to-all-start.4) | async-done | bytes 131104 | tf_op jit(solution)/shard_map/all_to_all | solution.py:486
  196.1 0.3 fusion.6
  196.4 0.6 add_convert_fusion
  (42 shorter events, 0.3 us)
Async XLA Ops:
  2.5 23.1 %collective-permute-start.18 = (bf16[3072,256]{1,0:T(8,128)(2,1)}, bf16[3072,256]{1,0:T(8,128)(2,1)}, u32[]{:S(2)}, u32[]{:S(2)}) collective-permute-start(bf16[3072,256]{1,0:T(8,128)(2,1)} %get-tuple-element.62.refs_1_), channel_id=1, source_target_pairs={{0,4},{1,5},{2,6},{3,7},{4,8},{5,9},{6,10},{7,11},{8,12},{9,13},{1... | collective-permute-start | bytes 4718600 | tf_op jit(solution)/shard_map/ppermute | solution.py:361
  8.0 6.5 %collective-permute-start = (bf16[128,1280]{1,0:T(8,128)(2,1)S(1)}, bf16[128,1280]{1,0:T(8,128)(2,1)S(1)}, u32[]{:S(2)}, u32[]{:S(2)}) collective-permute-start(bf16[128,1280]{1,0:T(8,128)(2,1)S(1)} %get-tuple-element.34.own_q_ref), channel_id=1, source_target_pairs={{0,16},{16,0},{32,48},{48,32},{64,80},{80,64},{96,112},{112,96},{1... | collective-permute-start | bytes 983048 | tf_op jit(solution)/shard_map/ppermute | solution.py:349
  13.2 3.9 %collective-permute-start.9 = (bf16[128,768]{1,0:T(8,128)(2,1)S(1)}, bf16[128,768]{1,0:T(8,128)(2,1)S(1)}, u32[]{:S(2)}, u32[]{:S(2)}) collective-permute-start(bf16[128,768]{1,0:T(8,128)(2,1)S(1)} %get-tuple-element.35.refs_0_), channel_id=1, source_target_pairs={{16,48},{48,80},{80,112},{112,144},{144,176},{176,208},{208,240},{... | collective-permute-start | bytes 589832 | tf_op jit(solution)/shard_map/ppermute | solution.py:371
  14.6 5.1 %collective-permute-start.1 = (bf16[128,768]{1,0:T(8,128)(2,1)S(1)}, bf16[128,768]{1,0:T(8,128)(2,1)S(1)}, u32[]{:S(2)}, u32[]{:S(2)}) collective-permute-start(bf16[128,768]{1,0:T(8,128)(2,1)S(1)} %slice.12), channel_id=1, source_target_pairs={{16,48},{48,80},{80,112},{112,144},{144,176},{176,208},{208,240},{... | collective-permute-start | bytes 589832 | tf_op jit(solution)/shard_map/ppermute | solution.py:372
  17.1 3.2 %collective-permute-start.10 = (bf16[128,768]{1,0:T(8,128)(2,1)S(1)}, bf16[128,768]{1,0:T(8,128)(2,1)S(1)}, u32[]{:S(2)}, u32[]{:S(2)}) collective-permute-start(bf16[128,768]{1,0:T(8,128)(2,1)S(1)} %collective-permute-done.9.refs_0_), channel_id=1, source_target_pairs={{48,80},{80,112},{112,144},{144,176},{176,208},{208,240},{240,272}... | collective-permute-start | bytes 589832 | tf_op jit(solution)/shard_map/ppermute | solution.py:371
  19.7 1.4 collective-permute-start.2
  20.3 10.3 %collective-permute-start.11 = (bf16[128,768]{1,0:T(8,128)(2,1)S(1)}, bf16[128,768]{1,0:T(8,128)(2,1)S(1)}, u32[]{:S(2)}, u32[]{:S(2)}) collective-permute-start(bf16[128,768]{1,0:T(8,128)(2,1)S(1)} %collective-permute-done.10.refs_0_), channel_id=1, source_target_pairs={{80,112},{112,144},{144,176},{176,208},{208,240},{240,272},{272,30... | collective-permute-start | bytes 589832 | tf_op jit(solution)/shard_map/ppermute | solution.py:371
  21.0 10.3 %collective-permute-start.3 = (bf16[128,768]{1,0:T(8,128)(2,1)S(1)}, bf16[128,768]{1,0:T(8,128)(2,1)S(1)}, u32[]{:S(2)}, u32[]{:S(2)}) collective-permute-start(bf16[128,768]{1,0:T(8,128)(2,1)S(1)} %collective-permute-done.2.refs_1_), channel_id=1, source_target_pairs={{80,112},{112,144},{144,176},{176,208},{208,240},{240,272},{272,30... | collective-permute-start | bytes 589832 | tf_op jit(solution)/shard_map/ppermute | solution.py:372
  25.7 63.6 %collective-permute-start.19 = (bf16[3072,256]{1,0:T(8,128)(2,1)}, bf16[3072,256]{1,0:T(8,128)(2,1)}, u32[]{:S(2)}, u32[]{:S(2)}) collective-permute-start(bf16[3072,256]{1,0:T(8,128)(2,1)} %collective-permute-done.18.refs_2_), channel_id=1, source_target_pairs={{0,4},{1,5},{2,6},{3,7},{4,8},{5,9},{6,10},{7,11},{8,12},{9,13},{1... | collective-permute-start | bytes 4718600 | tf_op jit(solution)/shard_map/ppermute | solution.py:361
  30.7 1.4 collective-permute-start.12
  31.4 1.4 collective-permute-start.4
  32.1 1.4 collective-permute-start.13
  32.8 1.4 collective-permute-start.5
  33.5 2.1 %collective-permute-start.14 = (bf16[128,768]{1,0:T(8,128)(2,1)S(1)}, bf16[128,768]{1,0:T(8,128)(2,1)S(1)}, u32[]{:S(2)}, u32[]{:S(2)}) collective-permute-start(bf16[128,768]{1,0:T(8,128)(2,1)S(1)} %collective-permute-done.13.refs_0_), channel_id=1, source_target_pairs={{176,208},{208,240},{240,272},{272,304},{304,336},{336,368},{368,4... | collective-permute-start | bytes 589832 | tf_op jit(solution)/shard_map/ppermute | solution.py:371
  34.2 2.7 %collective-permute-start.6 = (bf16[128,768]{1,0:T(8,128)(2,1)S(1)}, bf16[128,768]{1,0:T(8,128)(2,1)S(1)}, u32[]{:S(2)}, u32[]{:S(2)}) collective-permute-start(bf16[128,768]{1,0:T(8,128)(2,1)S(1)} %collective-permute-done.5.refs_1_), channel_id=1, source_target_pairs={{176,208},{208,240},{240,272},{272,304},{304,336},{336,368},{368,4... | collective-permute-start | bytes 589832 | tf_op jit(solution)/shard_map/ppermute | solution.py:372
  34.8 0.7 copy-start
  35.5 2.7 %collective-permute-start.15 = (bf16[128,768]{1,0:T(8,128)(2,1)S(1)}, bf16[128,768]{1,0:T(8,128)(2,1)}, u32[]{:S(2)}, u32[]{:S(2)}) collective-permute-start(bf16[128,768]{1,0:T(8,128)(2,1)S(1)} %collective-permute-done.14.refs_0_), channel_id=1, source_target_pairs={{208,240},{240,272},{272,304},{304,336},{336,368},{368,400},{400,4... | collective-permute-start | bytes 589832 | tf_op jit(solution)/shard_map/ppermute | solution.py:371
  36.9 2.0 %collective-permute-start.7 = (bf16[128,768]{1,0:T(8,128)(2,1)S(1)}, bf16[128,768]{1,0:T(8,128)(2,1)S(1)}, u32[]{:S(2)}, u32[]{:S(2)}) collective-permute-start(bf16[128,768]{1,0:T(8,128)(2,1)S(1)} %collective-permute-done.6.refs_1_), channel_id=1, source_target_pairs={{208,240},{240,272},{272,304},{304,336},{336,368},{368,400},{400,4... | collective-permute-start | bytes 589832 | tf_op jit(solution)/shard_map/ppermute | solution.py:372
  37.6 0.7 copy-start.2
  38.2 4.5 %collective-permute-start.16 = (bf16[128,768]{1,0:T(8,128)(2,1)}, bf16[128,768]{1,0:T(8,128)(2,1)S(1)}, u32[]{:S(2)}, u32[]{:S(2)}) collective-permute-start(bf16[128,768]{1,0:T(8,128)(2,1)} %collective-permute-done.15.refs_0_), channel_id=1, source_target_pairs={{240,272},{272,304},{304,336},{336,368},{368,400},{400,432},{432,4... | collective-permute-start | bytes 589832 | tf_op jit(solution)/shard_map/ppermute | solution.py:375
  38.9 3.9 %collective-permute-start.8 = (bf16[128,768]{1,0:T(8,128)(2,1)S(1)}, bf16[128,768]{1,0:T(8,128)(2,1)S(1)}, u32[]{:S(2)}, u32[]{:S(2)}) collective-permute-start(bf16[128,768]{1,0:T(8,128)(2,1)S(1)} %collective-permute-done.7.refs_1_), channel_id=1, source_target_pairs={{368,400},{400,432},{432,464},{464,496},{369,401},{401,433},{433,4... | collective-permute-start | bytes 589832 | tf_op jit(solution)/shard_map/ppermute | solution.py:376
  40.7 0.9 copy-start.1
  40.8 1.0 copy-start.3
  42.8 44.2 %copy-start.7 = (s32[128,2]{0,1:T(2,128)S(1)}, s32[128,2]{0,1:T(2,128)}, u32[]{:S(2)}) copy-start(s32[128,2]{0,1:T(2,128)} %param.33) | copy-start | bytes 3076
  42.9 48.8 %copy-start.5 = (f32[256]{0:T(256)S(1)}, f32[256]{0:T(256)}, u32[]{:S(2)}) copy-start(f32[256]{0:T(256)} %param.29) | copy-start | bytes 3076
  42.9 48.8 %copy-start.6 = (f32[128]{0:T(128)S(1)}, f32[128]{0:T(128)}, u32[]{:S(2)}) copy-start(f32[128]{0:T(128)} %param.28) | copy-start | bytes 1540
  43.0 48.7 %collective-permute-start.17 = (f32[776,128]{1,0:T(8,128)S(1)}, f32[776,128]{1,0:T(8,128)S(1)}, u32[]{:S(2)}, u32[]{:S(2)}) collective-permute-start(f32[776,128]{1,0:T(8,128)S(1)} %get-tuple-element.55), channel_id=1, source_target_pairs={{0,16},{16,0},{32,48},{48,32},{64,80},{80,64},{96,112},{112,96},{1... | collective-permute-start | bytes 1191944 | tf_op jit(solution)/shard_map/ppermute | solution.py:381
  89.3 71.7 %collective-permute-start.20 = (bf16[3072,256]{1,0:T(8,128)(2,1)}, bf16[3072,256]{1,0:T(8,128)(2,1)S(1)}, u32[]{:S(2)}, u32[]{:S(2)}) collective-permute-start(bf16[3072,256]{1,0:T(8,128)(2,1)} %collective-permute-done.19.refs_3_), channel_id=1, source_target_pairs={{0,4},{1,5},{2,6},{3,7},{4,8},{5,9},{6,10},{7,11},{8,12},{9,13},{1... | collective-permute-start | bytes 4718600 | tf_op jit(solution)/shard_map/ppermute | solution.py:361
  93.9 22.6 %all-to-all-start = ((bf16[16,128,128]{2,1,0:T(8,128)(2,1)}), bf16[16,128,128]{2,1,0:T(8,128)(2,1)S(1)}, u32[]{:S(2)}, u32[]{:S(2)}) async-start(bf16[16,128,128]{2,1,0:T(8,128)(2,1)} %get-tuple-element.58), calls=%async_computation | async-start | bytes 1048576 | tf_op jit(solution)/shard_map/all_to_all | solution.py:417
  100.0 60.9 %copy-start.4 = (f32[2048]{0:T(1024)S(1)}, f32[2048]{0:T(1024)}, u32[]{:S(2)}) copy-start(f32[2048]{0:T(1024)} %param.32) | copy-start | bytes 24580
  164.7 19.5 %copy-start.8 = (f32[128,2]{0,1:T(2,128)S(1)}, f32[128,2]{0,1:T(2,128)}, u32[]{:S(2)}) copy-start(f32[128,2]{0,1:T(2,128)} %param.34) | copy-start | bytes 3076
  180.5 15.6 %all-to-all-start.4 = ((bf16[16,32,128]{2,1,0:T(8,128)(2,1)}), bf16[16,32,128]{2,1,0:T(8,128)(2,1)S(1)}, u32[]{:S(2)}, u32[]{:S(2)}) async-start(bf16[16,32,128]{2,1,0:T(8,128)(2,1)} %bitcast.31), calls=%async_computation.4 | async-start | bytes 262144 | tf_op jit(solution)/shard_map/all_to_all | solution.py:486

commit v4 on v3

--- a/solution.py
+++ b/solution.py
@@ -264,11 +264,13 @@
         both = dot(normed, ref[:model_width, :])
         gate, up = both[:, :width], both[:, width:]
         hidden.append((gate / (1.0 + jnp.exp(-gate)) * up).astype(jnp.bfloat16))
+    pairs = [jnp.concatenate(hidden[i : i + 2], axis=1) for i in range(0, LINE, 2)]
     for j in range(parts // 2):
         start = model_width + j * width
-        down = dot(hidden[0], bufs[0][start : start + width, :])
-        for i in range(1, LINE):
-            down = down + dot(hidden[i], bufs[i][start : start + width, :])
+        down = jnp.zeros((2 * group_rows, 2 * width), jnp.float32)
+        for i in range(0, LINE, 2):
+            both = [ref[start : start + width, :] for ref in bufs[i : i + 2]]
+            down = down + dot(pairs[i // 2], jnp.concatenate(both, axis=0))
         down = down.astype(jnp.bfloat16)
         for core in range(2):
             half = down[core * group_rows : (core + 1) * group_rows]
@@ -348,7 +350,7 @@
     )(*[held(a) for a in fields + weights])
     got_all = lax.ppermute(own_all, SEQ, partner)
     got_kv = got_all[:, 4 * DK_B :]
-    queries = (own_all, got_all)
+    queries = (own_all[:, : 4 * DK_B], got_all[:, : 4 * DK_B])
 
     lines = head_devices // LINE
     packed = [packed]

time: 200 us -> 200 us (level)
    unnamed x19 -> x15, local copies, waits for them, and re-layouts: 2.33 us -> 0.15 us
  transfers between devices with their start and end apart: 23 -> 23, of which waited for: 4 -> 4; matrix products, arithmetic and copies ran while one was open for 1% -> 2% of each run, Pallas kernels for 3% -> 3%
where the time goes in v4:
time: 200 us; the launch traced here: 198 us
  starting transfers between devices  85.1 us (43%)
  blocking collectives  59.6 us (30%)
  waiting for transfers between devices  34 us (17%)
  Pallas kernels  11.3 us (6%)
  local copies, waits for them, and re-layouts  3.44 us (2%)
  between operations  2.11 us (1%)
    ppermute x1, starting transfers between devices, local(): got_state = lax.ppermute(state[1], SEQ, partner)  44.7 us
    all_to_all x1, blocking collectives, local(): lax.all_to_all(send_rows.reshape(chips, 2 * slot_count, columns), 'z', sp...  24.1 us
    all_to_all x1, blocking collectives, local(): lax.all_to_all(copies.reshape(2 * head_devices, group_rows, columns), ('c...  20.4 us
    all_to_all x1, waiting for transfers between devices, local(): lax.all_to_all(pieces, 'tp', split_axis=0, concat_axis=0, tiled=True)  16.3 us
    all_to_all x1, blocking collectives, summed_on_arrival(): lax.all_to_all(pieces, axis, split_axis=0, concat_axis=0, tiled=True)  15.1 us
    ppermute x3, starting transfers between devices, local(): packed.append(lax.ppermute(packed[-1], (*SEQ, 'tp'), along))  12.8 us
    all_to_all x1, waiting for transfers between devices, local(): lax.all_to_all(results, 'z', split_axis=0, concat_axis=0, tiled=True)  11.8 us
    ppermute x7, starting transfers between devices, local(): theirs = lax.ppermute(theirs, SEQ, pairs)  6.54 us
  transfers between devices with their start and end apart: 23, of which 4 were waited for; matrix products, arithmetic and copies ran while one was open for 2% of the time, Pallas kernels for 3%

profile of v4, /device:TPU:1, one launch (start us, length us, event | category | flops | bytes accessed | tf_op | source)
XLA Modules:
  0.0 197.6 jit_solution(2543871391191211680)
XLA Ops:
  0.0 2.5 %pack.1 = (bf16[128,1280]{1,0:T(8,128)(2,1)S(1)}, bf16[128,768]{1,0:T(8,128)(2,1)S(1)}, bf16[3072,256]{1,0:T(8,128)(2,1)}) custom-call(bf16[128,128]{1,0:T(8,128)(2,1)} %bitcast.70, bf16[128,256]{1,0:T(8,128)(2,1)} %bitcast.67, bf16[128,128]{1,0:T(8,128)(2,1)} %bitcast.71, bf16[128,128]{1,0:T(8,128)(2,1)} %bitcast.72, bf16[128,256]{1,0:T(8,128)(2,1)} %bitcast.68, ...), custom_call_target="tpu_custom_call" | custom-call | tf_op jit(solution)/shard_map/pack/pallas_call | solution.py:334
  2.5 5.5 %collective-permute-start.18 = (bf16[3072,256]{1,0:T(8,128)(2,1)}, bf16[3072,256]{1,0:T(8,128)(2,1)}, u32[]{:S(2)}, u32[]{:S(2)}) collective-permute-start(bf16[3072,256]{1,0:T(8,128)(2,1)} %get-tuple-element.62.refs_1_), channel_id=1, source_target_pairs={{0,4},{1,5},{2,6},{3,7},{4,8},{5,9},{6,10},{7,11},{8,12},{9,13},{1... | collective-permute-start | bytes 4718600 | tf_op jit(solution)/shard_map/ppermute | solution.py:363
  8.0 5.2 %collective-permute-start = (bf16[128,1280]{1,0:T(8,128)(2,1)S(1)}, bf16[128,1280]{1,0:T(8,128)(2,1)S(1)}, u32[]{:S(2)}, u32[]{:S(2)}) collective-permute-start(bf16[128,1280]{1,0:T(8,128)(2,1)S(1)} %get-tuple-element.34), channel_id=1, source_target_pairs={{0,16},{16,0},{32,48},{48,32},{64,80},{80,64},{96,112},{112,96},{1... | collective-permute-start | bytes 983048 | tf_op jit(solution)/shard_map/ppermute | solution.py:351
  13.2 1.3 collective-permute-start.9
  14.6 2.5 %collective-permute-start.1 = (bf16[128,768]{1,0:T(8,128)(2,1)S(1)}, bf16[128,768]{1,0:T(8,128)(2,1)S(1)}, u32[]{:S(2)}, u32[]{:S(2)}) collective-permute-start(bf16[128,768]{1,0:T(8,128)(2,1)S(1)} %slice.21), channel_id=1, source_target_pairs={{16,48},{48,80},{80,112},{112,144},{144,176},{176,208},{208,240},{... | collective-permute-start | bytes 589832 | tf_op jit(solution)/shard_map/ppermute | solution.py:374
  17.1 0.0 collective-permute-done.9.refs_0_
  17.1 0.7 collective-permute-start.10
  17.8 1.9 collective-permute-done.1.refs_1_
  19.7 0.7 collective-permute-start.2
  20.4 0.7 collective-permute-start.11
  21.1 0.7 collective-permute-start.3
  21.7 3.9 %collective-permute-done.18.refs_2_ = bf16[3072,256]{1,0:T(8,128)(2,1)} collective-permute-done((bf16[3072,256]{1,0:T(8,128)(2,1)}, bf16[3072,256]{1,0:T(8,128)(2,1)}, u32[]{:S(2)}, u32[]{:S(2)}) %collective-permute-start.18) | collective-permute-done | bytes 1572896 | tf_op jit(solution)/shard_map/ppermute | solution.py:363
  25.7 5.0 %collective-permute-start.19 = (bf16[3072,256]{1,0:T(8,128)(2,1)}, bf16[3072,256]{1,0:T(8,128)(2,1)}, u32[]{:S(2)}, u32[]{:S(2)}) collective-permute-start(bf16[3072,256]{1,0:T(8,128)(2,1)} %collective-permute-done.18.refs_2_), channel_id=1, source_target_pairs={{0,4},{1,5},{2,6},{3,7},{4,8},{5,9},{6,10},{7,11},{8,12},{9,13},{1... | collective-permute-start | bytes 4718600 | tf_op jit(solution)/shard_map/ppermute | solution.py:363
  30.7 0.7 collective-permute-start.12
  31.4 0.7 collective-permute-start.4
  32.1 0.7 collective-permute-start.13
  32.8 0.7 collective-permute-start.5
  33.5 0.7 collective-permute-start.14
  34.2 0.7 collective-permute-start.6
  34.9 0.7 collective-permute-start.15
  35.6 0.7 collective-permute-start.7
  36.2 0.7 collective-permute-start.16
  36.9 0.7 collective-permute-start.8
  37.7 0.9 slice.15.own_q_ref
  38.7 0.9 slice.20.got_q_ref
  39.7 0.7 absorb.10
  40.4 0.1 absorb.11
  40.5 0.1 absorb.12
  40.5 0.1 absorb.13
  40.6 0.1 absorb.14
  40.7 0.1 absorb.15
  40.8 0.1 absorb.16
  40.8 0.1 absorb.17
  40.9 0.1 absorb.18
  41.0 0.1 absorb.19
  41.1 44.7 %collective-permute-start.17 = (f32[776,128]{1,0:T(8,128)S(1)}, f32[776,128]{1,0:T(8,128)S(1)}, u32[]{:S(2)}, u32[]{:S(2)}) collective-permute-start(f32[776,128]{1,0:T(8,128)S(1)} %get-tuple-element.55), channel_id=1, source_target_pairs={{0,16},{16,0},{32,48},{48,32},{64,80},{80,64},{96,112},{112,96},{1... | collective-permute-start | bytes 1191944 | tf_op jit(solution)/shard_map/ppermute | solution.py:383
  87.1 0.1 copy.46
  87.2 0.1 eq.68
  87.4 0.6 reduce-window.6
  88.0 1.4 fetch.1
  89.4 0.1 pad_maximum_fusion.mix_ref
  89.5 2.4 %collective-permute-start.20 = (bf16[3072,256]{1,0:T(8,128)(2,1)}, bf16[3072,256]{1,0:T(8,128)(2,1)S(1)}, u32[]{:S(2)}, u32[]{:S(2)}) collective-permute-start(bf16[3072,256]{1,0:T(8,128)(2,1)} %collective-permute-done.19.refs_3_), channel_id=1, source_target_pairs={{0,4},{1,5},{2,6},{3,7},{4,8},{5,9},{6,10},{7,11},{8,12},{9,13},{1... | collective-permute-start | bytes 4718600 | tf_op jit(solution)/shard_map/ppermute | solution.py:363
  91.9 2.2 %finish.1 = (bf16[16,128,128]{2,1,0:T(8,128)(2,1)}, bf16[128,128]{1,0:T(8,128)(2,1)S(1)}) custom-call(f32[2]{0:T(128)S(1)} %pad_maximum_fusion.mix_ref, s32[1]{0:T(128)} %bitcast.at_ref, f32[776,128]{1,0:T(8,128)S(1)} %get-tuple-element.54.own_ref, f32[776,128]{1,0:T(8,128)S(1)} %collective-permute-done.17.got_ref, f32[1,128]{1,0:T(1,128)S(1)} %bitcast.57, ...), custom_call_target="tpu_custom_call" | custom-call | flops 201326592 | tf_op jit(solution)/shard_map/finish/pallas_call | solution.py:394
  94.1 5.5 %all-to-all-start = ((bf16[16,128,128]{2,1,0:T(8,128)(2,1)}), bf16[16,128,128]{2,1,0:T(8,128)(2,1)S(1)}, u32[]{:S(2)}, u32[]{:S(2)}) async-start(bf16[16,128,128]{2,1,0:T(8,128)(2,1)} %get-tuple-element.58), calls=%async_computation | async-start | bytes 1048576 | tf_op jit(solution)/shard_map/all_to_all | solution.py:419
  99.6 0.2 slice_reduce_fusion
  99.8 0.1 eq.64
  99.9 0.1 fusion.4
  100.0 0.1 reduce_sum.51
  100.2 0.1 copy.49
  100.3 0.1 fusion.1.select_ref
  100.4 16.3 %all-to-all-done.arrived_ref = bf16[16,128,128]{2,1,0:T(8,128)(2,1)S(1)} async-done(((bf16[16,128,128]{2,1,0:T(8,128)(2,1)}), bf16[16,128,128]{2,1,0:T(8,128)(2,1)S(1)}, u32[]{:S(2)}, u32[]{:S(2)}) %all-to-all-start) | async-done | bytes 524320 | tf_op jit(solution)/shard_map/all_to_all | solution.py:419
  116.7 0.2 place.1
  117.0 24.1 %all_to_all.25 = bf16[16,32,128]{2,1,0:T(8,128)(2,1)S(1)} all-to-all(bf16[16,32,128]{2,1,0:T(8,128)(2,1)S(1)} %bitcast.54), channel_id=1, replica_groups=mesh['z'=16,'core'=2,'tp'=16] {'z'}, dimensions={0} | all-to-all | bytes 262144 | tf_op jit(solution)/shard_map/all_to_all | solution.py:445
  141.1 0.1 broadcast_in_dim.24
  141.2 20.4 %all_to_all.26.rows_ref = bf16[32,64,128]{2,1,0:T(8,128)(2,1)S(1)} all-to-all(bf16[32,64,128]{2,1,0:T(8,128)(2,1)S(1)} %bitcast.58), channel_id=1, replica_groups=mesh['z'=16,'core'=2,'tp'=16] {'core','tp'}, dimensions={0} | all-to-all | bytes 1048576 | tf_op jit(solution)/shard_map/all_to_all | solution.py:458
  161.7 3.6 %experts.1 = bf16[32,64,128]{2,1,0:T(8,128)(2,1)S(1)} custom-call(bf16[32,64,128]{2,1,0:T(8,128)(2,1)S(1)} %all_to_all.26.rows_ref, f32[1,2048]{1,0:T(1,128)S(1)} %bitcast.55, bf16[3072,256]{1,0:T(8,128)(2,1)S(1)} %collective-permute-done.20.refs_0_, bf16[3072,256]{1,0:T(8,128)(2,1)} %get-tuple-element.62.refs_1_, ...), custom_call_target="tpu_custom_call" | custom-call | flops 805306368 | tf_op jit(solution)/shard_map/experts/pallas_call | solution.py:465
  165.3 15.1 %all_to_all.27 = bf16[32,64,128]{2,1,0:T(8,128)(2,1)S(1)} all-to-all(bf16[32,64,128]{2,1,0:T(8,128)(2,1)S(1)} %experts.1), channel_id=1, replica_groups=mesh['z'=16,'core'=2,'tp'=16] {'core','tp'}, dimensions={0} | all-to-all | bytes 1048576 | tf_op jit(solution)/shard_map/all_to_all | solution.py:286
  180.4 0.1 reduce.1
  180.4 0.7 copy.51
  181.1 3.7 %all-to-all-start.4 = ((bf16[16,32,128]{2,1,0:T(8,128)(2,1)}), bf16[16,32,128]{2,1,0:T(8,128)(2,1)S(1)}, u32[]{:S(2)}, u32[]{:S(2)}) async-start(bf16[16,32,128]{2,1,0:T(8,128)(2,1)} %bitcast.31), calls=%async_computation.4 | async-start | bytes 262144 | tf_op jit(solution)/shard_map/all_to_all | solution.py:488
  184.8 0.1 select_reduce_fusion
  185.0 11.8 %all-to-all-done.4 = bf16[16,32,128]{2,1,0:T(8,128)(2,1)S(1)} async-done(((bf16[16,32,128]{2,1,0:T(8,128)(2,1)}), bf16[16,32,128]{2,1,0:T(8,128)(2,1)S(1)}, u32[]{:S(2)}, u32[]{:S(2)}) %all-to-all-start.4) | async-done | bytes 131104 | tf_op jit(solution)/shard_map/all_to_all | solution.py:488
  196.7 0.3 fusion.6
  197.0 0.6 add_convert_fusion
  (40 shorter events, 0.2 us)
Async XLA Ops:
  2.5 33.0 %copy-start = (bf16[128,1280]{1,0:T(8,128)(2,1)}, bf16[128,1280]{1,0:T(8,128)(2,1)S(1)}, u32[]{:S(2)}) copy-start(bf16[128,1280]{1,0:T(8,128)(2,1)S(1)} %get-tuple-element.34) | copy-start | bytes 983044
  2.5 23.1 %collective-permute-start.18 = (bf16[3072,256]{1,0:T(8,128)(2,1)}, bf16[3072,256]{1,0:T(8,128)(2,1)}, u32[]{:S(2)}, u32[]{:S(2)}) collective-permute-start(bf16[3072,256]{1,0:T(8,128)(2,1)} %get-tuple-element.62.refs_1_), channel_id=1, source_target_pairs={{0,4},{1,5},{2,6},{3,7},{4,8},{5,9},{6,10},{7,11},{8,12},{9,13},{1... | collective-permute-start | bytes 4718600 | tf_op jit(solution)/shard_map/ppermute | solution.py:363
  8.0 6.5 %collective-permute-start = (bf16[128,1280]{1,0:T(8,128)(2,1)S(1)}, bf16[128,1280]{1,0:T(8,128)(2,1)S(1)}, u32[]{:S(2)}, u32[]{:S(2)}) collective-permute-start(bf16[128,1280]{1,0:T(8,128)(2,1)S(1)} %get-tuple-element.34), channel_id=1, source_target_pairs={{0,16},{16,0},{32,48},{48,32},{64,80},{80,64},{96,112},{112,96},{1... | collective-permute-start | bytes 983048 | tf_op jit(solution)/shard_map/ppermute | solution.py:351
  13.2 3.9 %collective-permute-start.9 = (bf16[128,768]{1,0:T(8,128)(2,1)S(1)}, bf16[128,768]{1,0:T(8,128)(2,1)S(1)}, u32[]{:S(2)}, u32[]{:S(2)}) collective-permute-start(bf16[128,768]{1,0:T(8,128)(2,1)S(1)} %get-tuple-element.35.refs_0_), channel_id=1, source_target_pairs={{16,48},{48,80},{80,112},{112,144},{144,176},{176,208},{208,240},{... | collective-permute-start | bytes 589832 | tf_op jit(solution)/shard_map/ppermute | solution.py:373
  14.6 2.6 %copy-start.4 = (bf16[128,1280]{1,0:T(8,128)(2,1)}, bf16[128,1280]{1,0:T(8,128)(2,1)S(1)}, u32[]{:S(2)}) copy-start(bf16[128,1280]{1,0:T(8,128)(2,1)S(1)} %collective-permute-done) | copy-start | bytes 983044
  14.6 5.1 %collective-permute-start.1 = (bf16[128,768]{1,0:T(8,128)(2,1)S(1)}, bf16[128,768]{1,0:T(8,128)(2,1)S(1)}, u32[]{:S(2)}, u32[]{:S(2)}) collective-permute-start(bf16[128,768]{1,0:T(8,128)(2,1)S(1)} %slice.21), channel_id=1, source_target_pairs={{16,48},{48,80},{80,112},{112,144},{144,176},{176,208},{208,240},{... | collective-permute-start | bytes 589832 | tf_op jit(solution)/shard_map/ppermute | solution.py:374
  17.1 3.2 %collective-permute-start.10 = (bf16[128,768]{1,0:T(8,128)(2,1)S(1)}, bf16[128,768]{1,0:T(8,128)(2,1)S(1)}, u32[]{:S(2)}, u32[]{:S(2)}) collective-permute-start(bf16[128,768]{1,0:T(8,128)(2,1)S(1)} %collective-permute-done.9.refs_0_), channel_id=1, source_target_pairs={{48,80},{80,112},{112,144},{144,176},{176,208},{208,240},{240,272}... | collective-permute-start | bytes 589832 | tf_op jit(solution)/shard_map/ppermute | solution.py:373
  19.7 1.4 collective-permute-start.2
  20.4 10.3 %collective-permute-start.11 = (bf16[128,768]{1,0:T(8,128)(2,1)S(1)}, bf16[128,768]{1,0:T(8,128)(2,1)S(1)}, u32[]{:S(2)}, u32[]{:S(2)}) collective-permute-start(bf16[128,768]{1,0:T(8,128)(2,1)S(1)} %collective-permute-done.10.refs_0_), channel_id=1, source_target_pairs={{80,112},{112,144},{144,176},{176,208},{208,240},{240,272},{272,30... | collective-permute-start | bytes 589832 | tf_op jit(solution)/shard_map/ppermute | solution.py:373
  21.1 10.3 %collective-permute-start.3 = (bf16[128,768]{1,0:T(8,128)(2,1)S(1)}, bf16[128,768]{1,0:T(8,128)(2,1)S(1)}, u32[]{:S(2)}, u32[]{:S(2)}) collective-permute-start(bf16[128,768]{1,0:T(8,128)(2,1)S(1)} %collective-permute-done.2.refs_1_), channel_id=1, source_target_pairs={{80,112},{112,144},{144,176},{176,208},{208,240},{240,272},{272,30... | collective-permute-start | bytes 589832 | tf_op jit(solution)/shard_map/ppermute | solution.py:374
  25.7 63.8 %collective-permute-start.19 = (bf16[3072,256]{1,0:T(8,128)(2,1)}, bf16[3072,256]{1,0:T(8,128)(2,1)}, u32[]{:S(2)}, u32[]{:S(2)}) collective-permute-start(bf16[3072,256]{1,0:T(8,128)(2,1)} %collective-permute-done.18.refs_2_), channel_id=1, source_target_pairs={{0,4},{1,5},{2,6},{3,7},{4,8},{5,9},{6,10},{7,11},{8,12},{9,13},{1... | collective-permute-start | bytes 4718600 | tf_op jit(solution)/shard_map/ppermute | solution.py:363
  30.7 1.4 collective-permute-start.12
  31.4 1.4 collective-permute-start.4
  32.1 1.4 collective-permute-start.13
  32.8 1.4 collective-permute-start.5
  33.5 1.4 collective-permute-start.14
  34.2 1.4 collective-permute-start.6
  34.9 1.4 collective-permute-start.15
  35.6 1.4 collective-permute-start.7
  36.2 4.7 %collective-permute-start.16 = (bf16[128,768]{1,0:T(8,128)(2,1)S(1)}, bf16[128,768]{1,0:T(8,128)(2,1)S(1)}, u32[]{:S(2)}, u32[]{:S(2)}) collective-permute-start(bf16[128,768]{1,0:T(8,128)(2,1)S(1)} %collective-permute-done.15.refs_0_), channel_id=1, source_target_pairs={{240,272},{272,304},{304,336},{336,368},{368,400},{400,432},{432,4... | collective-permute-start | bytes 589832 | tf_op jit(solution)/shard_map/ppermute | solution.py:377
  36.9 4.1 %collective-permute-start.8 = (bf16[128,768]{1,0:T(8,128)(2,1)S(1)}, bf16[128,768]{1,0:T(8,128)(2,1)S(1)}, u32[]{:S(2)}, u32[]{:S(2)}) collective-permute-start(bf16[128,768]{1,0:T(8,128)(2,1)S(1)} %collective-permute-done.7.refs_1_), channel_id=1, source_target_pairs={{368,400},{400,432},{432,464},{464,496},{369,401},{401,433},{433,4... | collective-permute-start | bytes 589832 | tf_op jit(solution)/shard_map/ppermute | solution.py:378
  40.9 46.2 %copy-start.5 = (s32[128,2]{0,1:T(2,128)S(1)}, s32[128,2]{0,1:T(2,128)}, u32[]{:S(2)}) copy-start(s32[128,2]{0,1:T(2,128)} %param.33) | copy-start | bytes 3076
  41.0 50.8 %copy-start.2 = (f32[256]{0:T(256)S(1)}, f32[256]{0:T(256)}, u32[]{:S(2)}) copy-start(f32[256]{0:T(256)} %param.29) | copy-start | bytes 3076
  41.0 50.8 %copy-start.3 = (f32[128]{0:T(128)S(1)}, f32[128]{0:T(128)}, u32[]{:S(2)}) copy-start(f32[128]{0:T(128)} %param.28) | copy-start | bytes 1540
  41.1 50.7 %collective-permute-start.17 = (f32[776,128]{1,0:T(8,128)S(1)}, f32[776,128]{1,0:T(8,128)S(1)}, u32[]{:S(2)}, u32[]{:S(2)}) collective-permute-start(f32[776,128]{1,0:T(8,128)S(1)} %get-tuple-element.55), channel_id=1, source_target_pairs={{0,16},{16,0},{32,48},{48,32},{64,80},{80,64},{96,112},{112,96},{1... | collective-permute-start | bytes 1191944 | tf_op jit(solution)/shard_map/ppermute | solution.py:383
  89.5 72.2 %collective-permute-start.20 = (bf16[3072,256]{1,0:T(8,128)(2,1)}, bf16[3072,256]{1,0:T(8,128)(2,1)S(1)}, u32[]{:S(2)}, u32[]{:S(2)}) collective-permute-start(bf16[3072,256]{1,0:T(8,128)(2,1)} %collective-permute-done.19.refs_3_), channel_id=1, source_target_pairs={{0,4},{1,5},{2,6},{3,7},{4,8},{5,9},{6,10},{7,11},{8,12},{9,13},{1... | collective-permute-start | bytes 4718600 | tf_op jit(solution)/shard_map/ppermute | solution.py:363
  94.1 22.7 %all-to-all-start = ((bf16[16,128,128]{2,1,0:T(8,128)(2,1)}), bf16[16,128,128]{2,1,0:T(8,128)(2,1)S(1)}, u32[]{:S(2)}, u32[]{:S(2)}) async-start(bf16[16,128,128]{2,1,0:T(8,128)(2,1)} %get-tuple-element.58), calls=%async_computation | async-start | bytes 1048576 | tf_op jit(solution)/shard_map/all_to_all | solution.py:419
  100.2 61.5 %copy-start.1 = (f32[2048]{0:T(1024)S(1)}, f32[2048]{0:T(1024)}, u32[]{:S(2)}) copy-start(f32[2048]{0:T(1024)} %param.32) | copy-start | bytes 24580
  165.3 19.5 %copy-start.6 = (f32[128,2]{0,1:T(2,128)S(1)}, f32[128,2]{0,1:T(2,128)}, u32[]{:S(2)}) copy-start(f32[128,2]{0,1:T(2,128)} %param.34) | copy-start | bytes 3076
  181.1 15.6 %all-to-all-start.4 = ((bf16[16,32,128]{2,1,0:T(8,128)(2,1)}), bf16[16,32,128]{2,1,0:T(8,128)(2,1)S(1)}, u32[]{:S(2)}, u32[]{:S(2)}) async-start(bf16[16,32,128]{2,1,0:T(8,128)(2,1)} %bitcast.31), calls=%async_computation.4 | async-start | bytes 262144 | tf_op jit(solution)/shard_map/all_to_all | solution.py:488

commit v5 on v4

--- a/solution.py
+++ b/solution.py
@@ -235,6 +235,23 @@
     ).astype(jnp.bfloat16)
 
 
+def settle(parts_ref, out_ref):
+    lines = parts_ref.shape[0] // (2 * LINE)
+    chips, both, _ = out_ref.shape
+    slots, share = both // 2, chips // LINE
+    for core in range(2):
+        for row in range(LINE):
+            at = (core * LINE + row) * lines
+            total = parts_ref[at].astype(jnp.float32)
+            for i in range(1, lines):
+                total = total + parts_ref[at + i].astype(jnp.float32)
+            total = total.astype(jnp.bfloat16)
+            for i in range(share):
+                out_ref[row * share + i, core * slots : (core + 1) * slots] = total[
+                    i * slots : (i + 1) * slots
+                ]
+
+
 def experts(rows_ref, gain_ref, *refs):
     here, froms, out_ref, bufs, sems = refs[0], refs[1:LINE], refs[LINE], refs[LINE + 1 : -1], refs[-1]
     copies = [pltpu.make_async_copy(a, b, sems.at[i]) for i, (a, b) in enumerate(zip(froms, bufs))]
@@ -280,11 +297,6 @@
 
 def held(value):
     return pltpu.with_memory_space_constraint(value, pltpu.HBM)
-
-
-def summed_on_arrival(pieces, axis):
-    arrived = lax.all_to_all(pieces, axis, split_axis=0, concat_axis=0, tiled=True)
-    return arrived.astype(jnp.float32)
 
 
 def local(
@@ -477,14 +489,14 @@
         compiler_params=pltpu.CompilerParams(vmem_limit_bytes=24 << 20),
         name="experts",
     )(arrived, norm_gain[None, :], packed[-1], *[held(a) for a in packed[:-1]])
-    results = (
-        summed_on_arrival(parts, ("core", "tp"))
-        .reshape(2, LINE, lines, share, slot_count, columns)
-        .sum(axis=2)
-        .astype(jnp.bfloat16)
-        .transpose(1, 2, 0, 3, 4)
-        .reshape(chips, 2 * slot_count, columns)
-    )
+    results = pl.pallas_call(
+        settle,
+        out_shape=jax.ShapeDtypeStruct((chips, 2 * slot_count, columns), jnp.bfloat16),
+        in_specs=[VMEM],
+        out_specs=VMEM,
+        compiler_params=pltpu.CompilerParams(vmem_limit_bytes=4 << 20),
+        name="settle",
+    )(lax.all_to_all(parts, ("core", "tp"), split_axis=0, concat_axis=0, tiled=True))
     returned = lax.all_to_all(results, "z", split_axis=0, concat_axis=0, tiled=True)
     returned_flat = returned.reshape(seq_devices * slot_count, columns).astype(jnp.float32)
     experts_sum = jnp.dot(combine, returned_flat, precision=lax.Precision.HIGHEST)

time: 200 us -> 200 us (level)
  no operation moved by 1% of the time
where the time goes in v5:
time: 200 us; the launch traced here: 198 us
  starting transfers between devices  85.1 us (43%)
  blocking collectives  59.6 us (30%)
  waiting for transfers between devices  34 us (17%)
  Pallas kernels  12 us (6%)
  local copies, waits for them, and re-layouts  2.78 us (1%)
  between operations  2.11 us (1%)
    ppermute x1, starting transfers between devices, local(): got_state = lax.ppermute(state[1], SEQ, partner)  44.7 us
    all_to_all x1, blocking collectives, local(): lax.all_to_all(send_rows.reshape(chips, 2 * slot_count, columns), 'z', sp...  24.1 us
    all_to_all x1, blocking collectives, local(): lax.all_to_all(copies.reshape(2 * head_devices, group_rows, columns), ('c...  20.4 us
    all_to_all x1, waiting for transfers between devices, local(): lax.all_to_all(pieces, 'tp', split_axis=0, concat_axis=0, tiled=True)  16.3 us
    all_to_all x1, blocking collectives, local(): lax.all_to_all(parts, ('core', 'tp'), split_axis=0, concat_axis=0, tiled=...  15.1 us
    ppermute x3, starting transfers between devices, local(): packed.append(lax.ppermute(packed[-1], (*SEQ, 'tp'), along))  12.8 us
    all_to_all x1, waiting for transfers between devices, local(): lax.all_to_all(results, 'z', split_axis=0, concat_axis=0, tiled=True)  11.8 us
    ppermute x7, starting transfers between devices, local(): theirs = lax.ppermute(theirs, SEQ, pairs)  6.54 us
  transfers between devices with their start and end apart: 23, of which 4 were waited for; matrix products, arithmetic and copies ran while one was open for 2% of the time, Pallas kernels for 3%

profile of v5, /device:TPU:1, one launch (start us, length us, event | category | flops | bytes accessed | tf_op | source)
XLA Modules:
  0.0 197.6 jit_solution(3068226754886836837)
XLA Ops:
  0.0 2.5 %pack.1 = (bf16[128,1280]{1,0:T(8,128)(2,1)S(1)}, bf16[128,768]{1,0:T(8,128)(2,1)S(1)}, bf16[3072,256]{1,0:T(8,128)(2,1)}) custom-call(bf16[128,128]{1,0:T(8,128)(2,1)} %bitcast.65, bf16[128,256]{1,0:T(8,128)(2,1)} %bitcast.62, bf16[128,128]{1,0:T(8,128)(2,1)} %bitcast.66, bf16[128,128]{1,0:T(8,128)(2,1)} %bitcast.67, bf16[128,256]{1,0:T(8,128)(2,1)} %bitcast.63, ...), custom_call_target="tpu_custom_call" | custom-call | tf_op jit(solution)/shard_map/pack/pallas_call | solution.py:346
  2.6 5.5 %collective-permute-start.18 = (bf16[3072,256]{1,0:T(8,128)(2,1)}, bf16[3072,256]{1,0:T(8,128)(2,1)}, u32[]{:S(2)}, u32[]{:S(2)}) collective-permute-start(bf16[3072,256]{1,0:T(8,128)(2,1)} %get-tuple-element.62.refs_1_), channel_id=1, source_target_pairs={{0,4},{1,5},{2,6},{3,7},{4,8},{5,9},{6,10},{7,11},{8,12},{9,13},{1... | collective-permute-start | bytes 4718600 | tf_op jit(solution)/shard_map/ppermute | solution.py:375
  8.0 5.2 %collective-permute-start = (bf16[128,1280]{1,0:T(8,128)(2,1)S(1)}, bf16[128,1280]{1,0:T(8,128)(2,1)S(1)}, u32[]{:S(2)}, u32[]{:S(2)}) collective-permute-start(bf16[128,1280]{1,0:T(8,128)(2,1)S(1)} %get-tuple-element.34), channel_id=1, source_target_pairs={{0,16},{16,0},{32,48},{48,32},{64,80},{80,64},{96,112},{112,96},{1... | collective-permute-start | bytes 983048 | tf_op jit(solution)/shard_map/ppermute | solution.py:363
  13.2 1.3 collective-permute-start.9
  14.6 2.5 %collective-permute-start.1 = (bf16[128,768]{1,0:T(8,128)(2,1)S(1)}, bf16[128,768]{1,0:T(8,128)(2,1)S(1)}, u32[]{:S(2)}, u32[]{:S(2)}) collective-permute-start(bf16[128,768]{1,0:T(8,128)(2,1)S(1)} %slice.21), channel_id=1, source_target_pairs={{16,48},{48,80},{80,112},{112,144},{144,176},{176,208},{208,240},{... | collective-permute-start | bytes 589832 | tf_op jit(solution)/shard_map/ppermute | solution.py:386
  17.1 0.0 collective-permute-done.9.refs_0_
  17.1 0.7 collective-permute-start.10
  17.8 1.9 collective-permute-done.1.refs_1_
  19.7 0.7 collective-permute-start.2
  20.4 0.7 collective-permute-start.11
  21.1 0.7 collective-permute-start.3
  21.7 3.9 %collective-permute-done.18.refs_2_ = bf16[3072,256]{1,0:T(8,128)(2,1)} collective-permute-done((bf16[3072,256]{1,0:T(8,128)(2,1)}, bf16[3072,256]{1,0:T(8,128)(2,1)}, u32[]{:S(2)}, u32[]{:S(2)}) %collective-permute-start.18) | collective-permute-done | bytes 1572896 | tf_op jit(solution)/shard_map/ppermute | solution.py:375
  25.7 5.0 %collective-permute-start.19 = (bf16[3072,256]{1,0:T(8,128)(2,1)}, bf16[3072,256]{1,0:T(8,128)(2,1)}, u32[]{:S(2)}, u32[]{:S(2)}) collective-permute-start(bf16[3072,256]{1,0:T(8,128)(2,1)} %collective-permute-done.18.refs_2_), channel_id=1, source_target_pairs={{0,4},{1,5},{2,6},{3,7},{4,8},{5,9},{6,10},{7,11},{8,12},{9,13},{1... | collective-permute-start | bytes 4718600 | tf_op jit(solution)/shard_map/ppermute | solution.py:375
  30.7 0.7 collective-permute-start.12
  31.4 0.7 collective-permute-start.4
  32.1 0.7 collective-permute-start.13
  32.8 0.7 collective-permute-start.5
  33.5 0.7 collective-permute-start.14
  34.2 0.7 collective-permute-start.6
  34.9 0.7 collective-permute-start.15
  35.6 0.7 collective-permute-start.7
  36.3 0.7 collective-permute-start.16
  36.9 0.7 collective-permute-start.8
  37.7 0.9 slice.15.own_q_ref
  38.7 0.9 slice.20.got_q_ref
  39.7 0.7 absorb.10
  40.4 0.1 absorb.11
  40.5 0.1 absorb.12
  40.5 0.1 absorb.13
  40.6 0.1 absorb.14
  40.7 0.1 absorb.15
  40.8 0.1 absorb.16
  40.8 0.1 absorb.17
  40.9 0.0 copy-start.5
  40.9 0.1 absorb.18
  41.0 0.1 absorb.19
  41.1 44.7 %collective-permute-start.17 = (f32[776,128]{1,0:T(8,128)S(1)}, f32[776,128]{1,0:T(8,128)S(1)}, u32[]{:S(2)}, u32[]{:S(2)}) collective-permute-start(f32[776,128]{1,0:T(8,128)S(1)} %get-tuple-element.55), channel_id=1, source_target_pairs={{0,16},{16,0},{32,48},{48,32},{64,80},{80,64},{96,112},{112,96},{1... | collective-permute-start | bytes 1191944 | tf_op jit(solution)/shard_map/ppermute | solution.py:395
  87.1 0.1 copy.37
  87.2 0.1 eq.68
  87.4 0.6 reduce-window.6
  88.0 1.4 fetch.1
  89.4 0.1 pad_maximum_fusion.mix_ref
  89.5 2.4 %collective-permute-start.20 = (bf16[3072,256]{1,0:T(8,128)(2,1)}, bf16[3072,256]{1,0:T(8,128)(2,1)S(1)}, u32[]{:S(2)}, u32[]{:S(2)}) collective-permute-start(bf16[3072,256]{1,0:T(8,128)(2,1)} %collective-permute-done.19.refs_3_), channel_id=1, source_target_pairs={{0,4},{1,5},{2,6},{3,7},{4,8},{5,9},{6,10},{7,11},{8,12},{9,13},{1... | collective-permute-start | bytes 4718600 | tf_op jit(solution)/shard_map/ppermute | solution.py:375
  91.9 2.2 %finish.1 = (bf16[16,128,128]{2,1,0:T(8,128)(2,1)}, bf16[128,128]{1,0:T(8,128)(2,1)S(1)}) custom-call(f32[2]{0:T(128)S(1)} %pad_maximum_fusion.mix_ref, s32[1]{0:T(128)} %bitcast.at_ref, f32[776,128]{1,0:T(8,128)S(1)} %get-tuple-element.54.own_ref, f32[776,128]{1,0:T(8,128)S(1)} %collective-permute-done.17.got_ref, f32[1,128]{1,0:T(1,128)S(1)} %bitcast.54, ...), custom_call_target="tpu_custom_call" | custom-call | flops 201326592 | tf_op jit(solution)/shard_map/finish/pallas_call | solution.py:406
  94.1 5.5 %all-to-all-start = ((bf16[16,128,128]{2,1,0:T(8,128)(2,1)}), bf16[16,128,128]{2,1,0:T(8,128)(2,1)S(1)}, u32[]{:S(2)}, u32[]{:S(2)}) async-start(bf16[16,128,128]{2,1,0:T(8,128)(2,1)} %get-tuple-element.58), calls=%async_computation | async-start | bytes 1048576 | tf_op jit(solution)/shard_map/all_to_all | solution.py:431
  99.6 0.2 slice_reduce_fusion
  99.8 0.1 eq.64
  100.0 0.1 fusion.4
  100.0 0.1 reduce_sum.42
  100.2 0.1 copy.40
  100.3 0.1 fusion.1.select_ref
  100.4 16.3 %all-to-all-done.arrived_ref = bf16[16,128,128]{2,1,0:T(8,128)(2,1)S(1)} async-done(((bf16[16,128,128]{2,1,0:T(8,128)(2,1)}), bf16[16,128,128]{2,1,0:T(8,128)(2,1)S(1)}, u32[]{:S(2)}, u32[]{:S(2)}) %all-to-all-start) | async-done | bytes 524320 | tf_op jit(solution)/shard_map/all_to_all | solution.py:431
  116.7 0.2 place.1
  117.0 24.1 %all_to_all.25 = bf16[16,32,128]{2,1,0:T(8,128)(2,1)S(1)} all-to-all(bf16[16,32,128]{2,1,0:T(8,128)(2,1)S(1)} %bitcast.51), channel_id=1, replica_groups=mesh['z'=16,'core'=2,'tp'=16] {'z'}, dimensions={0} | all-to-all | bytes 262144 | tf_op jit(solution)/shard_map/all_to_all | solution.py:457
  141.1 0.1 broadcast_in_dim.24
  141.2 20.4 %all_to_all.26.rows_ref = bf16[32,64,128]{2,1,0:T(8,128)(2,1)S(1)} all-to-all(bf16[32,64,128]{2,1,0:T(8,128)(2,1)S(1)} %bitcast.55), channel_id=1, replica_groups=mesh['z'=16,'core'=2,'tp'=16] {'core','tp'}, dimensions={0} | all-to-all | bytes 1048576 | tf_op jit(solution)/shard_map/all_to_all | solution.py:470
  161.7 3.6 %experts.1 = bf16[32,64,128]{2,1,0:T(8,128)(2,1)S(1)} custom-call(bf16[32,64,128]{2,1,0:T(8,128)(2,1)S(1)} %all_to_all.26.rows_ref, f32[1,2048]{1,0:T(1,128)S(1)} %bitcast.52, bf16[3072,256]{1,0:T(8,128)(2,1)S(1)} %collective-permute-done.20.refs_0_, bf16[3072,256]{1,0:T(8,128)(2,1)} %get-tuple-element.62.refs_1_, ...), custom_call_target="tpu_custom_call" | custom-call | flops 805306368 | tf_op jit(solution)/shard_map/experts/pallas_call | solution.py:477
  165.3 15.1 %all_to_all.27.parts_ref = bf16[32,64,128]{2,1,0:T(8,128)(2,1)S(1)} all-to-all(bf16[32,64,128]{2,1,0:T(8,128)(2,1)S(1)} %experts.1), channel_id=1, replica_groups=mesh['z'=16,'core'=2,'tp'=16] {'core','tp'}, dimensions={0} | all-to-all | bytes 1048576 | tf_op jit(solution)/shard_map/all_to_all | solution.py:499
  180.4 0.7 settle.1
  181.1 3.7 %all-to-all-start.4 = ((bf16[16,32,128]{2,1,0:T(8,128)(2,1)}), bf16[16,32,128]{2,1,0:T(8,128)(2,1)S(1)}, u32[]{:S(2)}, u32[]{:S(2)}) async-start(bf16[16,32,128]{2,1,0:T(8,128)(2,1)} %settle.1), calls=%async_computation.4 | async-start | bytes 262144 | tf_op jit(solution)/shard_map/all_to_all | solution.py:500
  184.8 0.1 select_reduce_fusion
  184.9 11.8 %all-to-all-done.4 = bf16[16,32,128]{2,1,0:T(8,128)(2,1)S(1)} async-done(((bf16[16,32,128]{2,1,0:T(8,128)(2,1)}), bf16[16,32,128]{2,1,0:T(8,128)(2,1)S(1)}, u32[]{:S(2)}, u32[]{:S(2)}) %all-to-all-start.4) | async-done | bytes 131104 | tf_op jit(solution)/shard_map/all_to_all | solution.py:500
  196.7 0.3 fusion.6
  197.0 0.6 add_convert_fusion
  (39 shorter events, 0.2 us)
Async XLA Ops:
  2.5 33.0 %copy-start = (bf16[128,1280]{1,0:T(8,128)(2,1)}, bf16[128,1280]{1,0:T(8,128)(2,1)S(1)}, u32[]{:S(2)}) copy-start(bf16[128,1280]{1,0:T(8,128)(2,1)S(1)} %get-tuple-element.34) | copy-start | bytes 983044
  2.6 23.1 %collective-permute-start.18 = (bf16[3072,256]{1,0:T(8,128)(2,1)}, bf16[3072,256]{1,0:T(8,128)(2,1)}, u32[]{:S(2)}, u32[]{:S(2)}) collective-permute-start(bf16[3072,256]{1,0:T(8,128)(2,1)} %get-tuple-element.62.refs_1_), channel_id=1, source_target_pairs={{0,4},{1,5},{2,6},{3,7},{4,8},{5,9},{6,10},{7,11},{8,12},{9,13},{1... | collective-permute-start | bytes 4718600 | tf_op jit(solution)/shard_map/ppermute | solution.py:375
  8.0 6.5 %collective-permute-start = (bf16[128,1280]{1,0:T(8,128)(2,1)S(1)}, bf16[128,1280]{1,0:T(8,128)(2,1)S(1)}, u32[]{:S(2)}, u32[]{:S(2)}) collective-permute-start(bf16[128,1280]{1,0:T(8,128)(2,1)S(1)} %get-tuple-element.34), channel_id=1, source_target_pairs={{0,16},{16,0},{32,48},{48,32},{64,80},{80,64},{96,112},{112,96},{1... | collective-permute-start | bytes 983048 | tf_op jit(solution)/shard_map/ppermute | solution.py:363
  13.2 3.9 %collective-permute-start.9 = (bf16[128,768]{1,0:T(8,128)(2,1)S(1)}, bf16[128,768]{1,0:T(8,128)(2,1)S(1)}, u32[]{:S(2)}, u32[]{:S(2)}) collective-permute-start(bf16[128,768]{1,0:T(8,128)(2,1)S(1)} %get-tuple-element.35.refs_0_), channel_id=1, source_target_pairs={{16,48},{48,80},{80,112},{112,144},{144,176},{176,208},{208,240},{... | collective-permute-start | bytes 589832 | tf_op jit(solution)/shard_map/ppermute | solution.py:385
  14.6 2.6 %copy-start.4 = (bf16[128,1280]{1,0:T(8,128)(2,1)}, bf16[128,1280]{1,0:T(8,128)(2,1)S(1)}, u32[]{:S(2)}) copy-start(bf16[128,1280]{1,0:T(8,128)(2,1)S(1)} %collective-permute-done) | copy-start | bytes 983044
  14.6 5.1 %collective-permute-start.1 = (bf16[128,768]{1,0:T(8,128)(2,1)S(1)}, bf16[128,768]{1,0:T(8,128)(2,1)S(1)}, u32[]{:S(2)}, u32[]{:S(2)}) collective-permute-start(bf16[128,768]{1,0:T(8,128)(2,1)S(1)} %slice.21), channel_id=1, source_target_pairs={{16,48},{48,80},{80,112},{112,144},{144,176},{176,208},{208,240},{... | collective-permute-start | bytes 589832 | tf_op jit(solution)/shard_map/ppermute | solution.py:386
  17.1 3.2 %collective-permute-start.10 = (bf16[128,768]{1,0:T(8,128)(2,1)S(1)}, bf16[128,768]{1,0:T(8,128)(2,1)S(1)}, u32[]{:S(2)}, u32[]{:S(2)}) collective-permute-start(bf16[128,768]{1,0:T(8,128)(2,1)S(1)} %collective-permute-done.9.refs_0_), channel_id=1, source_target_pairs={{48,80},{80,112},{112,144},{144,176},{176,208},{208,240},{240,272}... | collective-permute-start | bytes 589832 | tf_op jit(solution)/shard_map/ppermute | solution.py:385
  19.7 1.4 collective-permute-start.2
  20.4 10.3 %collective-permute-start.11 = (bf16[128,768]{1,0:T(8,128)(2,1)S(1)}, bf16[128,768]{1,0:T(8,128)(2,1)S(1)}, u32[]{:S(2)}, u32[]{:S(2)}) collective-permute-start(bf16[128,768]{1,0:T(8,128)(2,1)S(1)} %collective-permute-done.10.refs_0_), channel_id=1, source_target_pairs={{80,112},{112,144},{144,176},{176,208},{208,240},{240,272},{272,30... | collective-permute-start | bytes 589832 | tf_op jit(solution)/shard_map/ppermute | solution.py:385
  21.1 10.3 %collective-permute-start.3 = (bf16[128,768]{1,0:T(8,128)(2,1)S(1)}, bf16[128,768]{1,0:T(8,128)(2,1)S(1)}, u32[]{:S(2)}, u32[]{:S(2)}) collective-permute-start(bf16[128,768]{1,0:T(8,128)(2,1)S(1)} %collective-permute-done.2.refs_1_), channel_id=1, source_target_pairs={{80,112},{112,144},{144,176},{176,208},{208,240},{240,272},{272,30... | collective-permute-start | bytes 589832 | tf_op jit(solution)/shard_map/ppermute | solution.py:386
  25.7 63.8 %collective-permute-start.19 = (bf16[3072,256]{1,0:T(8,128)(2,1)}, bf16[3072,256]{1,0:T(8,128)(2,1)}, u32[]{:S(2)}, u32[]{:S(2)}) collective-permute-start(bf16[3072,256]{1,0:T(8,128)(2,1)} %collective-permute-done.18.refs_2_), channel_id=1, source_target_pairs={{0,4},{1,5},{2,6},{3,7},{4,8},{5,9},{6,10},{7,11},{8,12},{9,13},{1... | collective-permute-start | bytes 4718600 | tf_op jit(solution)/shard_map/ppermute | solution.py:375
  30.7 1.4 collective-permute-start.12
  31.4 1.4 collective-permute-start.4
  32.1 1.4 collective-permute-start.13
  32.8 1.4 collective-permute-start.5
  33.5 1.4 collective-permute-start.14
  34.2 1.4 collective-permute-start.6
  34.9 1.4 collective-permute-start.15
  35.6 1.4 collective-permute-start.7
  36.3 4.7 %collective-permute-start.16 = (bf16[128,768]{1,0:T(8,128)(2,1)S(1)}, bf16[128,768]{1,0:T(8,128)(2,1)S(1)}, u32[]{:S(2)}, u32[]{:S(2)}) collective-permute-start(bf16[128,768]{1,0:T(8,128)(2,1)S(1)} %collective-permute-done.15.refs_0_), channel_id=1, source_target_pairs={{240,272},{272,304},{304,336},{336,368},{368,400},{400,432},{432,4... | collective-permute-start | bytes 589832 | tf_op jit(solution)/shard_map/ppermute | solution.py:389
  36.9 4.1 %collective-permute-start.8 = (bf16[128,768]{1,0:T(8,128)(2,1)S(1)}, bf16[128,768]{1,0:T(8,128)(2,1)S(1)}, u32[]{:S(2)}, u32[]{:S(2)}) collective-permute-start(bf16[128,768]{1,0:T(8,128)(2,1)S(1)} %collective-permute-done.7.refs_1_), channel_id=1, source_target_pairs={{368,400},{400,432},{432,464},{464,496},{369,401},{401,433},{433,4... | collective-permute-start | bytes 589832 | tf_op jit(solution)/shard_map/ppermute | solution.py:390
  40.9 46.2 %copy-start.5 = (s32[128,2]{0,1:T(2,128)S(1)}, s32[128,2]{0,1:T(2,128)}, u32[]{:S(2)}) copy-start(s32[128,2]{0,1:T(2,128)} %param.33) | copy-start | bytes 3076
  41.0 50.8 %copy-start.2 = (f32[256]{0:T(256)S(1)}, f32[256]{0:T(256)}, u32[]{:S(2)}) copy-start(f32[256]{0:T(256)} %param.29) | copy-start | bytes 3076
  41.0 50.8 %copy-start.3 = (f32[128]{0:T(128)S(1)}, f32[128]{0:T(128)}, u32[]{:S(2)}) copy-start(f32[128]{0:T(128)} %param.28) | copy-start | bytes 1540
  41.1 50.7 %collective-permute-start.17 = (f32[776,128]{1,0:T(8,128)S(1)}, f32[776,128]{1,0:T(8,128)S(1)}, u32[]{:S(2)}, u32[]{:S(2)}) collective-permute-start(f32[776,128]{1,0:T(8,128)S(1)} %get-tuple-element.55), channel_id=1, source_target_pairs={{0,16},{16,0},{32,48},{48,32},{64,80},{80,64},{96,112},{112,96},{1... | collective-permute-start | bytes 1191944 | tf_op jit(solution)/shard_map/ppermute | solution.py:395
  89.5 72.2 %collective-permute-start.20 = (bf16[3072,256]{1,0:T(8,128)(2,1)}, bf16[3072,256]{1,0:T(8,128)(2,1)S(1)}, u32[]{:S(2)}, u32[]{:S(2)}) collective-permute-start(bf16[3072,256]{1,0:T(8,128)(2,1)} %collective-permute-done.19.refs_3_), channel_id=1, source_target_pairs={{0,4},{1,5},{2,6},{3,7},{4,8},{5,9},{6,10},{7,11},{8,12},{9,13},{1... | collective-permute-start | bytes 4718600 | tf_op jit(solution)/shard_map/ppermute | solution.py:375
  94.1 22.7 %all-to-all-start = ((bf16[16,128,128]{2,1,0:T(8,128)(2,1)}), bf16[16,128,128]{2,1,0:T(8,128)(2,1)S(1)}, u32[]{:S(2)}, u32[]{:S(2)}) async-start(bf16[16,128,128]{2,1,0:T(8,128)(2,1)} %get-tuple-element.58), calls=%async_computation | async-start | bytes 1048576 | tf_op jit(solution)/shard_map/all_to_all | solution.py:431
  100.2 61.5 %copy-start.1 = (f32[2048]{0:T(1024)S(1)}, f32[2048]{0:T(1024)}, u32[]{:S(2)}) copy-start(f32[2048]{0:T(1024)} %param.32) | copy-start | bytes 24580
  165.3 19.5 %copy-start.6 = (f32[128,2]{0,1:T(2,128)S(1)}, f32[128,2]{0,1:T(2,128)}, u32[]{:S(2)}) copy-start(f32[128,2]{0,1:T(2,128)} %param.34) | copy-start | bytes 3076
  181.1 15.7 %all-to-all-start.4 = ((bf16[16,32,128]{2,1,0:T(8,128)(2,1)}), bf16[16,32,128]{2,1,0:T(8,128)(2,1)S(1)}, u32[]{:S(2)}, u32[]{:S(2)}) async-start(bf16[16,32,128]{2,1,0:T(8,128)(2,1)} %settle.1), calls=%async_computation.4 | async-start | bytes 262144 | tf_op jit(solution)/shard_map/all_to_all | solution.py:500
